TPU v7x, 32 devices: a whole 2x2x4 slice. The times are simulated.
32 devices in a mesh: sp: 8 (over z, y), tp: 4 (over x, core).
Axes of the slice: x: 2, y: 2, z: 4, core: 2. Of those that a mesh axis runs over, the one named last changes fastest.
Arguments:
- resid: bfloat16 [12288, 2048], P(('sp', 'tp')), may hold values from -6 to 6
- cond: bfloat16 [2048], P('sp'), may hold values from -6 to 6
- mod_shift: bfloat16 [2048, 2048], P('sp', 'tp'), may hold values from -0.125 to 0.125
- mod_scale: bfloat16 [2048, 2048], P('sp', 'tp'), may hold values from -0.125 to 0.125
- mod_gate: bfloat16 [2048, 2048], P('sp', 'tp'), may hold values from -0.125 to 0.125
- norm_gain: float32 [2048], replicated, may hold values from 0.1 to 1.9
- context: bfloat16 [512, 2048], P('sp'), may hold values from -6 to 6
- w_query: bfloat16 [2048, 2048], P(None, 'tp'), may hold values from -0.125 to 0.125
- w_key: bfloat16 [2048, 2048], P(None, 'tp'), may hold values from -0.125 to 0.125
- w_value: bfloat16 [2048, 2048], P(None, 'tp'), may hold values from -0.125 to 0.125
- query_gain: float32 [128], replicated, may hold values from 0.5 to 6, as said below
- key_gain: float32 [128], replicated, may hold values from 0.5 to 6, as said below
- offset_bias: float32 [16, 15, 31], P('tp'), may hold values from -4 to 4
- context_bias: float32 [16], P('tp'), may hold values from -4.5 to 1
- w_out: bfloat16 [2048, 2048], replicated, may hold values from -0.5 to 0.5
Outputs:
- mixed: bfloat16 [12288, 2048], P(('sp', 'tp'))
Inputs may be any that keep to these rules, and one draw needn't show every extreme that they name: `query_gain`: positive gains. `key_gain`: positive gains.
All inputs are finite; a program needn't handle non-finite values.
Results may differ from a plain program's by a relative error of at most 0.0085.
The roundings to bfloat16 on the way count: a program that leaves them out, or rounds other values in their place, can miss the bound.
Values may be sent and summed in bfloat16 or wider, within the bound.
No kernel may reach another device: no remote copies, remote signals or barrier semaphores. Data moves between devices by JAX's collectives and lax.ppermute only.
A program may use at most 128 MiB of HBM per device.

v0:
```python
import jax
import jax.numpy as jnp
from jax import lax
from jax.sharding import PartitionSpec as P

HEAD_DIM = 128
GRID_W = 64
WIN_ROWS = 8
WIN_COLS = 16
R_DEV = 24


EPS = 1e-06


def padded_2(cells, sides, width):
    for axis, dim in sides:
        count = lax.axis_size(axis)
        ends = count - 1
        head = lax.slice_in_dim(cells, 0, width, axis=dim)
        tail = lax.slice_in_dim(cells, cells.shape[dim] - width, cells.shape[dim], axis=dim)
        cells = jnp.concatenate(
            [
                lax.ppermute(tail, axis, [(i, (i + 1) % count) for i in range(ends)]),
                cells,
                lax.ppermute(head, axis, [((i + 1) % count, i) for i in range(ends)]),
            ],
            axis=dim,
        )
    return cells


def head_norm(values, gain, heads_local):
    count = values.shape[0]
    split = values.reshape(count, heads_local, -1)
    scaled = split * lax.rsqrt(jnp.mean(split * split, axis=-1, keepdims=True) + EPS) * gain
    return scaled.reshape(count, -1).astype(jnp.bfloat16)


def project_context(rows_in, norm_gain, w_key, w_value, key_gain, heads_local):
    floats = rows_in.astype(jnp.float32)
    inverse = lax.rsqrt(jnp.mean(floats * floats, axis=-1, keepdims=True) + EPS)
    normed = (floats * inverse * norm_gain).astype(jnp.bfloat16)
    keys = head_norm(
        jnp.dot(normed, w_key, preferred_element_type=jnp.float32), key_gain, heads_local
    )
    values = jnp.dot(normed, w_value, preferred_element_type=jnp.float32).astype(jnp.bfloat16)
    return (keys, values)


def attend_rows(
    queries, key_at, value_at, row_offset, offset_bias, ctx_key, ctx_value, context_bias
):
    grid_w = queries.shape[1]
    columns = jnp.arange(grid_w, dtype=jnp.int32)
    col_begin = jnp.clip(columns - WIN_COLS // 2, 0, grid_w - WIN_COLS)
    valid = (columns[None, :] >= col_begin[:, None]) & (
        columns[None, :] < col_begin[:, None] + WIN_COLS
    )
    col_offset = jnp.clip(columns[None, :] - columns[:, None] + WIN_COLS - 1, 0, 2 * WIN_COLS - 2)
    col_onehot = (col_offset[..., None] == jnp.arange(2 * WIN_COLS - 1, dtype=jnp.int32)).astype(
        jnp.float32
    )
    row_onehot = (
        row_offset[:, :, None] == jnp.arange(2 * WIN_ROWS - 1, dtype=jnp.int32)[None, None, :]
    ).astype(jnp.float32)
    bias = jnp.einsum(
        "nir,hrj,ckj->nhcik", row_onehot, offset_bias, col_onehot, precision=lax.Precision.HIGHEST
    )
    factor = HEAD_DIM ** (-0.5)
    s_win = (
        jnp.stack(
            [
                jnp.einsum(
                    "nchd,nkhd->nhck", queries, key_at(i), preferred_element_type=jnp.float32
                )
                for i in range(WIN_ROWS)
            ],
            axis=3,
        )
        * factor
        + bias
    )
    s_win = jnp.where(valid[None, None, :, None, :], s_win, -1e30)
    s_ctx = (
        jnp.einsum("nchd,jhd->nhcj", queries, ctx_key, preferred_element_type=jnp.float32) * factor
    )
    s_ctx = s_ctx + context_bias[None, :, None, None]
    top = jnp.maximum(jnp.max(s_win, axis=(3, 4)), jnp.max(s_ctx, axis=3))
    e_win = jnp.exp(s_win - top[..., None, None])
    e_ctx = jnp.exp(s_ctx - top[..., None])
    total = jnp.sum(e_win, axis=(3, 4)) + jnp.sum(e_ctx, axis=3)
    p_win = (e_win / total[..., None, None]).astype(jnp.bfloat16)
    p_ctx = (e_ctx / total[..., None]).astype(jnp.bfloat16)
    out = jnp.einsum("nhcj,jhd->nchd", p_ctx, ctx_value, preferred_element_type=jnp.float32)
    for i in range(WIN_ROWS):
        out = out + jnp.einsum(
            "nhck,nkhd->nchd", p_win[:, :, :, i], value_at(i), preferred_element_type=jnp.float32
        )
    count = queries.shape[0]
    return out.astype(jnp.bfloat16).reshape(count * grid_w, -1)


def shards(
    resid,
    cond,
    mod_shift,
    mod_scale,
    mod_gate,
    norm_gain,
    context,
    w_query,
    w_key,
    w_value,
    query_gain,
    key_gain,
    offset_bias,
    context_bias,
    w_out,
):
    heads_local = offset_bias.shape[0]
    width = w_query.shape[1]
    lifted = jax.nn.silu(cond.astype(jnp.float32)).astype(jnp.bfloat16)
    shift_part = jnp.dot(lifted, mod_shift, preferred_element_type=jnp.float32)
    scale_part = jnp.dot(lifted, mod_scale, preferred_element_type=jnp.float32)
    gate_part = jnp.dot(lifted, mod_gate, preferred_element_type=jnp.float32)
    summed = lax.psum((shift_part, scale_part, gate_part), "sp")
    shift, scale, gate = (
        lax.all_gather(summed[0], "tp", axis=0, tiled=True),
        lax.all_gather(summed[1], "tp", axis=0, tiled=True),
        lax.all_gather(summed[2], "tp", axis=0, tiled=True),
    )
    floats = resid.astype(jnp.float32)
    inverse = lax.rsqrt(jnp.mean(floats * floats, axis=-1, keepdims=True) + EPS)
    normed = (floats * inverse * norm_gain * (1.0 + scale) + shift).astype(jnp.bfloat16)
    piece = lax.all_gather(normed, "tp", axis=0, tiled=True)
    queries = head_norm(
        jnp.dot(piece, w_query, preferred_element_type=jnp.float32), query_gain, heads_local
    )
    keys = head_norm(
        jnp.dot(piece, w_key, preferred_element_type=jnp.float32), key_gain, heads_local
    )
    values = jnp.dot(piece, w_value, preferred_element_type=jnp.float32).astype(jnp.bfloat16)
    projected = jnp.concatenate([queries, keys, values], axis=1)
    query = projected[:, :width]
    key_value = projected[:, width:]
    keys, values = project_context(
        lax.all_gather(context, "sp", axis=0, tiled=True),
        norm_gain,
        w_key,
        w_value,
        key_gain,
        heads_local,
    )
    ctx_both = jnp.concatenate([keys, values], axis=1)
    ctx_key = ctx_both[:, :width]
    ctx_value = ctx_both[:, width:]
    ctx_count = ctx_key.shape[0]
    ctx_key = ctx_key.reshape(ctx_count, heads_local, HEAD_DIM)
    ctx_value = ctx_value.reshape(ctx_count, heads_local, HEAD_DIM)
    reach = WIN_ROWS // 2
    grid = key_value.reshape(R_DEV, GRID_W, 2 * width)
    padded = padded_2(grid, (("sp", 0),), reach)
    padded = padded.reshape(R_DEV + 2 * reach, GRID_W, 2, heads_local, HEAD_DIM)
    total_rows = R_DEV * lax.axis_size("sp")
    first = lax.axis_index("sp") * R_DEV
    global_rows = first + jnp.arange(R_DEV, dtype=jnp.int32)
    row_start = jnp.clip(global_rows - reach, 0, total_rows - WIN_ROWS)
    window_rows = jnp.arange(WIN_ROWS, dtype=jnp.int32)[None, :]
    row_offset = row_start[:, None] + window_rows - global_rows[:, None] + WIN_ROWS - 1
    queries = query.reshape(R_DEV, GRID_W, heads_local, HEAD_DIM)
    upper = min(reach, R_DEV)
    lower = max(upper, R_DEV - reach)
    edge_rows = list(range(upper)) + list(range(lower, R_DEV))
    edge_index = jnp.array(edge_rows, dtype=jnp.int32)
    edge_window = (jnp.take(row_start, edge_index) - first + reach)[:, None] + window_rows
    edge_kv = jnp.take(padded, edge_window, axis=0)
    edge_out = attend_rows(
        jnp.take(queries, edge_index, axis=0),
        lambda i: edge_kv[:, i, :, 0],
        lambda i: edge_kv[:, i, :, 1],
        jnp.take(row_offset, edge_index, axis=0),
        offset_bias,
        ctx_key,
        ctx_value,
        context_bias,
    )
    pieces = [edge_out[: upper * GRID_W]]
    middle = lower - upper
    inner_out = attend_rows(
        queries[upper:lower],
        lambda i: padded[upper + i : upper + i + middle, :, 0],
        lambda i: padded[upper + i : upper + i + middle, :, 1],
        row_offset[upper:lower],
        offset_bias,
        ctx_key,
        ctx_value,
        context_bias,
    )
    pieces.append(inner_out)
    pieces.append(edge_out[upper * GRID_W :])
    attended = jnp.concatenate(pieces, axis=0)
    full_rows = lax.all_to_all(attended, "tp", split_axis=0, concat_axis=1, tiled=True)
    result = jnp.dot(full_rows, w_out, preferred_element_type=jnp.float32)
    return (floats + gate * result).astype(jnp.bfloat16)


def solution(mesh):
    in_specs = (
        P(("sp", "tp"), None),
        P("sp"),
        P("sp", "tp"),
        P("sp", "tp"),
        P("sp", "tp"),
        P(),
        P("sp", None),
        P(None, "tp"),
        P(None, "tp"),
        P(None, "tp"),
        P(),
        P(),
        P("tp", None, None),
        P("tp"),
        P(),
    )
    out_specs = P(("sp", "tp"), None)
    return jax.shard_map(shards, mesh=mesh, in_specs=in_specs, out_specs=out_specs, check_vma=False)
```

profile of v0, /device:TPU:0, one launch (start us, length us, event | category | flops | bytes accessed | tf_op | source)
XLA Modules:
  0.0 350.9 jit_solution(10941702433033910941)
XLA Ops:
  11.3 24.2 %all-reduce = (f32[512]{0:T(512)S(1)}, f32[512]{0:T(512)S(1)}, f32[512]{0:T(512)}) all-reduce(f32[512]{0:T(512)S(1)} %bitcast.429, f32[512]{0:T(512)S(1)} %bitcast.430, f32[512]{0:T(512)S(1)} %bitcast.431), channel_id=1, replica_groups=mesh['sp'=8,'tp'=4] {'sp'}, use_global_device_ids=true, to_apply=%region_5.6 | all-reduce | flops 1536 | bytes 12288 | tf_op jit(solution)/shard_map/psum | solution.py:127
  35.4 5.2 %all-gather.2 = f32[4,1,512]{2,1,0:T(1,128)S(1)} all-gather(f32[1,1,512]{2,1,0:T(1,128)S(1)} %bitcast.435), channel_id=1, replica_groups=mesh['sp'=8,'tp'=4] {'tp'}, dimensions={0}, use_global_device_ids=true | all-gather | bytes 10240 | tf_op jit(solution)/shard_map/all_gather | solution.py:129
  40.6 5.2 %all-gather.1 = f32[4,1,512]{2,1,0:T(1,128)S(1)} all-gather(f32[1,1,512]{2,1,0:T(1,128)S(1)} %bitcast.434), channel_id=1, replica_groups=mesh['sp'=8,'tp'=4] {'tp'}, dimensions={0}, use_global_device_ids=true | all-gather | bytes 10240 | tf_op jit(solution)/shard_map/all_gather | solution.py:130
  47.6 3.2 fusion.16
  54.6 6.0 %fusion.25 = f32[64,64,4,8,8]{1,4,3,2,0:T(8,128)} fusion(f32[64,64,4,15]{1,3,2,0:T(8,128)S(1)} %fusion.64, s32[8,8]{1,0:T(8,128)S(1)} %gather_fusion.3), kind=kOutput, calls=%fused_computation.68 | convolution fusion | flops 188744640 | bytes 5177600 | tf_op jit(solution)/shard_map/nir,hrj,ckj->nhcik/dot_general | solution.py:67
  60.5 9.6 %copy.413 = f32[64,64,4,8,8]{0,1,2,3,4:T(8,128)} copy(f32[64,64,4,8,8]{1,4,3,2,0:T(8,128)} %fusion.25) | data formatting | bytes 8388608 | tf_op jit(solution)/shard_map/nir,hrj,ckj->nhcik/dot_general | solution.py:67
  70.4 12.2 %fusion.23 = f32[64,64,4,16,8]{1,3,4,2,0:T(8,128)} fusion(f32[64,64,4,15]{1,3,2,0:T(8,128)} %copy-done.7, s32[16,8]{0,1:T(8,128)S(1)} %copy.455), kind=kOutput, calls=%fused_computation.66 | convolution fusion | flops 377489280 | bytes 9372160 | tf_op jit(solution)/shard_map/nir,hrj,ckj->nhcik/dot_general | solution.py:67
  82.6 18.2 %copy.456 = f32[64,64,4,16,8]{0,1,2,3,4:T(8,128)} copy(f32[64,64,4,16,8]{1,3,4,2,0:T(8,128)} %fusion.23) | data formatting | bytes 16777216 | tf_op jit(solution)/shard_map/nir,hrj,ckj->nhcik/dot_general | solution.py:67
  103.1 3.1 bitcast_reduce_fusion.4
  109.5 6.7 %bitcast_reduce_fusion.2 = (f32[1536,4]{0,1:T(4,128)S(1)}, f32[1536,512]{0,1:T(8,128)S(1)}) fusion(bf16[1536,2048]{1,0:T(8,128)(2,1)} %all-gather.8.cloned.1.call-done, bf16[2048,512]{1,0:T(8,128)(2,1)S(1)} %copy-done), kind=kOutput, calls=%fused_computation.51 | convolution fusion | flops 3222792192 | bytes 11558912 | tf_op jit(solution)/shard_map/dot_general | solution.py:141
  117.8 3.5 convolution_convert_fusion
  122.5 2.9 copy.406
  125.4 4.7 %concatenate.18 = bf16[24,64,2,4,128]{4,3,2,1,0:T(4,128)(2,1)S(1)} reshape(bf16[1536,1024]{1,0:T(8,128)(2,1)} %copy.406) | data formatting | bytes 6291456 | tf_op jit(solution)/shard_map/concatenate | solution.py:22
  132.8 8.2 %fusion.117 = (bf16[16,64,1,4,128]{4,3,2,1,0:T(4,128)(2,1)}, bf16[16,64,1,4,128]{4,3,2,1,0:T(4,128)(2,1)}, bf16[16,64,1,4,128]{4,3,2,1,0:T(4,128)(2,1)}, bf16[16...) fusion(bf16[24,64,2,4,128]{4,3,2,1,0:T(4,128)(2,1)S(1)} %concat, ...), kind=kLoop, calls=%fused_computation.262 | loop fusion | bytes 33554432 | tf_op jit(solution)/shard_map/slice | solution.py:193
  140.9 3.7 %bitcast_reduce_fusion.3 = (f32[1536,4]{0,1:T(4,128)S(1)}, f32[1536,512]{0,1:T(8,128)S(1)}) fusion(bf16[1536,2048]{1,0:T(8,128)(2,1)S(1)} %bitcast.437, bf16[2048,512]{1,0:T(8,128)(2,1)S(1)} %copy-done.38), kind=kOutput, calls=%fused_computation.55 | convolution fusion | flops 3222792192 | bytes 11558912 | tf_op jit(solution)/shard_map/dot_general | solution.py:138
  145.1 3.2 reshape.343
  159.1 6.5 %copy-done.6 = f32[16,4,64,8,64]{2,4,1,0,3:T(8,128)} copy-done((f32[16,4,64,8,64]{2,4,1,0,3:T(8,128)}, f32[16,4,64,8,64]{2,4,1,0,3:T(8,128)S(1)}, u32[]{:S(2)}) %copy-start.6) | copy-done | bytes 8388632
  167.8 4.5 %slice-done.5 = s8[4194304]{0:T(1024)(128)(4,1)S(1)} async-done(((s8[16777216]{0:T(1024)(128)(4,1)}), s8[4194304]{0:T(1024)(128)(4,1)S(1)}, s32[]{:S(2)}) %slice-start.5) | async-done | bytes 4194328
  172.3 13.0 %fusion.113 = (f32[16,4,64]{2,1,0:T(4,128)S(1)}, f32[16,4,64,8,64]{2,4,1,0,3:T(8,128)}) fusion(f32[64,64,4,16,8]{0,1,2,3,4:T(8,128)S(1)} %bitcast.409, f32[16,4,64,8,64]{2,4,1,0,3:T(8,128)} %copy-done.6, pred[64,64]{0,1:T(8,128)(4,1)S(1)} %fusion.101), kind=kLoop, calls=%fused_computation.260 | loop fusion | flops 8384512 | bytes 25186304 | tf_op jit(solution)/shard_map/reduce_max | solution.py:89
  187.8 3.3 copy.402
  198.7 5.4 %collective-permute-start = (bf16[4,64,1024]{2,1,0:T(8,128)(2,1)}, bf16[4,64,1024]{2,1,0:T(8,128)(2,1)}, u32[]{:S(2)}, u32[]{:S(2)}) collective-permute-start(bf16[4,64,1024]{2,1,0:T(8,128)(2,1)} %bitcast.24), channel_id=1, source_target_pairs={{0,4},{4,8},{8,12},{12,16},{16,20},{20,24},{24,28},{1,5},{5,9},{9,... | collective-permute-start | bytes 1572872 | tf_op jit(solution)/shard_map/ppermute | solution.py:24
  204.0 8.6 %fusion.1 = f32[16,4,64]{2,1,0:T(4,128)S(1)} fusion(f32[16,4,64,8,64]{2,4,1,0,3:T(8,128)} %get-tuple-element.9, f32[16,4,64]{2,1,0:T(4,128)S(1)} %copy.458), kind=kLoop, calls=%fused_computation.8 | loop fusion | flops 4190208 | bytes 8421376 | tf_op jit(solution)/shard_map/reduce_sum | solution.py:92
  212.6 7.7 %divide_convert_fusion = bf16[16,4,64,8,64]{2,4,1,0,3:T(8,128)(2,1)S(1)} fusion(f32[16,4,64,8,64]{2,4,1,0,3:T(8,128)} %get-tuple-element.9, f32[16,4,64]{2,1,0:T(4,128)S(1)} %copy.462, f32[16,4,64]{2,1,0:T(4,128)S(1)} %copy.458), kind=kLoop, calls=%fused_computation.6 | loop fusion | flops 6291456 | bytes 12615680 | tf_op jit(solution)/shard_map/convert_element_type | solution.py:93
  223.8 2.7 fusion.10
  240.2 3.7 %pad_maximum_fusion = bf16[32,64,2,4,128]{4,1,3,2,0:T(8,128)(2,1)} fusion(bf16[4,64,2,4,128]{4,1,3,2,0:T(8,128)(2,1)S(1)} %copy.410, bf16[24,64,2,4,128]{4,1,3,2,0:T(8,128)(2,1)} %copy.409, bf16[4,64,2,4,128]{4,1,3,2,0:T(8,128)(2,1)S(1)} %copy.408), kind=kLoop, calls=%fused_computation.29 | loop fusion | flops 4194304 | bytes 8388608 | tf_op jit(solution)/shard_map/concatenate | solution.py:22
  243.9 8.1 %gather_fusion.2 = bf16[64,64,2,4,128]{4,1,3,2,0:T(8,128)(2,1)} fusion(bf16[32,64,2,4,128]{4,1,3,2,0:T(8,128)(2,1)} %pad_maximum_fusion, s32[1024]{0:T(1024)S(1)} %pad_clamp_fusion), kind=kCustom, calls=%fused_computation.2 | custom fusion | bytes 16777472 | tf_op jit(solution)/shard_map/jit(_take)/gather | solution.py:177
  252.0 7.5 %copy_select_fusion = bf16[8,8,64,2,4,128]{5,2,4,0,3,1:T(8,128)(2,1)} fusion(bf16[8,8,64,2,4,128]{5,2,4,3,1,0:T(8,128)(2,1)} %bitcast.415, pred[8,8]{0,1:T(8,128)(4,1)S(1)} %fusion.107), kind=kLoop, calls=%fused_computation.14 | loop fusion | flops 4194304 | bytes 16777280 | tf_op jit(solution)/shard_map/jit(_take)/select_n | solution.py:177
  278.9 12.4 %fusion.115 = (f32[8,4,64]{2,1,0:T(4,128)S(1)}, f32[8,4,64,8,64]{2,4,1,0,3:T(8,128)}) fusion(f32[64,64,4,8,8]{0,1,2,3,4:T(8,128)} %copy.413, f32[8,4,64,8,64]{2,4,1,0,3:T(8,128)} %fusion.37, pred[64,64]{0,1:T(8,128)(4,1)S(1)} %fusion.101), kind=kLoop, calls=%fused_computation.261 | loop fusion | flops 4192256 | bytes 12595200 | tf_op jit(solution)/shard_map/reduce_max | solution.py:89
  292.6 4.9 %fusion.4 = f32[8,4,64]{2,1,0:T(4,128)S(1)} fusion(f32[8,4,64,8,64]{2,4,1,0,3:T(8,128)} %get-tuple-element.11, f32[8,4,64]{2,1,0:T(4,128)S(1)} %copy.415), kind=kLoop, calls=%fused_computation.19 | loop fusion | flops 2095104 | bytes 4210688 | tf_op jit(solution)/shard_map/reduce_sum | solution.py:92
  309.5 4.3 %all-to-all-start = ((bf16[4,384,512]{1,2,0:T(8,128)(2,1)}), bf16[4,384,512]{1,2,0:T(8,128)(2,1)}, u32[]{:S(2)}, u32[]{:S(2)}) async-start(bf16[4,384,512]{1,2,0:T(8,128)(2,1)} %copy.480), calls=%async_computation | async-start | bytes 3145728 | tf_op jit(solution)/shard_map/all_to_all | solution.py:203
  313.8 21.0 %all-gather = f32[4,1,512]{2,1,0:T(1,128)S(1)} all-gather(f32[1,1,512]{2,1,0:T(1,128)S(1)} %bitcast.433), channel_id=1, replica_groups=mesh['sp'=8,'tp'=4] {'tp'}, dimensions={0}, use_global_device_ids=true | all-gather | bytes 10240 | tf_op jit(solution)/shard_map/all_gather | solution.py:131
  334.8 9.1 %fusion.17 = bf16[384,2048]{1,0:T(8,128)(2,1)} fusion(bf16[384,2048]{1,0:T(8,128)(2,1)} %param.16, bf16[384,2048]{0,1:T(8,128)(2,1)} %bitcast.128, bf16[2048,2048]{1,0:T(8,128)(2,1)} %param.30, f32[2048]{0:T(1024)S(1)} %bitcast.432), kind=kOutput, calls=%fused_computation.47 | convolution fusion | flops 3224371200 | bytes 13115392 | tf_op jit(solution)/shard_map/dot_general | solution.py:204
  (224 shorter events, 93.8 us)
Async XLA Ops:
  6.5 96.5 %copy-start = (bf16[2048,512]{1,0:T(8,128)(2,1)S(1)}, bf16[2048,512]{1,0:T(8,128)(2,1)}, u32[]{:S(2)}) copy-start(bf16[2048,512]{1,0:T(8,128)(2,1)} %param.24) | copy-start | bytes 6291460
  6.5 44.3 %copy-start.34 = (s32[8]{0:T(128)S(1)}, s32[8]{0:T(128)}, u32[]{:S(2)}) copy-start(s32[8]{0:T(128)} %constant.131) | copy-start | bytes 100
  6.5 45.7 %copy-start.28 = (f32[4,15,31]{2,0,1:T(4,128)S(1)}, f32[4,15,31]{2,0,1:T(4,128)}, u32[]{:S(2)}) copy-start(f32[4,15,31]{2,0,1:T(4,128)} %param.28) | copy-start | bytes 22324
  6.5 94.4 %all-gather.6.cloned.1.call-start = ((), (), s32[]{:S(2)}) async-start(), calls=%async_computation.1 | async-start | bytes 2359296 | tf_op jit(solution)/shard_map/all_gather | solution.py:148
  7.3 102.3 %all-gather.8.cloned.1.call-start = ((), (), s32[]{:S(2)}) async-start(), calls=%async_computation.2 | async-start | bytes 7864320 | tf_op jit(solution)/shard_map/all_gather | solution.py:136
  82.6 18.3 %copy-start.32 = (f32[128]{0:T(128)S(1)}, f32[128]{0:T(128)}, u32[]{:S(2)}) copy-start(f32[128]{0:T(128)} %param.26) | copy-start | bytes 1540
  82.6 18.3 %copy-start.33 = (f32[128]{0:T(128)S(1)}, f32[128]{0:T(128)}, u32[]{:S(2)}) copy-start(f32[128]{0:T(128)} %param.27) | copy-start | bytes 1540
  82.6 20.4 %copy-start.29 = (f32[2048]{0:T(1024)S(1)}, f32[2048]{0:T(1024)}, u32[]{:S(2)}) copy-start(f32[2048]{0:T(1024)} %param.21) | copy-start | bytes 24580
  103.1 4.2 %copy-start.27 = (bf16[512,2048]{1,0:T(8,128)(2,1)S(1)}, bf16[512,2048]{1,0:T(8,128)(2,1)}, u32[]{:S(2)}) copy-start(bf16[512,2048]{1,0:T(8,128)(2,1)} %all-gather.6.cloned.1.call-done) | copy-start | bytes 6291460
  103.1 4.2 %copy-start.36 = (bf16[2048,512]{1,0:T(8,128)(2,1)S(1)}, bf16[2048,512]{1,0:T(8,128)(2,1)}, u32[]{:S(2)}) copy-start(bf16[2048,512]{1,0:T(8,128)(2,1)} %param.25) | copy-start | bytes 6291460
  109.5 7.1 %copy-start.35 = (bf16[1536,2048]{1,0:T(8,128)(2,1)S(1)}, bf16[1536,2048]{1,0:T(8,128)(2,1)}, u32[]{:S(2)}) copy-start(bf16[1536,2048]{1,0:T(8,128)(2,1)} %all-gather.8.cloned.1.call-done) | copy-start | bytes 18874372
  130.1 10.8 %slice-start.8 = ((s8[6291456]{0:T(1024)(128)(4,1)}), s8[4194304]{0:T(1024)(128)(4,1)S(1)}, s32[]{:S(2)}) async-start(s8[6291456]{0:T(1024)(128)(4,1)} %bitcast.436), calls=%async_computation.11 | async-start | bytes 8388608
  132.7 8.2 %slice-start.9 = ((s8[6291456]{0:T(1024)(128)(4,1)}), s8[2097152]{0:T(1024)(128)(4,1)S(1)}, s32[]{:S(2)}) async-start(s8[6291456]{0:T(1024)(128)(4,1)} %bitcast.436), calls=%async_computation.12 | async-start | bytes 4194304
  132.7 8.2 %copy-start.38 = (bf16[2048,512]{1,0:T(8,128)(2,1)S(1)}, bf16[2048,512]{1,0:T(8,128)(2,1)}, u32[]{:S(2)}) copy-start(bf16[2048,512]{1,0:T(8,128)(2,1)} %param.23) | copy-start | bytes 6291460
  148.3 5.3 %copy-start.26 = (bf16[16,64,1,4,128]{4,3,2,1,0:T(4,128)(2,1)S(1)}, bf16[16,64,1,4,128]{4,3,2,1,0:T(4,128)(2,1)}, u32[]{:S(2)}) copy-start(bf16[16,64,1,4,128]{4,3,2,1,0:T(4,128)(2,1)} %get-tuple-element.50) | copy-start | bytes 3145732
  157.0 10.8 %slice-start.2 = ((s8[16777216]{0:T(1024)(128)(4,1)}), s8[4194304]{0:T(1024)(128)(4,1)S(1)}, s32[]{:S(2)}) async-start(s8[16777216]{0:T(1024)(128)(4,1)} %bitcast.408), calls=%async_computation.5 | async-start | bytes 8388608
  157.7 7.9 %copy-start.9 = (bf16[512,512]{0,1:T(8,128)(2,1)S(1)}, bf16[512,512]{0,1:T(8,128)(2,1)}, u32[]{:S(2)}) copy-start(bf16[512,512]{0,1:T(8,128)(2,1)} %fusion.62) | copy-start | bytes 1572868
  157.7 10.1 %slice-start.3 = ((s8[16777216]{0:T(1024)(128)(4,1)}), s8[4194304]{0:T(1024)(128)(4,1)S(1)}, s32[]{:S(2)}) async-start(s8[16777216]{0:T(1024)(128)(4,1)} %bitcast.408), calls=%async_computation.6 | async-start | bytes 8388608
  159.1 6.5 %copy-start.6 = (f32[16,4,64,8,64]{2,4,1,0,3:T(8,128)}, f32[16,4,64,8,64]{2,4,1,0,3:T(8,128)S(1)}, u32[]{:S(2)}) copy-start(f32[16,4,64,8,64]{2,4,1,0,3:T(8,128)S(1)} %bitcast_dynamic-update-slice_fusion) | copy-start | bytes 25165828
  166.8 18.5 %copy-start.2 = (f32[4,512,1024]{1,2,0}, f32[4,512,1024]{1,2,0:S(1)}, u32[]{:S(2)}) copy-start(f32[4,512,1024]{1,2,0:S(1)} %fusion.123) | copy-start | bytes 25165828
  166.8 5.5 %slice-start.5 = ((s8[16777216]{0:T(1024)(128)(4,1)}), s8[4194304]{0:T(1024)(128)(4,1)S(1)}, s32[]{:S(2)}) async-start(s8[16777216]{0:T(1024)(128)(4,1)} %bitcast.408), calls=%async_computation.8 | async-start | bytes 8388608
  195.3 41.8 %collective-permute-start.1 = (bf16[4,64,1024]{2,1,0:T(8,128)(2,1)}, bf16[4,64,1024]{2,1,0:T(8,128)(2,1)}, u32[]{:S(2)}, u32[]{:S(2)}) collective-permute-start(bf16[4,64,1024]{2,1,0:T(8,128)(2,1)} %bitcast.25), channel_id=1, source_target_pairs={{4,0},{8,4},{12,8},{16,12},{20,16},{24,20},{28,24},{5,1},{9,5},{13... | collective-permute-start | bytes 1572872 | tf_op jit(solution)/shard_map/ppermute | solution.py:26
  198.7 40.0 %collective-permute-start = (bf16[4,64,1024]{2,1,0:T(8,128)(2,1)}, bf16[4,64,1024]{2,1,0:T(8,128)(2,1)}, u32[]{:S(2)}, u32[]{:S(2)}) collective-permute-start(bf16[4,64,1024]{2,1,0:T(8,128)(2,1)} %bitcast.24), channel_id=1, source_target_pairs={{0,4},{4,8},{8,12},{12,16},{16,20},{20,24},{24,28},{1,5},{5,9},{9,... | collective-permute-start | bytes 1572872 | tf_op jit(solution)/shard_map/ppermute | solution.py:24
  220.3 3.4 copy-start.39
  278.9 12.4 %copy-start.5 = (f32[4,512,512]{1,2,0:S(1)}, f32[4,512,512]{1,2,0}, u32[]{:S(2)}) copy-start(f32[4,512,512]{1,2,0} %copy-done.4) | copy-start | bytes 12582916
  291.3 6.2 %copy-start.40 = (bf16[512,512]{0,1:T(8,128)(2,1)S(1)}, bf16[512,512]{0,1:T(8,128)(2,1)}, u32[]{:S(2)}) copy-start(bf16[512,512]{0,1:T(8,128)(2,1)} %convolution_convert_fusion.1) | copy-start | bytes 1572868
  292.6 6.8 %slice-start.6 = ((s8[8388608]{0:T(1024)(128)(4,1)}), s8[4194304]{0:T(1024)(128)(4,1)S(1)}, s32[]{:S(2)}) async-start(s8[8388608]{0:T(1024)(128)(4,1)} %bitcast.413), calls=%async_computation.9 | async-start | bytes 8388608
  292.6 8.4 %slice-start = ((s8[8388608]{0:T(1024)(128)(4,1)}), s8[4194304]{0:T(1024)(128)(4,1)S(1)}, s32[]{:S(2)}) async-start(s8[8388608]{0:T(1024)(128)(4,1)} %bitcast.403), calls=%async_computation.3 | async-start | bytes 8388608
  297.6 3.6 %slice-start.1 = ((s8[8388608]{0:T(1024)(128)(4,1)}), s8[4194304]{0:T(1024)(128)(4,1)S(1)}, s32[]{:S(2)}) async-start(s8[8388608]{0:T(1024)(128)(4,1)} %bitcast.403), calls=%async_computation.4 | async-start | bytes 8388608
  307.8 6.0 %copy-start.31 = (f32[512]{0:T(512)S(1)}, f32[512]{0:T(512)}, u32[]{:S(2)}) copy-start(f32[512]{0:T(512)} %get-tuple-element.7) | copy-start | bytes 6148
  309.5 25.3 %all-to-all-start = ((bf16[4,384,512]{1,2,0:T(8,128)(2,1)}), bf16[4,384,512]{1,2,0:T(8,128)(2,1)}, u32[]{:S(2)}, u32[]{:S(2)}) async-start(bf16[4,384,512]{1,2,0:T(8,128)(2,1)} %copy.480), calls=%async_computation | async-start | bytes 3145728 | tf_op jit(solution)/shard_map/all_to_all | solution.py:203
  334.8 9.1 %copy-start.1 = (bf16[2048,512]{1,0:T(8,128)(2,1)S(1)}, bf16[2048,512]{1,0:T(8,128)(2,1)}, u32[]{:S(2)}) copy-start(bf16[2048,512]{1,0:T(8,128)(2,1)} %param.24) | copy-start | bytes 6291460
  (24 other events, 40.9 us)
Sparse Core Ops, SparseCore 0:
  9.5 52.0 all-gather.5
  63.1 44.8 all-gather.7
where the time goes:
time: 356 us; the launch traced here: 351 us
  local copies, waits for them, and re-layouts  104 us (29%)
  matrix products  89.7 us (25%)
  other arithmetic  75.7 us (21%)
  blocking collectives  55.5 us (16%)
  between operations  14.7 us (4%)
  starting transfers between devices  11 us (3%)
    dot_general x2, local copies, waits for them, and re-layouts, attend_rows(): jnp.einsum('nir,hrj,ckj->nhcik', row_onehot, offset_bias, col_onehot, pre...  27.8 us
    reduce_max x4, other arithmetic, attend_rows(): top = jnp.maximum(jnp.max(s_win, axis=(3, 4)), jnp.max(s_ctx, axis=3))  26.8 us
    dot_general x16, matrix products, attend_rows(): jnp.einsum('nchd,nkhd->nhck', queries, key_at(i), preferred_element_type=...  24.7 us
    psum x1, blocking collectives, shards(): summed = lax.psum((shift_part, scale_part, gate_part), 'sp')  24.2 us
    all_gather x1, blocking collectives, shards(): lax.all_gather(summed[2], 'tp', axis=0, tiled=True)  21 us
    dot_general x3, matrix products, attend_rows(): jnp.einsum('nir,hrj,ckj->nhcik', row_onehot, offset_bias, col_onehot, pre...  19.2 us
    unnamed x105, local copies, waits for them, and re-layouts  19 us
    reduce_sum x4, other arithmetic, attend_rows(): total = jnp.sum(e_win, axis=(3, 4)) + jnp.sum(e_ctx, axis=3)  17.2 us
  transfers between devices with their start and end apart: 5, of which 0 were waited for; matrix products, arithmetic and copies ran while one was open for 28% of the time, Pallas kernels for 0%

commit v1 on v0

v1 whole, which is shorter than its diff:
```python
import functools
import math

import jax
import jax.numpy as jnp
from jax import lax
from jax.experimental import pallas as pl
from jax.experimental.pallas import tpu as pltpu
from jax.sharding import PartitionSpec as P

HEAD_DIM = 128
GRID_W = 64
WIN_ROWS = 8
WIN_COLS = 16
REACH = WIN_ROWS // 2
EPS = 1e-06
LOG2E = math.log2(math.e)
BLANK = 2 * WIN_ROWS
TABLES = BLANK + 1
F32 = jnp.float32
BF16 = jnp.bfloat16
MIB = 1 << 20

VM = pl.BlockSpec(memory_space=pltpu.VMEM)
SM = pl.BlockSpec(memory_space=pltpu.SMEM)


def params(mib):
    return pltpu.CompilerParams(vmem_limit_bytes=mib * MIB)


def cost(flops, nbytes, exps=0):
    return pl.CostEstimate(flops=int(flops), bytes_accessed=int(nbytes), transcendentals=int(exps))


def mod_kernel(cond_ref, shift_ref, scale_ref, gate_ref, out_ref):
    cond = cond_ref[...].astype(F32)
    lifted = (cond / (1.0 + jnp.exp(-cond))).astype(BF16)
    lifted = jnp.broadcast_to(lifted, (16, lifted.shape[1]))
    width = shift_ref.shape[1]
    for i, ref in enumerate((shift_ref, scale_ref, gate_ref)):
        part = jnp.dot(lifted, ref[...], preferred_element_type=F32)
        out_ref[:, i * width : (i + 1) * width] = part[:1]


def mod_part(cond, mod_shift, mod_scale, mod_gate):
    rows, width = mod_shift.shape
    return pl.pallas_call(
        mod_kernel,
        out_shape=jax.ShapeDtypeStruct((1, 3 * width), F32),
        in_specs=[VM] * 4,
        out_specs=VM,
        name="mod_part",
        compiler_params=params(8),
        cost_estimate=cost(96 * rows * width, 6 * rows * width),
    )(cond.reshape(1, -1), mod_shift, mod_scale, mod_gate)


def place_kernel(count, spots_ref, *refs):
    pieces, gain_ref, out_ref = refs[:count], refs[count], refs[count + 1]
    width = pieces[0].shape[1] // 3
    for i, piece in enumerate(pieces):
        spot = pl.multiple_of(spots_ref[i] * width, width)
        gain = gain_ref[:, pl.ds(spot, width)]
        out_ref[0:1, pl.ds(spot, width)] = piece[:, :width]
        out_ref[1:2, pl.ds(spot, width)] = gain * (1.0 + piece[:, width : 2 * width])
        out_ref[2:3, pl.ds(spot, width)] = piece[:, 2 * width :]


def place_mods(pieces, spots, norm_gain):
    depth = norm_gain.shape[0]
    return pl.pallas_call(
        functools.partial(place_kernel, len(pieces)),
        out_shape=jax.ShapeDtypeStruct((8, depth), F32),
        in_specs=[SM] + [VM] * (len(pieces) + 1),
        out_specs=VM,
        name="place_mods",
        compiler_params=params(4),
        cost_estimate=cost(1 << 20, 1 << 16),
    )(spots, *pieces, norm_gain.reshape(1, -1))


def table_kernel(bias_ref, out_ref):
    heads = out_ref.shape[0]
    column = lax.broadcasted_iota(jnp.int32, (GRID_W, 2 * GRID_W), 0)
    lane = lax.broadcasted_iota(jnp.int32, (GRID_W, 2 * GRID_W), 1)
    left = lane < GRID_W
    begin = jnp.clip(column - WIN_COLS // 2, 0, GRID_W - WIN_COLS)
    key = jnp.where(left, lane, lane - GRID_W)
    valid = (key >= begin) & (key < begin + WIN_COLS)
    empty = jnp.full((GRID_W, 2 * GRID_W), -1e30, F32)
    for h in range(heads):
        rolled = []
        for d in range(2 * WIN_ROWS - 1):
            row = jnp.broadcast_to(bias_ref[h, d : d + 1, :] * LOG2E, (GRID_W, 2 * GRID_W))
            lo = pltpu.roll(row, 2 * GRID_W - WIN_COLS + 1, 1, stride=1, stride_axis=0)
            hi = pltpu.roll(row, GRID_W - WIN_COLS + 1, 1, stride=1, stride_axis=0)
            rolled.append((jnp.where(valid & left, lo, empty), jnp.where(valid & ~left, hi, empty)))
        for d in range(2 * WIN_ROWS - 2):
            out_ref[h, d] = jnp.where(left, rolled[d][0], rolled[d + 1][1])
        out_ref[h, 2 * WIN_ROWS - 2] = rolled[WIN_ROWS + 2][0]
        out_ref[h, 2 * WIN_ROWS - 1] = rolled[WIN_ROWS - REACH - 1][1]
        out_ref[h, BLANK] = empty


def bias_tables(offset_bias):
    heads, rows, cols = offset_bias.shape
    padded = jnp.pad(offset_bias, ((0, 0), (0, 16 - rows), (0, 2 * GRID_W - cols)))
    return pl.pallas_call(
        table_kernel,
        out_shape=jax.ShapeDtypeStruct((heads, TABLES, GRID_W, 2 * GRID_W), F32),
        in_specs=[VM],
        out_specs=VM,
        name="bias_tables",
        compiler_params=params(8),
        cost_estimate=cost(1 << 22, heads * TABLES * GRID_W * 2 * GRID_W * 4),
    )(padded)


def normed_heads(values, gain, heads):
    parts = []
    for h in range(heads):
        part = values[:, h * HEAD_DIM : (h + 1) * HEAD_DIM]
        square = jnp.mean(part * part, axis=-1, keepdims=True)
        parts.append((part * lax.rsqrt(square + EPS) * gain).astype(BF16))
    return jnp.concatenate(parts, axis=1)


def qkv_kernel(count, heads, tile, *refs):
    pieces = refs[:count]
    mods_ref, wq_ref, wk_ref, wv_ref, qg_ref, kg_ref, q_ref, kv_ref, normed = refs[count:]
    width = heads * HEAD_DIM
    strip = 16
    shift, gain = mods_ref[0:1, :], mods_ref[1:2, :]
    base = 0
    for piece in pieces:

        def one(i, _, piece=piece, base=base):
            at = pl.multiple_of(i * strip, strip)
            floats = piece[pl.ds(at, strip), :].astype(F32)
            inverse = lax.rsqrt(jnp.mean(floats * floats, axis=-1, keepdims=True) + EPS)
            normed[pl.ds(base + at, strip), :] = (floats * inverse * gain + shift).astype(BF16)
            return 0

        lax.fori_loop(0, piece.shape[0] // strip, one, 0, unroll=2)
        base += piece.shape[0]

    def project(i, _):
        rows = pl.ds(pl.multiple_of(i * tile, tile), tile)
        x = normed[rows, :]
        q_ref[rows, :] = normed_heads(
            jnp.dot(x, wq_ref[...], preferred_element_type=F32), qg_ref[...], heads
        )
        kv_ref[rows, :width] = normed_heads(
            jnp.dot(x, wk_ref[...], preferred_element_type=F32), kg_ref[...], heads
        )
        kv_ref[rows, width:] = jnp.dot(x, wv_ref[...], preferred_element_type=F32).astype(BF16)
        return 0

    lax.fori_loop(0, base // tile, project, 0)


def qkv(pieces, mods, w_query, w_key, w_value, query_gain, key_gain, heads):
    total = sum(p.shape[0] for p in pieces)
    depth, width = w_query.shape
    tile = 256 if total % 256 == 0 else 128
    return pl.pallas_call(
        functools.partial(qkv_kernel, len(pieces), heads, tile),
        out_shape=(
            jax.ShapeDtypeStruct((total, width), BF16),
            jax.ShapeDtypeStruct((total, 2 * width), BF16),
        ),
        in_specs=[VM] * (len(pieces) + 6),
        out_specs=(VM, VM),
        scratch_shapes=[pltpu.VMEM((total, depth), BF16)],
        name="qkv",
        compiler_params=params(40),
        cost_estimate=cost(6 * total * depth * width, total * depth * 2 + 6 * depth * width),
    )(*pieces, mods, w_query, w_key, w_value, query_gain.reshape(1, -1), key_gain.reshape(1, -1))


def context_kernel(heads, x_ref, gain_ref, wk_ref, wv_ref, kg_ref, kv_ref):
    width = heads * HEAD_DIM
    floats = x_ref[...].astype(F32)
    inverse = lax.rsqrt(jnp.mean(floats * floats, axis=-1, keepdims=True) + EPS)
    x = (floats * inverse * gain_ref[...]).astype(BF16)
    kv_ref[:, :width] = normed_heads(
        jnp.dot(x, wk_ref[...], preferred_element_type=F32), kg_ref[...], heads
    )
    kv_ref[:, width:] = jnp.dot(x, wv_ref[...], preferred_element_type=F32).astype(BF16)


def context_kv(context, norm_gain, w_key, w_value, key_gain, heads):
    count, depth = context.shape
    width = w_key.shape[1]
    return pl.pallas_call(
        functools.partial(context_kernel, heads),
        out_shape=jax.ShapeDtypeStruct((count, 2 * width), BF16),
        in_specs=[VM] * 5,
        out_specs=VM,
        name="context_kv",
        compiler_params=params(16),
        cost_estimate=cost(4 * count * depth * width, 4 * depth * width),
    )(context, norm_gain.reshape(1, -1), w_key, w_value, key_gain.reshape(1, -1))


def attend_kernel(heads, span, groups, counts, meta_ref, cbias_ref, *refs):
    n_q, n_kv, n_ctx = counts
    q_refs, refs = refs[:n_q], refs[n_q:]
    kv_refs, refs = refs[:n_kv], refs[n_kv:]
    ctx_refs, refs = refs[:n_ctx], refs[n_ctx:]
    tab_ref, out_ref, keys, queries, context, scores, weights = refs
    width = heads * HEAD_DIM
    block = span * GRID_W
    key_rows = span + WIN_ROWS
    window = key_rows * GRID_W
    ctx_count = context.shape[0]
    factor = LOG2E * HEAD_DIM**-0.5
    lines = 2 * GRID_W
    for i, ref in enumerate(kv_refs):
        at = pl.multiple_of((meta_ref[2 + i] + REACH) * GRID_W, GRID_W)
        keys[pl.ds(at, ref.shape[0]), :] = ref[...]
    at = 0
    for ref in q_refs:
        queries[at : at + ref.shape[0], :] = ref[...]
        at += ref.shape[0]
    at = 0
    for ref in ctx_refs:
        context[at : at + ref.shape[0], :] = ref[...]
        at += ref.shape[0]
    first, total = meta_ref[0], meta_ref[1]
    nt = (((1,), (1,)), ((), ()))

    def group(i, _):
        row = meta_ref[2 + n_kv + 2 * i]
        q_at = pl.multiple_of(meta_ref[3 + n_kv + 2 * i], GRID_W)
        top = first + row
        start = jnp.clip(top - REACH, 0, total - key_rows)
        k_at = pl.multiple_of((start - first + REACH) * GRID_W, GRID_W)
        spots = []
        for r in range(span):
            g = top + r
            a = jnp.clip(g - REACH, 0, total - WIN_ROWS)
            for p in range(key_rows // 2):
                u = start + 2 * p
                lv = (u >= a) & (u < a + WIN_ROWS)
                rv = (u + 1 >= a) & (u + 1 < a + WIN_ROWS)
                both = jnp.where(rv, u - g + WIN_ROWS - 1, BLANK - 2)
                spots.append(jnp.where(lv, both, jnp.where(rv, BLANK - 1, BLANK)))
        out_at = pl.multiple_of(i * block, block)
        for h in range(heads):
            hk = slice(h * HEAD_DIM, (h + 1) * HEAD_DIM)
            hv = slice(width + h * HEAD_DIM, width + (h + 1) * HEAD_DIM)
            q = queries[pl.ds(q_at, block), hk]
            scores[h, :, :window] = lax.dot_general(
                q, keys[pl.ds(k_at, window), hk], nt, preferred_element_type=F32
            )
            scores[h, :, window:] = lax.dot_general(
                q, context[:, hk], nt, preferred_element_type=F32
            )
            cbias = cbias_ref[h] * LOG2E
            sums = []
            for r in range(span):
                rows = slice(r * GRID_W, (r + 1) * GRID_W)
                tops = None
                for p in range(key_rows // 2):
                    cols = slice(p * lines, (p + 1) * lines)
                    tile = scores[h, rows, cols] * factor
                    tile = tile + tab_ref[h, spots[r * (key_rows // 2) + p]]
                    scores[h, rows, cols] = tile
                    tops = tile if tops is None else jnp.maximum(tops, tile)
                ctx = scores[h, rows, window : window + lines]
                for p in range(1, ctx_count // lines):
                    cols = slice(window + p * lines, window + (p + 1) * lines)
                    ctx = jnp.maximum(ctx, scores[h, rows, cols])
                tops = jnp.maximum(tops, ctx * factor + cbias)
                high = jnp.max(tops, axis=1, keepdims=True)
                acc = None
                for p in range(key_rows // 2 + ctx_count // lines):
                    cols = slice(p * lines, (p + 1) * lines)
                    tile = scores[h, rows, cols]
                    if p < key_rows // 2:
                        tile = jnp.exp2(tile - high)
                    else:
                        tile = jnp.exp2(tile * factor - (high - cbias))
                    acc = tile if acc is None else acc + tile
                    weights[h, rows, cols] = tile.astype(BF16)
                sums.append(jnp.sum(acc, axis=1, keepdims=True))
            out = jnp.dot(
                weights[h, :, :window], keys[pl.ds(k_at, window), hv], preferred_element_type=F32
            )
            out = out + jnp.dot(
                weights[h, :, window:], context[:, hv], preferred_element_type=F32
            )
            out = out / jnp.concatenate(sums, axis=0)
            out_ref[pl.ds(out_at, block), hk] = out.astype(BF16)
        return 0

    lax.fori_loop(0, groups, group, 0)


def attend(queries, kvs, ctx, tables, context_bias, meta, span, groups, rows):
    heads = tables.shape[0]
    width = heads * HEAD_DIM
    block = span * GRID_W
    ctx_count = sum(c.shape[0] for c in ctx)
    keys = (span + WIN_ROWS) * GRID_W + ctx_count
    q_rows = sum(q.shape[0] for q in queries)
    elements = groups * block * heads * keys
    return pl.pallas_call(
        functools.partial(
            attend_kernel, heads, span, groups, (len(queries), len(kvs), len(ctx))
        ),
        out_shape=jax.ShapeDtypeStruct((groups * block, width), BF16),
        in_specs=[SM, SM] + [VM] * (len(queries) + len(kvs) + len(ctx) + 1),
        out_specs=VM,
        scratch_shapes=[
            pltpu.VMEM(((rows + 2 * REACH) * GRID_W, 2 * width), BF16),
            pltpu.VMEM((q_rows, width), BF16),
            pltpu.VMEM((ctx_count, 2 * width), BF16),
            pltpu.VMEM((heads, block, keys), F32),
            pltpu.VMEM((heads, block, keys), BF16),
        ],
        name="attend",
        compiler_params=params(40),
        cost_estimate=cost(8 * elements * HEAD_DIM, 8 << 20, elements),
    )(meta, context_bias, *queries, *kvs, *ctx, tables)


def out_kernel(count, tile, spots_ref, *refs):
    pieces = refs[:count]
    w_ref, resid_ref, mods_ref, out_ref = refs[count:]
    depth = pieces[0].shape[1]

    def one(i, _):
        cols = pl.ds(pl.multiple_of(i * tile, tile), tile)
        total = None
        for j, piece in enumerate(pieces):
            rows = pl.ds(pl.multiple_of(spots_ref[j] * depth, depth), depth)
            part = jnp.dot(piece[...], w_ref[rows, cols], preferred_element_type=F32)
            total = part if total is None else total + part
        gate = mods_ref[2:3, cols]
        out_ref[:, cols] = (resid_ref[:, cols].astype(F32) + gate * total).astype(BF16)
        return 0

    lax.fori_loop(0, w_ref.shape[1] // tile, one, 0)


def out_project(pieces, spots, w_out, resid, mods):
    count, width = resid.shape
    return pl.pallas_call(
        functools.partial(out_kernel, len(pieces), 256),
        out_shape=jax.ShapeDtypeStruct((count, width), BF16),
        in_specs=[SM] + [VM] * (len(pieces) + 3),
        out_specs=VM,
        name="out_project",
        compiler_params=params(24),
        cost_estimate=cost(2 * count * width * w_out.shape[0], w_out.size * 2 + 4 * resid.size),
    )(spots, *pieces, w_out, resid, mods)


def swap(count, bit):
    return [(i, i ^ bit) for i in range(count)]


def shards(
    resid,
    cond,
    mod_shift,
    mod_scale,
    mod_gate,
    norm_gain,
    context,
    w_query,
    w_key,
    w_value,
    query_gain,
    key_gain,
    offset_bias,
    context_bias,
    w_out,
):
    heads = offset_bias.shape[0]
    sp, tp = lax.axis_size("sp"), lax.axis_size("tp")
    me_s, me_t = lax.axis_index("sp"), lax.axis_index("tp")
    own = resid.shape[0]
    tokens = own * tp
    rows = tokens // GRID_W

    part = mod_part(cond, mod_shift, mod_scale, mod_gate)
    bit = 1
    while bit < sp:
        part = part + lax.ppermute(part, "sp", swap(sp, bit))
        bit *= 2
    parts = [part]
    bit = 1
    while bit < tp:
        parts += [lax.ppermute(p, "tp", swap(tp, bit)) for p in parts]
        bit *= 2
    spots = me_t ^ jnp.arange(tp, dtype=jnp.int32)
    mods = place_mods(parts, spots, norm_gain)

    tables = bias_tables(offset_bias)
    ctx = lax.all_gather(
        context_kv(context, norm_gain, w_key, w_value, key_gain, heads), "sp", axis=0, tiled=True
    )
    piece = lax.all_gather(resid, "tp", axis=0, tiled=True)
    q, kv = qkv([piece], mods, w_query, w_key, w_value, query_gain, key_gain, heads)

    edge = REACH * GRID_W
    above = lax.ppermute(kv[tokens - edge :], "sp", [(i, i + 1) for i in range(sp - 1)])
    below = lax.ppermute(kv[:edge], "sp", [(i + 1, i) for i in range(sp - 1)])
    span = 4 if rows % 4 == 0 else 2
    groups = rows // span
    meta = [me_s * rows, sp * rows, 0, -REACH, rows]
    for i in range(groups):
        meta += [i * span, i * span * GRID_W]
    meta = jnp.stack([jnp.asarray(m, jnp.int32) for m in meta])
    attended = attend(
        [q], [kv, above, below], [ctx], tables, context_bias, meta, span, groups, rows
    )
    full = lax.all_to_all(attended.reshape(tp, own, -1), "tp", split_axis=0, concat_axis=0)
    return out_project(
        [full[i] for i in range(tp)], jnp.arange(tp, dtype=jnp.int32), w_out, resid, mods
    )


def solution(mesh):
    in_specs = (
        P(("sp", "tp"), None),
        P("sp"),
        P("sp", "tp"),
        P("sp", "tp"),
        P("sp", "tp"),
        P(),
        P("sp", None),
        P(None, "tp"),
        P(None, "tp"),
        P(None, "tp"),
        P(),
        P(),
        P("tp", None, None),
        P("tp"),
        P(),
    )
    out_specs = P(("sp", "tp"), None)
    return jax.shard_map(shards, mesh=mesh, in_specs=in_specs, out_specs=out_specs, check_vma=False)
```

time: 356 us -> 179 us (0.50); the launches traced: 351 us -> 178 us
  matrix products: 89.7 us -> 0 us
  local copies, waits for them, and re-layouts: 104 us -> 20.8 us
  other arithmetic: 75.7 us -> 0.03 us
  waiting for transfers between devices: 0.75 us -> 55.6 us
  Pallas kernels: 0 us -> 49.2 us
  blocking collectives: 55.5 us -> 22.8 us
  starting transfers between devices: 11 us -> 16 us
    dot_general x46 -> x0, matrix products: 87.7 us -> none  [the longest x16 24.7 us: attend_rows(): jnp.einsum('nchd,nkhd->nhck', queries, key_at(i), preferred_element_type=...]
    pallas_call x0 -> x7, Pallas kernels: none -> 49.2 us  [the longest x1 20 us: qkv(): pl.pallas_call(functools.partial(qkv_kernel, len(pieces), heads, tile), o...]
    all_gather x2, waiting for transfers between devices: 0.02 us -> 45.6 us  [the longest x1 24 us: shards(): piece = lax.all_gather(resid, 'tp', axis=0, tiled=True)]
    all_gather x3 -> x0, blocking collectives: 31.3 us -> none  [the longest x1 21 us: shards(): lax.all_gather(summed[2], 'tp', axis=0, tiled=True)]
    dot_general x2 -> x0, local copies, waits for them, and re-layouts: 27.8 us -> none  [attend_rows(): jnp.einsum('nir,hrj,ckj->nhcik', row_onehot, offset_bias, col_onehot, pre...]
    reduce_max x4 -> x0, other arithmetic: 26.8 us -> none  [attend_rows(): top = jnp.maximum(jnp.max(s_win, axis=(3, 4)), jnp.max(s_ctx, axis=3))]
    psum x1 -> x0, blocking collectives: 24.2 us -> none  [shards(): summed = lax.psum((shift_part, scale_part, gate_part), 'sp')]
    all_to_all x0 -> x1, blocking collectives: none -> 22.8 us  [shards(): lax.all_to_all(attended.reshape(tp, own, -1), 'tp', split_axis=0, concat_...]
  transfers between devices with their start and end apart: 5 -> 10, of which waited for: 0 -> 8; matrix products, arithmetic and copies ran while one was open for 28% -> 1% of each run, Pallas kernels for 0% -> 13%
where the time goes in v1:
time: 179 us; the launch traced here: 178 us
  waiting for transfers between devices  55.6 us (31%)
  Pallas kernels  49.2 us (27%)
  blocking collectives  22.8 us (13%)
  local copies, waits for them, and re-layouts  20.8 us (12%)
  starting transfers between devices  16 us (9%)
  between operations  13.7 us (8%)
    all_gather x1, waiting for transfers between devices, shards(): piece = lax.all_gather(resid, 'tp', axis=0, tiled=True)  24 us
    all_to_all x1, blocking collectives, shards(): lax.all_to_all(attended.reshape(tp, own, -1), 'tp', split_axis=0, concat_...  22.8 us
    all_gather x1, waiting for transfers between devices, shards(): lax.all_gather(context_kv(context, norm_gain, w_key, w_value, key_gain, h...  21.6 us
    pallas_call x1, Pallas kernels, qkv(): pl.pallas_call(functools.partial(qkv_kernel, len(pieces), heads, tile), o...  20 us
    unnamed x49, local copies, waits for them, and re-layouts  19.5 us
    pallas_call x1, Pallas kernels, attend(): pl.pallas_call(functools.partial(attend_kernel, heads, span, groups, (len...  19.3 us
    ppermute x3, starting transfers between devices, shards(): part = part + lax.ppermute(part, 'sp', swap(sp, bit))  8.27 us
    pallas_call x1, Pallas kernels, out_project(): pl.pallas_call(functools.partial(out_kernel, len(pieces), 256), out_shape...  6.55 us
  transfers between devices with their start and end apart: 10, of which 8 were waited for; matrix products, arithmetic and copies ran while one was open for 1% of the time, Pallas kernels for 13%

profile of v1, /device:TPU:0, one launch (start us, length us, event | category | flops | bytes accessed | tf_op | source)
XLA Modules:
  0.0 178.2 jit_solution(14654240299612117155)
XLA Ops:
  7.3 1.6 copy-done.2
  8.9 1.6 copy-done.4
  12.8 1.6 context_kv.1
  14.7 3.0 %collective-permute-start = (f32[1,1536]{1,0:T(1,128)S(1)}, f32[1,1536]{1,0:T(1,128)S(1)}, u32[]{:S(2)}, u32[]{:S(2)}) collective-permute-start(f32[1,1536]{1,0:T(1,128)S(1)} %mod_part.1), channel_id=1, source_target_pairs={{0,4},{4,0},{8,12},{12,8},{16,20},{20,16},{24,28},{28,24},{1,5},{5... | collective-permute-start | bytes 18440 | tf_op jit(solution)/shard_map/ppermute | solution.py:393
  17.8 1.6 collective-permute-done
  19.4 2.1 %collective-permute-start.1 = (f32[1,1536]{1,0:T(1,128)S(1)}, f32[1,1536]{1,0:T(1,128)S(1)}, u32[]{:S(2)}, u32[]{:S(2)}) collective-permute-start(f32[1,1536]{1,0:T(1,128)S(1)} %add.11), channel_id=1, source_target_pairs={{0,8},{4,12},{8,0},{12,4},{16,24},{20,28},{24,16},{28,20},{1,9},{5... | collective-permute-start | bytes 18440 | tf_op jit(solution)/shard_map/ppermute | solution.py:393
  21.5 1.6 collective-permute-done.1
  23.1 3.1 %collective-permute-start.2 = (f32[1,1536]{1,0:T(1,128)S(1)}, f32[1,1536]{1,0:T(1,128)S(1)}, u32[]{:S(2)}, u32[]{:S(2)}) collective-permute-start(f32[1,1536]{1,0:T(1,128)S(1)} %add.12), channel_id=1, source_target_pairs={{0,16},{4,20},{8,24},{12,28},{16,0},{20,4},{24,8},{28,12},{1,17},{... | collective-permute-start | bytes 18440 | tf_op jit(solution)/shard_map/ppermute | solution.py:393
  26.2 1.6 collective-permute-done.2
  27.9 1.9 %collective-permute-start.4 = (f32[1,1536]{1,0:T(1,128)S(1)}, f32[1,1536]{1,0:T(1,128)S(1)}, u32[]{:S(2)}, u32[]{:S(2)}) collective-permute-start(f32[1,1536]{1,0:T(1,128)S(1)} %add.13.refs_0_), channel_id=1, source_target_pairs={{0,2},{1,3},{2,0},{3,1},{4,6},{5,7},{6,4},{7,5},{8,10},{9,11},{10,... | collective-permute-start | bytes 18440 | tf_op jit(solution)/shard_map/ppermute | solution.py:398
  29.8 1.1 collective-permute-start.5
  30.9 1.0 collective-permute-done.4.refs_2_
  31.9 1.8 %collective-permute-done.5.refs_3_ = f32[1,1536]{1,0:T(1,128)S(1)} collective-permute-done((f32[1,1536]{1,0:T(1,128)S(1)}, f32[1,1536]{1,0:T(1,128)S(1)}, u32[]{:S(2)}, u32[]{:S(2)}) %collective-permute-start.5) | collective-permute-done | bytes 6176 | tf_op jit(solution)/shard_map/ppermute | solution.py:398
  34.3 24.0 %all-gather.3.cloned.1.call-done.refs_0_ = bf16[1536,2048]{1,0:T(8,128)(2,1)} async-done(((bf16[384,2048]{1,0:T(8,128)(2,1)}), bf16[1536,2048]{1,0:T(8,128)(2,1)}) %all-gather.3.cloned.1.call-update) | async-done | bytes 6291472 | tf_op jit(solution)/shard_map/all_gather | solution.py:407
  58.3 1.6 copy-done.5
  59.9 1.6 copy-done.16
  61.5 20.0 %qkv.1 = (bf16[1536,512]{1,0:T(8,128)(2,1)S(1)}, bf16[1536,1024]{1,0:T(8,128)(2,1)S(1)}) custom-call(bf16[1536,2048]{1,0:T(8,128)(2,1)} %all-gather.3.cloned.1.call-done.refs_0_, f32[8,2048]{1,0:T(8,128)S(1)} %place_mods.1.refs_1_.refs_6_, bf16[2048,512]{1,0:T(8,128)(2,1)S(1)} %copy-done.16, bf16[2048,512]{1,0:T(8,128)(2,1)S(1)} %copy-done.3, ...), custom_call_target="tpu_custom_call" | custom-call | flops 9663676416 | bytes 12582912 | tf_op jit(solution)/shard_map/qkv/pallas_call | solution.py:167
  81.5 1.1 fusion
  82.6 1.6 copy-done.6
  84.2 3.4 %collective-permute-start.6 = (bf16[256,1024]{1,0:T(8,128)(2,1)}, bf16[256,1024]{1,0:T(8,128)(2,1)S(1)}, u32[]{:S(2)}, u32[]{:S(2)}) collective-permute-start(bf16[256,1024]{1,0:T(8,128)(2,1)} %get-tuple-element.10), channel_id=1, source_target_pairs={{0,4},{4,8},{8,12},{12,16},{16,20},{20,24},{24,28},{1,5},{5,9},{9,... | collective-permute-start | bytes 1572872 | tf_op jit(solution)/shard_map/ppermute | solution.py:411
  87.6 1.3 collective-permute-start.7
  89.1 1.0 bias_tables.1.refs_5_
  90.1 21.6 %all-gather.5.cloned.1.call-done.refs_4_ = bf16[512,1024]{1,0:T(8,128)(2,1)} async-done(((bf16[64,1024]{1,0:T(8,128)(2,1)}), bf16[512,1024]{1,0:T(8,128)(2,1)}) %all-gather.5.cloned.1.call-update) | async-done | bytes 1048592 | tf_op jit(solution)/shard_map/all_gather | solution.py:404
  111.7 1.7 collective-permute-done.6.refs_2_
  113.4 1.9 %copy-done.7 = bf16[1536,1024]{1,0:T(8,128)(2,1)S(1)} copy-done((bf16[1536,1024]{1,0:T(8,128)(2,1)S(1)}, bf16[1536,1024]{1,0:T(8,128)(2,1)}, u32[]{:S(2)}) %copy-start.7) | copy-done | bytes 3145752
  115.3 1.2 copy-done.17
  116.5 1.4 copy-done.21
  117.9 19.3 %attend.1 = bf16[1536,512]{1,0:T(8,128)(2,1)S(1)} custom-call(s32[17]{0:T(128)S(1)} %stack.7.meta_ref, f32[4]{0:T(128)S(1)} %copy-done.19, bf16[1536,512]{1,0:T(8,128)(2,1)S(1)} %copy-done.21, bf16[1536,1024]{1,0:T(8,128)(2,1)S(1)} %copy-done.7, bf16[256,1024]{1,0:T(8,128)(2,1)S(1)} %collective-permute-done.6.refs_2_, ...), custom_call_target="tpu_custom_call" | custom-call | flops 8053063680 | bytes 8388608 | tf_op jit(solution)/shard_map/attend/pallas_call | solution.py:310
  137.2 22.8 %all_to_all.5 = bf16[4,384,512]{2,1,0:T(8,128)(2,1)S(1)} all-to-all(bf16[4,384,512]{2,1,0:T(8,128)(2,1)S(1)} %bitcast.13), channel_id=1, replica_groups=mesh['sp'=8,'tp'=4] {'tp'}, dimensions={0} | all-to-all | bytes 3145728 | tf_op jit(solution)/shard_map/all_to_all | solution.py:422
  160.1 1.3 copy-done.1
  161.4 3.4 %copy-done = bf16[2048,2048]{1,0:T(8,128)(2,1)S(1)} copy-done((bf16[2048,2048]{1,0:T(8,128)(2,1)S(1)}, bf16[2048,2048]{1,0:T(8,128)(2,1)}, u32[]{:S(2)}) %copy-start) | copy-done | bytes 8388632
  164.8 6.6 %out_project.1 = bf16[384,2048]{1,0:T(8,128)(2,1)} custom-call(s32[4]{0:T(128)S(1)} %iota.6.spots_ref, bf16[384,512]{1,0:T(8,128)(2,1)S(1)} %get-tuple-element.14.refs_0_, bf16[384,512]{1,0:T(8,128)(2,1)S(1)} %get-tuple-element.13.refs_1_, bf16[384,512]{1,0:T(8,128)(2,1)S(1)} %get-tuple-element.12.refs_2_, bf16[384,512]{1,0:T(8,128)(2,1)S(1)} %get-tuple-element.11.refs_3_, ...), custom_call_target="tpu_custom_call" | custom-call | flops 3221225472 | bytes 11534336 | tf_op jit(solution)/shard_map/out_project/pallas_call | solution.py:351
  (58 shorter events, 4.2 us)
Async XLA Ops:
  6.5 51.7 %all-gather.3.cloned.1.call-start = ((), (), s32[]{:S(2)}) async-start(), calls=%async_computation.1 | async-start | bytes 7864320 | tf_op jit(solution)/shard_map/all_gather | solution.py:407
  7.3 104.4 %all-gather.5.cloned.1.call-start = ((), (), s32[]{:S(2)}) async-start(), calls=%async_computation.2 | async-start | bytes 1179648 | tf_op jit(solution)/shard_map/all_gather | solution.py:404
  7.3 1.6 copy-start.2
  8.9 1.6 copy-start.4
  10.5 0.9 copy-start.8
  12.8 1.7 copy-start.23
  12.8 1.7 copy-start.9
  12.8 1.7 copy-start.10
  12.8 1.7 copy-start.11
  12.8 20.9 %copy-start.13 = (f32[2048]{0:T(1024)S(1)}, f32[2048]{0:T(1024)}, u32[]{:S(2)}) copy-start(f32[2048]{0:T(1024)} %param.20) | copy-start | bytes 24580
  12.8 45.5 %copy-start.3 = (bf16[2048,512]{1,0:T(8,128)(2,1)S(1)}, bf16[2048,512]{1,0:T(8,128)(2,1)}, u32[]{:S(2)}) copy-start(bf16[2048,512]{1,0:T(8,128)(2,1)} %wk_ref.1) | copy-start | bytes 6291460
  12.8 45.5 %copy-start.15 = (f32[128]{0:T(128)S(1)}, f32[128]{0:T(128)}, u32[]{:S(2)}) copy-start(f32[128]{0:T(128)} %param.26) | copy-start | bytes 1540
  12.8 45.4 %copy-start.18 = (f32[128]{0:T(128)S(1)}, f32[128]{0:T(128)}, u32[]{:S(2)}) copy-start(f32[128]{0:T(128)} %param.25) | copy-start | bytes 1540
  14.7 4.6 %collective-permute-start = (f32[1,1536]{1,0:T(1,128)S(1)}, f32[1,1536]{1,0:T(1,128)S(1)}, u32[]{:S(2)}, u32[]{:S(2)}) collective-permute-start(f32[1,1536]{1,0:T(1,128)S(1)} %mod_part.1), channel_id=1, source_target_pairs={{0,4},{4,0},{8,12},{12,8},{16,20},{20,16},{24,28},{28,24},{1,5},{5... | collective-permute-start | bytes 18440 | tf_op jit(solution)/shard_map/ppermute | solution.py:393
  19.4 3.7 %collective-permute-start.1 = (f32[1,1536]{1,0:T(1,128)S(1)}, f32[1,1536]{1,0:T(1,128)S(1)}, u32[]{:S(2)}, u32[]{:S(2)}) collective-permute-start(f32[1,1536]{1,0:T(1,128)S(1)} %add.11), channel_id=1, source_target_pairs={{0,8},{4,12},{8,0},{12,4},{16,24},{20,28},{24,16},{28,20},{1,9},{5... | collective-permute-start | bytes 18440 | tf_op jit(solution)/shard_map/ppermute | solution.py:393
  23.1 4.7 %collective-permute-start.2 = (f32[1,1536]{1,0:T(1,128)S(1)}, f32[1,1536]{1,0:T(1,128)S(1)}, u32[]{:S(2)}, u32[]{:S(2)}) collective-permute-start(f32[1,1536]{1,0:T(1,128)S(1)} %add.12), channel_id=1, source_target_pairs={{0,16},{4,20},{8,24},{12,28},{16,0},{20,4},{24,8},{28,12},{1,17},{... | collective-permute-start | bytes 18440 | tf_op jit(solution)/shard_map/ppermute | solution.py:393
  27.9 2.0 %collective-permute-start.3 = (f32[1,1536]{1,0:T(1,128)S(1)}, f32[1,1536]{1,0:T(1,128)S(1)}, u32[]{:S(2)}, u32[]{:S(2)}) collective-permute-start(f32[1,1536]{1,0:T(1,128)S(1)} %add.13.refs_0_), channel_id=1, source_target_pairs={{0,1},{1,0},{2,3},{3,2},{4,5},{5,4},{6,7},{7,6},{8,9},{9,8},{10,11... | collective-permute-start | bytes 18440 | tf_op jit(solution)/shard_map/ppermute | solution.py:398
  27.9 3.9 %collective-permute-start.4 = (f32[1,1536]{1,0:T(1,128)S(1)}, f32[1,1536]{1,0:T(1,128)S(1)}, u32[]{:S(2)}, u32[]{:S(2)}) collective-permute-start(f32[1,1536]{1,0:T(1,128)S(1)} %add.13.refs_0_), channel_id=1, source_target_pairs={{0,2},{1,3},{2,0},{3,1},{4,6},{5,7},{6,4},{7,5},{8,10},{9,11},{10,... | collective-permute-start | bytes 18440 | tf_op jit(solution)/shard_map/ppermute | solution.py:398
  29.8 3.9 %collective-permute-start.5 = (f32[1,1536]{1,0:T(1,128)S(1)}, f32[1,1536]{1,0:T(1,128)S(1)}, u32[]{:S(2)}, u32[]{:S(2)}) collective-permute-start(f32[1,1536]{1,0:T(1,128)S(1)} %collective-permute-done.3.refs_1_), channel_id=1, source_target_pairs={{0,2},{1,3},{2,0},{3,1},{4,6},{5,7},{6,4},{7,5},{8,10},{9,11},{10,... | collective-permute-start | bytes 18440 | tf_op jit(solution)/shard_map/ppermute | solution.py:398
  58.3 1.6 copy-start.5
  59.9 1.6 copy-start.16
  81.5 6.1 %copy-start.20 = (bf16[1536,512]{1,0:T(8,128)(2,1)}, bf16[1536,512]{1,0:T(8,128)(2,1)S(1)}, u32[]{:S(2)}) copy-start(bf16[1536,512]{1,0:T(8,128)(2,1)S(1)} %get-tuple-element.7.refs_0_) | copy-start | bytes 4718596
  81.5 7.4 %copy-start.22 = (f32[4,15,31]{2,0,1:T(4,128)S(1)}, f32[4,15,31]{2,0,1:T(4,128)}, u32[]{:S(2)}) copy-start(f32[4,15,31]{2,0,1:T(4,128)} %param.27) | copy-start | bytes 22324
  81.5 31.9 %copy-start.19 = (f32[4]{0:T(128)S(1)}, f32[4]{0:T(128)}, u32[]{:S(2)}) copy-start(f32[4]{0:T(128)} %cbias_ref.1) | copy-start | bytes 52
  82.6 1.6 copy-start.6
  84.2 29.2 %collective-permute-start.6 = (bf16[256,1024]{1,0:T(8,128)(2,1)}, bf16[256,1024]{1,0:T(8,128)(2,1)S(1)}, u32[]{:S(2)}, u32[]{:S(2)}) collective-permute-start(bf16[256,1024]{1,0:T(8,128)(2,1)} %get-tuple-element.10), channel_id=1, source_target_pairs={{0,4},{4,8},{8,12},{12,16},{16,20},{20,24},{24,28},{1,5},{5,9},{9,... | collective-permute-start | bytes 1572872 | tf_op jit(solution)/shard_map/ppermute | solution.py:411
  87.6 25.8 %collective-permute-start.7 = (bf16[256,1024]{1,0:T(8,128)(2,1)}, bf16[256,1024]{1,0:T(8,128)(2,1)S(1)}, u32[]{:S(2)}, u32[]{:S(2)}) collective-permute-start(bf16[256,1024]{1,0:T(8,128)(2,1)} %get-tuple-element.9), channel_id=1, source_target_pairs={{4,0},{8,4},{12,8},{16,12},{20,16},{24,20},{28,24},{5,1},{9,5},{13... | collective-permute-start | bytes 1572872 | tf_op jit(solution)/shard_map/ppermute | solution.py:412
  113.4 1.9 %copy-start.7 = (bf16[1536,1024]{1,0:T(8,128)(2,1)S(1)}, bf16[1536,1024]{1,0:T(8,128)(2,1)}, u32[]{:S(2)}) copy-start(bf16[1536,1024]{1,0:T(8,128)(2,1)} %copy-done.6) | copy-start | bytes 9437188
  115.3 1.2 copy-start.17
  116.5 1.4 copy-start.21
  160.0 1.4 copy-start.1
  161.4 3.4 %copy-start = (bf16[2048,2048]{1,0:T(8,128)(2,1)S(1)}, bf16[2048,2048]{1,0:T(8,128)(2,1)}, u32[]{:S(2)}) copy-start(bf16[2048,2048]{1,0:T(8,128)(2,1)} %refs_4_.3) | copy-start | bytes 25165828
  (2 other events, 1.4 us)
Sparse Core Ops, SparseCore 0:
  8.9 49.3 all-gather.2
  60.4 51.2 all-gather.4

commit v2 on v1

--- a/solution.py
+++ b/solution.py
@@ -7,6 +7,7 @@
 from jax.experimental import pallas as pl
 from jax.experimental.pallas import tpu as pltpu
 from jax.sharding import PartitionSpec as P
+
 
 HEAD_DIM = 128
 GRID_W = 64
@@ -204,8 +205,8 @@
     )(context, norm_gain.reshape(1, -1), w_key, w_value, key_gain.reshape(1, -1))
 
 
-def attend_kernel(heads, span, groups, counts, meta_ref, cbias_ref, *refs):
-    n_q, n_kv, n_ctx = counts
+def attend_kernel(heads, span, groups, q_spec, kv_spec, n_ctx, meta_ref, cbias_ref, *refs):
+    n_q, n_kv = q_spec[-1][0] + 1, kv_spec[-1][0] + 1
     q_refs, refs = refs[:n_q], refs[n_q:]
     kv_refs, refs = refs[:n_kv], refs[n_kv:]
     ctx_refs, refs = refs[:n_ctx], refs[n_ctx:]
@@ -217,13 +218,15 @@
     ctx_count = context.shape[0]
     factor = LOG2E * HEAD_DIM**-0.5
     lines = 2 * GRID_W
-    for i, ref in enumerate(kv_refs):
-        at = pl.multiple_of((meta_ref[2 + i] + REACH) * GRID_W, GRID_W)
-        keys[pl.ds(at, ref.shape[0]), :] = ref[...]
-    at = 0
-    for ref in q_refs:
-        queries[at : at + ref.shape[0], :] = ref[...]
-        at += ref.shape[0]
+    base = 2
+    for i, (j, at, size) in enumerate(q_spec):
+        to = pl.multiple_of(meta_ref[base + i] * GRID_W, GRID_W)
+        queries[pl.ds(to, size), :] = q_refs[j][at : at + size, :]
+    base += len(q_spec)
+    for i, (j, at, size) in enumerate(kv_spec):
+        to = pl.multiple_of((meta_ref[base + i] + REACH) * GRID_W, GRID_W)
+        keys[pl.ds(to, size), :] = kv_refs[j][at : at + size, :]
+    base += len(kv_spec)
     at = 0
     for ref in ctx_refs:
         context[at : at + ref.shape[0], :] = ref[...]
@@ -232,8 +235,8 @@
     nt = (((1,), (1,)), ((), ()))
 
     def group(i, _):
-        row = meta_ref[2 + n_kv + 2 * i]
-        q_at = pl.multiple_of(meta_ref[3 + n_kv + 2 * i], GRID_W)
+        row = meta_ref[base + i]
+        q_at = pl.multiple_of(row * GRID_W, GRID_W)
         top = first + row
         start = jnp.clip(top - REACH, 0, total - key_rows)
         k_at = pl.multiple_of((start - first + REACH) * GRID_W, GRID_W)
@@ -247,7 +250,6 @@
                 rv = (u + 1 >= a) & (u + 1 < a + WIN_ROWS)
                 both = jnp.where(rv, u - g + WIN_ROWS - 1, BLANK - 2)
                 spots.append(jnp.where(lv, both, jnp.where(rv, BLANK - 1, BLANK)))
-        out_at = pl.multiple_of(i * block, block)
         for h in range(heads):
             hk = slice(h * HEAD_DIM, (h + 1) * HEAD_DIM)
             hv = slice(width + h * HEAD_DIM, width + (h + 1) * HEAD_DIM)
@@ -292,31 +294,31 @@
             out = out + jnp.dot(
                 weights[h, :, window:], context[:, hv], preferred_element_type=F32
             )
-            out = out / jnp.concatenate(sums, axis=0)
-            out_ref[pl.ds(out_at, block), hk] = out.astype(BF16)
+            out = (out / jnp.concatenate(sums, axis=0)).astype(BF16)
+            for r in range(span):
+                to = pl.multiple_of(meta_ref[base + groups + i * span + r] * GRID_W, GRID_W)
+                out_ref[pl.ds(to, GRID_W), hk] = out[r * GRID_W : (r + 1) * GRID_W]
         return 0
 
     lax.fori_loop(0, groups, group, 0)
 
 
-def attend(queries, kvs, ctx, tables, context_bias, meta, span, groups, rows):
+def attend(queries, q_spec, kvs, kv_spec, ctx, tables, context_bias, meta, span, groups, rows):
     heads = tables.shape[0]
     width = heads * HEAD_DIM
     block = span * GRID_W
     ctx_count = sum(c.shape[0] for c in ctx)
     keys = (span + WIN_ROWS) * GRID_W + ctx_count
-    q_rows = sum(q.shape[0] for q in queries)
     elements = groups * block * heads * keys
+    meta = jnp.stack([jnp.asarray(m, jnp.int32) for m in meta])
     return pl.pallas_call(
-        functools.partial(
-            attend_kernel, heads, span, groups, (len(queries), len(kvs), len(ctx))
-        ),
+        functools.partial(attend_kernel, heads, span, groups, q_spec, kv_spec, len(ctx)),
         out_shape=jax.ShapeDtypeStruct((groups * block, width), BF16),
         in_specs=[SM, SM] + [VM] * (len(queries) + len(kvs) + len(ctx) + 1),
         out_specs=VM,
         scratch_shapes=[
             pltpu.VMEM(((rows + 2 * REACH) * GRID_W, 2 * width), BF16),
-            pltpu.VMEM((q_rows, width), BF16),
+            pltpu.VMEM((rows * GRID_W, width), BF16),
             pltpu.VMEM((ctx_count, 2 * width), BF16),
             pltpu.VMEM((heads, block, keys), F32),
             pltpu.VMEM((heads, block, keys), BF16),
@@ -361,6 +363,162 @@
 
 def swap(count, bit):
     return [(i, i ^ bit) for i in range(count)]
+
+
+def tie(value, other):
+    return lax.optimization_barrier((value, other))[0]
+
+
+def plain(resid, mods, ctx, tables, weights, gains, context_bias, w_out, heads):
+    sp, tp = lax.axis_size("sp"), lax.axis_size("tp")
+    me_s = lax.axis_index("sp")
+    own = resid.shape[0]
+    tokens = own * tp
+    rows = tokens // GRID_W
+    piece = lax.all_gather(resid, "tp", axis=0, tiled=True)
+    q, kv = qkv([piece], mods, *weights, *gains, heads)
+    edge = REACH * GRID_W
+    above = lax.ppermute(kv[tokens - edge :], "sp", [(i, i + 1) for i in range(sp - 1)])
+    below = lax.ppermute(kv[:edge], "sp", [(i + 1, i) for i in range(sp - 1)])
+    span = 4 if rows % 4 == 0 else 2
+    groups = rows // span
+    meta = [me_s * rows, sp * rows, 0, 0, -REACH, rows]
+    meta += [i * span for i in range(groups)] + list(range(rows))
+    q_spec = [(0, 0, tokens)]
+    kv_spec = [(0, 0, tokens), (1, 0, edge), (2, 0, edge)]
+    attended = attend(
+        [q], q_spec, [kv, above, below], kv_spec, ctx, tables, context_bias, meta, span, groups, rows
+    )
+    full = lax.all_to_all(attended.reshape(tp, own, -1), "tp", split_axis=0, concat_axis=0)
+    return out_project(
+        [full[i] for i in range(tp)], jnp.arange(tp, dtype=jnp.int32), w_out, resid, mods
+    )
+
+
+CHUNKS = 3
+
+
+def chunk_row(parity, j, block_rows, chunk_rows):
+    return jnp.where(parity == 0, j * chunk_rows, block_rows - (j + 1) * chunk_rows)
+
+
+def staged_tokens(resid):
+    block_rows = resid.shape[0] // GRID_W
+    chunk_rows = block_rows // CHUNKS
+    parity = lax.axis_index("tp") % 2
+    across = []
+    for j in range(CHUNKS):
+        at = chunk_row(parity, j, block_rows, chunk_rows) * GRID_W
+        chunk = lax.dynamic_slice_in_dim(resid, at, chunk_rows * GRID_W)
+        across.append(lax.ppermute(chunk, "tp", swap(4, 2)))
+    partner = lax.ppermute(resid, "tp", swap(4, 1))
+    return partner, across
+
+
+def staged(resid, mods, staged_in, ctx, tables, weights, gains, context_bias, w_out, heads):
+    sp, tp = lax.axis_size("sp"), lax.axis_size("tp")
+    me_s, me_t = lax.axis_index("sp"), lax.axis_index("tp")
+    parity, chip = me_t % 2, me_t // 2
+    own = resid.shape[0]
+    block_rows = own // GRID_W
+    chunk_rows = block_rows // CHUNKS
+    chunk = chunk_rows * GRID_W
+    rows = block_rows * tp
+    chip_rows = 2 * block_rows
+    edge = REACH * GRID_W
+    partner, across = staged_in
+
+    def piece_row(source, j):
+        return source * block_rows + chunk_row(source % 2, j, block_rows, chunk_rows)
+
+    qs, kvs, q_spec, piece_rows = [], [], [], []
+
+    def project(pieces, piece_at):
+        q, kv = qkv(pieces, mods, *weights, *gains, heads)
+        at = 0
+        for piece, row in zip(pieces, piece_at):
+            q_spec.append((len(qs), at, piece.shape[0]))
+            piece_rows.append(row)
+            at += piece.shape[0]
+        qs.append(q)
+        kvs.append(kv)
+
+    project([resid, partner], [me_t * block_rows, (me_t ^ 1) * block_rows])
+    down = [(s * tp + t, (s - 1) * tp + t) for s in range(1, sp) for t in range(tp)]
+    up = [(s * tp + t, (s + 1) * tp + t) for s in range(sp - 1) for t in range(tp)]
+    early = [p for p in down if p[0] % tp < 2] + [p for p in up if p[0] % tp >= 2]
+    late = [p for p in up if p[0] % tp < 2] + [p for p in down if p[0] % tp >= 2]
+    at = jnp.where(chip == parity, 0, own) + jnp.where(chip == 0, 0, own - edge)
+    early_kv = lax.ppermute(
+        lax.dynamic_slice_in_dim(kvs[0], at, edge), ("sp", "tp"), early
+    )
+    early_row = jnp.where(chip == 0, rows, -REACH)
+
+    late_kv, late_rows = [], []
+    at = jnp.where(chip + parity == 1, 0, chunk)
+    beside = lax.ppermute(across[0], "tp", swap(4, 1))
+    for j in range(CHUNKS):
+        direct, beside = tie((across[j], beside), kvs[-1])
+        if j == 0:
+            following = lax.ppermute(tie(across[1], kvs[-1]), "tp", swap(4, 1))
+        project([direct, beside], [piece_row(me_t ^ 2, j), piece_row(me_t ^ 3, j)])
+        beside = following
+        if 0 < j < CHUNKS - 1:
+            beside = lax.ppermute(tie(across[j + 1], kvs[-1]), "tp", swap(4, 1))
+        if j * chunk_rows < REACH:
+            late_kv.append(
+                lax.ppermute(
+                    lax.dynamic_slice_in_dim(kvs[-1], at, chunk), ("sp", "tp"), late
+                )
+            )
+            late_rows.append(
+                jnp.where(chip == 0, -(j + 1) * chunk_rows, rows + j * chunk_rows)
+            )
+
+    def places(lead):
+        return [
+            (r + jnp.where(lead == 0, 0, block_rows)) % chip_rows for r in range(chip_rows)
+        ]
+
+    span = REACH
+    groups = chip_rows // span
+    head = [me_s * rows, sp * rows]
+    far_groups = [(1 - chip) * chip_rows + i * span for i in range(groups)]
+    near_groups = [chip * chip_rows + i * span for i in range(groups)]
+    far_spec = [(j - 1, at, size) for j, at, size in q_spec[2:]]
+    away = attend(
+        qs[1:],
+        far_spec,
+        kvs + [early_kv],
+        q_spec + [(len(kvs), 0, edge)],
+        ctx,
+        tables,
+        context_bias,
+        head + piece_rows[2:] + piece_rows + [early_row] + far_groups + places(parity),
+        span,
+        groups,
+        rows,
+    )
+    from_2 = lax.ppermute(away[:own], "tp", swap(4, 2))
+    from_3 = lax.ppermute(away[own:], "tp", swap(4, 3))
+
+    used = 2 + 2 * len(late_kv)
+    home = attend(
+        [tie(qs[0], away)],
+        q_spec[:2],
+        kvs[: 1 + len(late_kv)] + late_kv,
+        q_spec[:used] + [(1 + len(late_kv) + j, 0, chunk) for j in range(len(late_kv))],
+        ctx,
+        tables,
+        context_bias,
+        head + piece_rows[:2] + piece_rows[:used] + late_rows + near_groups + places(parity),
+        span,
+        groups,
+        rows,
+    )
+    from_1 = lax.ppermute(home[own:], "tp", swap(4, 1))
+    spots = me_t ^ jnp.arange(tp, dtype=jnp.int32)
+    return out_project([home[:own], from_1, from_2, from_3], spots, w_out, resid, mods)
 
 
 def shards(
@@ -382,47 +540,42 @@
 ):
     heads = offset_bias.shape[0]
     sp, tp = lax.axis_size("sp"), lax.axis_size("tp")
-    me_s, me_t = lax.axis_index("sp"), lax.axis_index("tp")
-    own = resid.shape[0]
-    tokens = own * tp
-    rows = tokens // GRID_W
+    me_t = lax.axis_index("tp")
+    block_rows = resid.shape[0] // GRID_W
+    split = tp == 4 and block_rows % CHUNKS == 0 and 2 * block_rows % REACH == 0
+    split = split and REACH % (block_rows // CHUNKS) == 0
 
     part = mod_part(cond, mod_shift, mod_scale, mod_gate)
     bit = 1
     while bit < sp:
         part = part + lax.ppermute(part, "sp", swap(sp, bit))
         bit *= 2
+    if split:
+        staged_in = staged_tokens(resid)
     parts = [part]
-    bit = 1
-    while bit < tp:
+    bit = tp // 2
+    while bit:
         parts += [lax.ppermute(p, "tp", swap(tp, bit)) for p in parts]
-        bit *= 2
-    spots = me_t ^ jnp.arange(tp, dtype=jnp.int32)
-    mods = place_mods(parts, spots, norm_gain)
+        bit //= 2
+    spots = [0]
+    bit = tp // 2
+    while bit:
+        spots += [v ^ bit for v in spots]
+        bit //= 2
+    mods = place_mods(parts, me_t ^ jnp.array(spots, jnp.int32), norm_gain)
 
     tables = bias_tables(offset_bias)
-    ctx = lax.all_gather(
-        context_kv(context, norm_gain, w_key, w_value, key_gain, heads), "sp", axis=0, tiled=True
-    )
-    piece = lax.all_gather(resid, "tp", axis=0, tiled=True)
-    q, kv = qkv([piece], mods, w_query, w_key, w_value, query_gain, key_gain, heads)
-
-    edge = REACH * GRID_W
-    above = lax.ppermute(kv[tokens - edge :], "sp", [(i, i + 1) for i in range(sp - 1)])
-    below = lax.ppermute(kv[:edge], "sp", [(i + 1, i) for i in range(sp - 1)])
-    span = 4 if rows % 4 == 0 else 2
-    groups = rows // span
-    meta = [me_s * rows, sp * rows, 0, -REACH, rows]
-    for i in range(groups):
-        meta += [i * span, i * span * GRID_W]
-    meta = jnp.stack([jnp.asarray(m, jnp.int32) for m in meta])
-    attended = attend(
-        [q], [kv, above, below], [ctx], tables, context_bias, meta, span, groups, rows
-    )
-    full = lax.all_to_all(attended.reshape(tp, own, -1), "tp", split_axis=0, concat_axis=0)
-    return out_project(
-        [full[i] for i in range(tp)], jnp.arange(tp, dtype=jnp.int32), w_out, resid, mods
-    )
+    ctx = context_kv(context, norm_gain, w_key, w_value, key_gain, heads)
+    bit = sp // 2
+    while bit:
+        ctx = jnp.concatenate([ctx, lax.ppermute(ctx, "sp", swap(sp, bit))], axis=0)
+        bit //= 2
+    weights, gains = (w_query, w_key, w_value), (query_gain, key_gain)
+    if split:
+        return staged(
+            resid, mods, staged_in, [ctx], tables, weights, gains, context_bias, w_out, heads
+        )
+    return plain(resid, mods, [ctx], tables, weights, gains, context_bias, w_out, heads)
 
 
 def solution(mesh):

time: 179 us -> 136 us (0.76)
  waiting for transfers between devices: 55.6 us -> 27.4 us
  starting transfers between devices: 16 us -> 42.1 us
  blocking collectives: 22.8 us -> 0 us
  between operations: 13.7 us -> 0.61 us
  local copies, waits for them, and re-layouts: 20.8 us -> 13.4 us
  other arithmetic: 0.03 us -> 2.16 us
    all_gather x2 -> x0, waiting for transfers between devices: 45.6 us -> none  [the longest x1 24 us: shards(): piece = lax.all_gather(resid, 'tp', axis=0, tiled=True)]
    ppermute x2 -> x16, starting transfers between devices: 4.69 us -> 35.4 us  [the longest x1 11.3 us: staged(): from_2 = lax.ppermute(away[:own], 'tp', swap(4, 2))]
    all_to_all x1 -> x0, blocking collectives: 22.8 us -> none  [shards(): lax.all_to_all(attended.reshape(tp, own, -1), 'tp', split_axis=0, concat_...]
    ppermute x2 -> x16, waiting for transfers between devices: 1.68 us -> 20.6 us  [the longest x1 9.92 us: staged(): from_2 = lax.ppermute(away[:own], 'tp', swap(4, 2))]
    unnamed x49 -> x69, local copies, waits for them, and re-layouts: 19.5 us -> 8.92 us
    dynamic_slice x0 -> x4, local copies, waits for them, and re-layouts: none -> 3.47 us  [the longest x1 1.74 us: staged_tokens(): chunk = lax.dynamic_slice_in_dim(resid, at, chunk_rows * GRID_W)]
    ppermute x3, starting transfers between devices: 8.27 us -> 5.85 us  [shards(): part = part + lax.ppermute(part, 'sp', swap(sp, bit))]
    ppermute x3, starting transfers between devices: 3.04 us -> 0.78 us  [shards(): parts += [lax.ppermute(p, 'tp', swap(tp, bit)) for p in parts]]
  transfers between devices with their start and end apart: 10 -> 22, of which waited for: 8 -> 8; matrix products, arithmetic and copies ran while one was open for 1% -> 5% of each run, Pallas kernels for 13% -> 24%
where the time goes in v2:
time: 136 us; the launch traced here: 135 us
  Pallas kernels  49.1 us (36%)
  starting transfers between devices  42.1 us (31%)
  waiting for transfers between devices  27.4 us (20%)
  local copies, waits for them, and re-layouts  13.4 us (10%)
  other arithmetic  2.16 us (2%)
    pallas_call x2, Pallas kernels, attend(): pl.pallas_call(functools.partial(attend_kernel, heads, span, groups, q_sp...  21.1 us
    pallas_call x4, Pallas kernels, qkv(): pl.pallas_call(functools.partial(qkv_kernel, len(pieces), heads, tile), o...  18.7 us
    ppermute x1, starting transfers between devices, staged(): from_2 = lax.ppermute(away[:own], 'tp', swap(4, 2))  11.3 us
    ppermute x1, waiting for transfers between devices, staged(): from_2 = lax.ppermute(away[:own], 'tp', swap(4, 2))  9.92 us
    ppermute x2, starting transfers between devices, staged(): lax.ppermute(lax.dynamic_slice_in_dim(kvs[-1], at, chunk), ('sp', 'tp'),...  9.2 us
    unnamed x69, local copies, waits for them, and re-layouts  8.92 us
    ppermute x1, waiting for transfers between devices, staged(): from_3 = lax.ppermute(away[own:], 'tp', swap(4, 3))  7.9 us
    ppermute x3, starting transfers between devices, shards(): ctx = jnp.concatenate([ctx, lax.ppermute(ctx, 'sp', swap(sp, bit))], axis=0)  6.67 us
  transfers between devices with their start and end apart: 22, of which 8 were waited for; matrix products, arithmetic and copies ran while one was open for 5% of the time, Pallas kernels for 24%

profile of v2, /device:TPU:0, one launch (start us, length us, event | category | flops | bytes accessed | tf_op | source)
XLA Modules:
  0.0 134.7 jit_solution(14928256452466025075)
XLA Ops:
  0.5 1.7 %constant_dynamic-slice_fusion.3 = (bf16[128,2048]{1,0:T(8,128)(2,1)S(1)}, bf16[128,2048]{1,0:T(8,128)(2,1)S(1)}, bf16[128,2048]{1,0:T(8,128)(2,1)S(1)}) fusion(bf16[384,2048]{1,0:T(8,128)(2,1)} %refs_5_.9, s32[]{:T(128)S(6)} %select_n.209, s32[]{:T(128)S(6)} %select_n.207), kind=kLoop, calls=%fused_computation.6 | loop fusion | bytes 3145736 | tf_op jit(solution)/shard_map/dynamic_slice | solution.py:412
  2.2 2.5 %collective-permute-start.7 = (bf16[128,2048]{1,0:T(8,128)(2,1)S(1)}, bf16[128,2048]{1,0:T(8,128)(2,1)S(1)}, u32[]{:S(2)}, u32[]{:S(2)}) collective-permute-start(bf16[128,2048]{1,0:T(8,128)(2,1)S(1)} %get-tuple-element.41), channel_id=1, source_target_pairs={{0,2},{1,3},{2,0},{3,1},{4,6},{5,7},{6,4},{7,5},{8,10},{9,11},{10,... | collective-permute-start | bytes 1572872 | tf_op jit(solution)/shard_map/ppermute | solution.py:413
  8.5 1.6 %collective-permute-start.1 = (f32[1,1536]{1,0:T(1,128)S(1)}, f32[1,1536]{1,0:T(1,128)S(1)}, u32[]{:S(2)}, u32[]{:S(2)}) collective-permute-start(f32[1,1536]{1,0:T(1,128)S(1)} %mod_part.1), channel_id=1, source_target_pairs={{0,4},{4,0},{8,12},{12,8},{16,20},{20,16},{24,28},{28,24},{1,5},{5... | collective-permute-start | bytes 18440 | tf_op jit(solution)/shard_map/ppermute | solution.py:551
  10.0 2.1 %collective-permute-done.1 = f32[1,1536]{1,0:T(1,128)S(1)} collective-permute-done((f32[1,1536]{1,0:T(1,128)S(1)}, f32[1,1536]{1,0:T(1,128)S(1)}, u32[]{:S(2)}, u32[]{:S(2)}) %collective-permute-start.1) | collective-permute-done | bytes 6176 | tf_op jit(solution)/shard_map/ppermute | solution.py:551
  12.2 1.6 %collective-permute-start.2 = (f32[1,1536]{1,0:T(1,128)S(1)}, f32[1,1536]{1,0:T(1,128)S(1)}, u32[]{:S(2)}, u32[]{:S(2)}) collective-permute-start(f32[1,1536]{1,0:T(1,128)S(1)} %add.200), channel_id=1, source_target_pairs={{0,8},{4,12},{8,0},{12,4},{16,24},{20,28},{24,16},{28,20},{1,9},{5... | collective-permute-start | bytes 18440 | tf_op jit(solution)/shard_map/ppermute | solution.py:551
  13.8 2.1 %collective-permute-done.2 = f32[1,1536]{1,0:T(1,128)S(1)} collective-permute-done((f32[1,1536]{1,0:T(1,128)S(1)}, f32[1,1536]{1,0:T(1,128)S(1)}, u32[]{:S(2)}, u32[]{:S(2)}) %collective-permute-start.2) | collective-permute-done | bytes 6176 | tf_op jit(solution)/shard_map/ppermute | solution.py:551
  15.9 2.7 %collective-permute-start.3 = (f32[1,1536]{1,0:T(1,128)S(1)}, f32[1,1536]{1,0:T(1,128)S(1)}, u32[]{:S(2)}, u32[]{:S(2)}) collective-permute-start(f32[1,1536]{1,0:T(1,128)S(1)} %add.201), channel_id=1, source_target_pairs={{0,16},{4,20},{8,24},{12,28},{16,0},{20,4},{24,8},{28,12},{1,17},{... | collective-permute-start | bytes 18440 | tf_op jit(solution)/shard_map/ppermute | solution.py:551
  18.5 1.9 %collective-permute-done.3 = f32[1,1536]{1,0:T(1,128)S(1)} collective-permute-done((f32[1,1536]{1,0:T(1,128)S(1)}, f32[1,1536]{1,0:T(1,128)S(1)}, u32[]{:S(2)}, u32[]{:S(2)}) %collective-permute-start.3) | collective-permute-done | bytes 6176 | tf_op jit(solution)/shard_map/ppermute | solution.py:551
  20.7 1.6 %copy-done.1 = bf16[2048,512]{1,0:T(8,128)(2,1)S(1)} copy-done((bf16[2048,512]{1,0:T(8,128)(2,1)S(1)}, bf16[2048,512]{1,0:T(8,128)(2,1)}, u32[]{:S(2)}) %copy-start.1) | copy-done | bytes 2097176
  24.6 3.0 %collective-permute-start.14 = (bf16[64,1024]{1,0:T(8,128)(2,1)S(1)}, bf16[64,1024]{1,0:T(8,128)(2,1)S(1)}, u32[]{:S(2)}, u32[]{:S(2)}) collective-permute-start(bf16[64,1024]{1,0:T(8,128)(2,1)S(1)} %context_kv.1), channel_id=1, source_target_pairs={{0,16},{4,20},{8,24},{12,28},{16,0},{20,4},{24,8},{28,12},{1,17},{... | collective-permute-start | bytes 393224 | tf_op jit(solution)/shard_map/ppermute | solution.py:571
  28.8 1.5 %collective-permute-start.9 = (bf16[128,2048]{1,0:T(8,128)(2,1)S(1)}, bf16[128,2048]{1,0:T(8,128)(2,1)S(1)}, u32[]{:S(2)}, u32[]{:S(2)}) collective-permute-start(bf16[128,2048]{1,0:T(8,128)(2,1)S(1)} %get-tuple-element.40), channel_id=1, source_target_pairs={{0,2},{1,3},{2,0},{3,1},{4,6},{5,7},{6,4},{7,5},{8,10},{9,11},{10,... | collective-permute-start | bytes 1572872 | tf_op jit(solution)/shard_map/ppermute | solution.py:413
  30.9 2.2 %collective-permute-start.15 = (bf16[128,1024]{1,0:T(8,128)(2,1)S(1)}, bf16[128,1024]{1,0:T(8,128)(2,1)S(1)}, u32[]{:S(2)}, u32[]{:S(2)}) collective-permute-start(bf16[128,1024]{1,0:T(8,128)(2,1)S(1)} %pad_maximum_fusion.2), channel_id=1, source_target_pairs={{0,8},{4,12},{8,0},{12,4},{16,24},{20,28},{24,16},{28,20},{1,9},{5... | collective-permute-start | bytes 786440 | tf_op jit(solution)/shard_map/ppermute | solution.py:571
  33.1 10.1 %qkv.4 = (bf16[768,512]{1,0:T(8,128)(2,1)S(1)}, bf16[768,1024]{1,0:T(8,128)(2,1)S(1)}) custom-call(bf16[384,2048]{1,0:T(8,128)(2,1)S(1)} %copy-done.6, bf16[384,2048]{1,0:T(8,128)(2,1)} %collective-permute-done.refs_1_, f32[8,2048]{1,0:T(8,128)S(1)} %place_mods.1.refs_2_.refs_6_, bf16[2048,512]{1,0:T(8,128)(2,1)S(1)} %copy-done.4, ...), custom_call_target="tpu_custom_call" | custom-call | flops 4831838208 | bytes 9437184 | tf_op jit(solution)/shard_map/qkv/pallas_call | solution.py:168
  43.2 1.1 copy-done.12
  44.8 1.5 %collective-permute-start.11 = (bf16[128,2048]{1,0:T(8,128)(2,1)S(1)}, bf16[128,2048]{1,0:T(8,128)(2,1)S(1)}, u32[]{:S(2)}, u32[]{:S(2)}) collective-permute-start(bf16[128,2048]{1,0:T(8,128)(2,1)S(1)} %get-tuple-element.39), channel_id=1, source_target_pairs={{0,2},{1,3},{2,0},{3,1},{4,6},{5,7},{6,4},{7,5},{8,10},{9,11},{10,... | collective-permute-start | bytes 1572872 | tf_op jit(solution)/shard_map/ppermute | solution.py:413
  47.3 1.5 %collective-permute-start.16 = (bf16[256,1024]{1,0:T(8,128)(2,1)}, bf16[256,1024]{1,0:T(8,128)(2,1)}, u32[]{:S(2)}, u32[]{:S(2)}) collective-permute-start(bf16[256,1024]{1,0:T(8,128)(2,1)} %pad_maximum_fusion.1), channel_id=1, source_target_pairs={{0,4},{4,0},{8,12},{12,8},{16,20},{20,16},{24,28},{28,24},{1,5},{5... | collective-permute-start | bytes 1572872 | tf_op jit(solution)/shard_map/ppermute | solution.py:571
  48.8 2.9 %qkv.5 = (bf16[256,512]{1,0:T(8,128)(2,1)S(1)}, bf16[256,1024]{1,0:T(8,128)(2,1)S(1)}) custom-call(bf16[128,2048]{1,0:T(8,128)(2,1)S(1)} %collective-permute-done.7.refs_0_, bf16[128,2048]{1,0:T(8,128)(2,1)S(1)} %collective-permute-done.8.refs_1_, f32[8,2048]{1,0:T(8,128)S(1)} %place_mods.1.refs_2_.refs_6_, bf16[2048,512]{1,0:T(8,128)(2,1)S(1)} %copy-done.4, ...), custom_call_target="tpu_custom_call" | custom-call | flops 1610612736 | bytes 7340032 | tf_op jit(solution)/shard_map/qkv/pallas_call | solution.py:168
  51.8 2.9 %qkv.6 = (bf16[256,512]{1,0:T(8,128)(2,1)S(1)}, bf16[256,1024]{1,0:T(8,128)(2,1)S(1)}) custom-call(bf16[128,2048]{1,0:T(8,128)(2,1)S(1)} %collective-permute-done.9.refs_0_, bf16[128,2048]{1,0:T(8,128)(2,1)S(1)} %collective-permute-done.10.refs_1_, f32[8,2048]{1,0:T(8,128)S(1)} %place_mods.1.refs_2_.refs_6_, bf16[2048,512]{1,0:T(8,128)(2,1)S(1)} %copy-done.4, ...), custom_call_target="tpu_custom_call" | custom-call | flops 1610612736 | bytes 7340032 | tf_op jit(solution)/shard_map/qkv/pallas_call | solution.py:168
  56.2 2.6 %collective-permute-done.11.refs_0_ = bf16[128,2048]{1,0:T(8,128)(2,1)S(1)} collective-permute-done((bf16[128,2048]{1,0:T(8,128)(2,1)S(1)}, bf16[128,2048]{1,0:T(8,128)(2,1)S(1)}, u32[]{:S(2)}, u32[]{:S(2)}) %collective-permute-start.11) | collective-permute-done | bytes 524320 | tf_op jit(solution)/shard_map/ppermute | solution.py:413
  59.2 1.0 bias_tables.1.refs_9_.refs_7_
  60.6 1.6 %collective-permute-start.13 = (bf16[256,1024]{1,0:T(8,128)(2,1)S(1)}, bf16[256,1024]{1,0:T(8,128)(2,1)S(1)}, u32[]{:S(2)}, u32[]{:S(2)}) collective-permute-start(bf16[256,1024]{1,0:T(8,128)(2,1)S(1)} %constant_dynamic-slice_fusion.2), channel_id=1, source_target_pairs={{4,0},{5,1},{8,4},{9,5},{12,8},{13,9},{16,12},{17,13},{20,16},{21,... | collective-permute-start | bytes 1572872 | tf_op jit(solution)/shard_map/ppermute | solution.py:452
  62.2 1.2 pad_maximum_fusion.refs_8_.refs_6_
  63.4 4.6 %collective-permute-start.17 = (bf16[128,1024]{1,0:T(8,128)(2,1)S(1)}, bf16[128,1024]{1,0:T(8,128)(2,1)S(1)}, u32[]{:S(2)}, u32[]{:S(2)}) collective-permute-start(bf16[128,1024]{1,0:T(8,128)(2,1)S(1)} %constant_dynamic-slice_fusion.1), channel_id=1, source_target_pairs={{0,4},{1,5},{4,8},{5,9},{8,12},{9,13},{12,16},{13,17},{16,20},{17,... | collective-permute-start | bytes 786440 | tf_op jit(solution)/shard_map/ppermute | solution.py:470
  68.0 1.7 %constant_dynamic-slice_fusion = bf16[128,1024]{1,0:T(8,128)(2,1)} fusion(bf16[256,1024]{1,0:T(8,128)(2,1)} %copy-done.16, s32[]{:T(128)S(6)} %select_n.213), kind=kLoop, calls=%fused_computation.3 | loop fusion | bytes 524292 | tf_op jit(solution)/shard_map/dynamic_slice | solution.py:471
  69.7 4.6 %collective-permute-start.18 = (bf16[128,1024]{1,0:T(8,128)(2,1)}, bf16[128,1024]{1,0:T(8,128)(2,1)S(1)}, u32[]{:S(2)}, u32[]{:S(2)}) collective-permute-start(bf16[128,1024]{1,0:T(8,128)(2,1)} %constant_dynamic-slice_fusion), channel_id=1, source_target_pairs={{0,4},{1,5},{4,8},{5,9},{8,12},{9,13},{12,16},{13,17},{16,20},{17,... | collective-permute-start | bytes 786440 | tf_op jit(solution)/shard_map/ppermute | solution.py:470
  74.3 2.9 %qkv.7 = (bf16[256,512]{1,0:T(8,128)(2,1)S(1)}, bf16[256,1024]{1,0:T(8,128)(2,1)S(1)}) custom-call(bf16[128,2048]{1,0:T(8,128)(2,1)S(1)} %collective-permute-done.11.refs_0_, bf16[128,2048]{1,0:T(8,128)(2,1)S(1)} %collective-permute-done.12.refs_1_, f32[8,2048]{1,0:T(8,128)S(1)} %place_mods.1.refs_2_.refs_6_, bf16[2048,512]{1,0:T(8,128)(2,1)S(1)} %copy-done.5, ...), custom_call_target="tpu_custom_call" | custom-call | flops 1610612736 | bytes 7340032 | tf_op jit(solution)/shard_map/qkv/pallas_call | solution.py:168
  77.3 10.6 %attend.2 = bf16[768,512]{1,0:T(8,128)(2,1)S(1)} custom-call(s32[32]{0:T(128)S(1)} %stack.154.meta_ref, f32[4]{0:T(128)S(1)} %copy-done.26, bf16[256,512]{1,0:T(8,128)(2,1)S(1)} %copy-done.23, bf16[256,512]{1,0:T(8,128)(2,1)S(1)} %copy-done.25, bf16[256,512]{1,0:T(8,128)(2,1)S(1)} %get-tuple-element.36.refs_2_, bf16[768,1024]{1,0:T(8,128)(2,1)S(1)} %copy-done.13, ...), custom_call_target="tpu_custom_call" | custom-call | flops 4026531840 | bytes 8388608 | tf_op jit(solution)/shard_map/attend/pallas_call | solution.py:314
  88.2 10.5 %attend.3 = bf16[768,512]{1,0:T(8,128)(2,1)S(1)} custom-call(s32[27]{0:T(128)S(1)} %stack.147.meta_ref, f32[4]{0:T(128)S(1)} %copy-done.26, bf16[768,512]{1,0:T(8,128)(2,1)S(1)} %copy-done.28, bf16[768,1024]{1,0:T(8,128)(2,1)S(1)} %copy-done.13, bf16[256,1024]{1,0:T(8,128)(2,1)S(1)} %copy-done.15, bf16[256,1024]{1,0:T(8,128)(2,1)S(1)} %copy-done.17, ...), custom_call_target="tpu_custom_call" | custom-call | flops 4026531840 | bytes 8388608 | tf_op jit(solution)/shard_map/attend/pallas_call | solution.py:314
  98.9 11.3 %collective-permute-start.20 = (bf16[384,512]{1,0:T(8,128)(2,1)S(1)}, bf16[384,512]{1,0:T(8,128)(2,1)S(1)}, u32[]{:S(2)}, u32[]{:S(2)}) collective-permute-start(bf16[384,512]{1,0:T(8,128)(2,1)S(1)} %get-tuple-element.43), channel_id=1, source_target_pairs={{0,2},{1,3},{2,0},{3,1},{4,6},{5,7},{6,4},{7,5},{8,10},{9,11},{10,... | collective-permute-start | bytes 1179656 | tf_op jit(solution)/shard_map/ppermute | solution.py:502
  110.3 9.9 %collective-permute-done.20.refs_2_ = bf16[384,512]{1,0:T(8,128)(2,1)S(1)} collective-permute-done((bf16[384,512]{1,0:T(8,128)(2,1)S(1)}, bf16[384,512]{1,0:T(8,128)(2,1)S(1)}, u32[]{:S(2)}, u32[]{:S(2)}) %collective-permute-start.20) | collective-permute-done | bytes 393248 | tf_op jit(solution)/shard_map/ppermute | solution.py:502
  120.2 7.9 %collective-permute-done.21.refs_3_ = bf16[384,512]{1,0:T(8,128)(2,1)S(1)} collective-permute-done((bf16[384,512]{1,0:T(8,128)(2,1)S(1)}, bf16[384,512]{1,0:T(8,128)(2,1)S(1)}, u32[]{:S(2)}, u32[]{:S(2)}) %collective-permute-start.21) | collective-permute-done | bytes 393248 | tf_op jit(solution)/shard_map/ppermute | solution.py:503
  128.1 6.5 %out_project.1 = bf16[384,2048]{1,0:T(8,128)(2,1)} custom-call(s32[4]{0:T(128)S(1)} %iota_xor_fusion.spots_ref, bf16[384,512]{1,0:T(8,128)(2,1)S(1)} %get-tuple-element.45.refs_0_, bf16[384,512]{1,0:T(8,128)(2,1)S(1)} %collective-permute-done.19.refs_1_, bf16[384,512]{1,0:T(8,128)(2,1)S(1)} %collective-permute-done.20.refs_2_, ...), custom_call_target="tpu_custom_call" | custom-call | flops 3221225472 | bytes 11534336 | tf_op jit(solution)/shard_map/out_project/pallas_call | solution.py:353
  (111 shorter events, 12.7 us)
Async XLA Ops:
  0.0 20.7 %copy-start = (bf16[2048,512]{1,0:T(8,128)(2,1)S(1)}, bf16[2048,512]{1,0:T(8,128)(2,1)}, u32[]{:S(2)}) copy-start(bf16[2048,512]{1,0:T(8,128)(2,1)} %wk_ref.1) | copy-start | bytes 6291460
  0.0 20.7 %copy-start.8 = (bf16[64,2048]{1,0:T(8,128)(2,1)S(1)}, bf16[64,2048]{1,0:T(8,128)(2,1)}, u32[]{:S(2)}) copy-start(bf16[64,2048]{1,0:T(8,128)(2,1)} %x_ref.1) | copy-start | bytes 786436
  0.0 33.1 %collective-permute-start = (bf16[384,2048]{1,0:T(8,128)(2,1)}, bf16[384,2048]{1,0:T(8,128)(2,1)}, u32[]{:S(2)}, u32[]{:S(2)}) collective-permute-start(bf16[384,2048]{1,0:T(8,128)(2,1)} %refs_5_.9), channel_id=1, source_target_pairs={{0,1},{1,0},{2,3},{3,2},{4,5},{5,4},{6,7},{7,6},{8,9},{9,8},{10,11... | collective-permute-start | bytes 4718600 | tf_op jit(solution)/shard_map/ppermute | solution.py:414
  0.5 32.6 %copy-start.6 = (bf16[384,2048]{1,0:T(8,128)(2,1)S(1)}, bf16[384,2048]{1,0:T(8,128)(2,1)}, u32[]{:S(2)}) copy-start(bf16[384,2048]{1,0:T(8,128)(2,1)} %refs_5_.9) | copy-start | bytes 4718596
  2.2 30.8 %collective-permute-start.7 = (bf16[128,2048]{1,0:T(8,128)(2,1)S(1)}, bf16[128,2048]{1,0:T(8,128)(2,1)S(1)}, u32[]{:S(2)}, u32[]{:S(2)}) collective-permute-start(bf16[128,2048]{1,0:T(8,128)(2,1)S(1)} %get-tuple-element.41), channel_id=1, source_target_pairs={{0,2},{1,3},{2,0},{3,1},{4,6},{5,7},{6,4},{7,5},{8,10},{9,11},{10,... | collective-permute-start | bytes 1572872 | tf_op jit(solution)/shard_map/ppermute | solution.py:413
  8.5 3.7 %collective-permute-start.1 = (f32[1,1536]{1,0:T(1,128)S(1)}, f32[1,1536]{1,0:T(1,128)S(1)}, u32[]{:S(2)}, u32[]{:S(2)}) collective-permute-start(f32[1,1536]{1,0:T(1,128)S(1)} %mod_part.1), channel_id=1, source_target_pairs={{0,4},{4,0},{8,12},{12,8},{16,20},{20,16},{24,28},{28,24},{1,5},{5... | collective-permute-start | bytes 18440 | tf_op jit(solution)/shard_map/ppermute | solution.py:551
  12.2 3.7 %collective-permute-start.2 = (f32[1,1536]{1,0:T(1,128)S(1)}, f32[1,1536]{1,0:T(1,128)S(1)}, u32[]{:S(2)}, u32[]{:S(2)}) collective-permute-start(f32[1,1536]{1,0:T(1,128)S(1)} %add.200), channel_id=1, source_target_pairs={{0,8},{4,12},{8,0},{12,4},{16,24},{20,28},{24,16},{28,20},{1,9},{5... | collective-permute-start | bytes 18440 | tf_op jit(solution)/shard_map/ppermute | solution.py:551
  15.9 4.6 %collective-permute-start.3 = (f32[1,1536]{1,0:T(1,128)S(1)}, f32[1,1536]{1,0:T(1,128)S(1)}, u32[]{:S(2)}, u32[]{:S(2)}) collective-permute-start(f32[1,1536]{1,0:T(1,128)S(1)} %add.201), channel_id=1, source_target_pairs={{0,16},{4,20},{8,24},{12,28},{16,0},{20,4},{24,8},{28,12},{1,17},{... | collective-permute-start | bytes 18440 | tf_op jit(solution)/shard_map/ppermute | solution.py:551
  20.5 7.2 %collective-permute-start.4 = (f32[1,1536]{1,0:T(1,128)S(1)}, f32[1,1536]{1,0:T(1,128)S(1)}, u32[]{:S(2)}, u32[]{:S(2)}) collective-permute-start(f32[1,1536]{1,0:T(1,128)S(1)} %add.202.refs_0_), channel_id=1, source_target_pairs={{0,2},{1,3},{2,0},{3,1},{4,6},{5,7},{6,4},{7,5},{8,10},{9,11},{10,... | collective-permute-start | bytes 18440 | tf_op jit(solution)/shard_map/ppermute | solution.py:558
  23.7 9.4 %copy-start.21 = (f32[128]{0:T(128)S(1)}, f32[128]{0:T(128)}, u32[]{:S(2)}) copy-start(f32[128]{0:T(128)} %param.26) | copy-start | bytes 1540
  24.6 6.2 %collective-permute-start.14 = (bf16[64,1024]{1,0:T(8,128)(2,1)S(1)}, bf16[64,1024]{1,0:T(8,128)(2,1)S(1)}, u32[]{:S(2)}, u32[]{:S(2)}) collective-permute-start(bf16[64,1024]{1,0:T(8,128)(2,1)S(1)} %context_kv.1), channel_id=1, source_target_pairs={{0,16},{4,20},{8,24},{12,28},{16,0},{20,4},{24,8},{28,12},{1,17},{... | collective-permute-start | bytes 393224 | tf_op jit(solution)/shard_map/ppermute | solution.py:571
  27.6 1.2 collective-permute-start.5
  27.6 2.7 %collective-permute-start.6 = (f32[1,1536]{1,0:T(1,128)S(1)}, f32[1,1536]{1,0:T(1,128)S(1)}, u32[]{:S(2)}, u32[]{:S(2)}) collective-permute-start(f32[1,1536]{1,0:T(1,128)S(1)} %collective-permute-done.4.refs_1_), channel_id=1, source_target_pairs={{0,1},{1,0},{2,3},{3,2},{4,5},{5,4},{6,7},{7,6},{8,9},{9,8},{10,11... | collective-permute-start | bytes 18440 | tf_op jit(solution)/shard_map/ppermute | solution.py:558
  28.8 15.5 %collective-permute-start.9 = (bf16[128,2048]{1,0:T(8,128)(2,1)S(1)}, bf16[128,2048]{1,0:T(8,128)(2,1)S(1)}, u32[]{:S(2)}, u32[]{:S(2)}) collective-permute-start(bf16[128,2048]{1,0:T(8,128)(2,1)S(1)} %get-tuple-element.40), channel_id=1, source_target_pairs={{0,2},{1,3},{2,0},{3,1},{4,6},{5,7},{6,4},{7,5},{8,10},{9,11},{10,... | collective-permute-start | bytes 1572872 | tf_op jit(solution)/shard_map/ppermute | solution.py:413
  30.9 15.5 %collective-permute-start.15 = (bf16[128,1024]{1,0:T(8,128)(2,1)S(1)}, bf16[128,1024]{1,0:T(8,128)(2,1)S(1)}, u32[]{:S(2)}, u32[]{:S(2)}) collective-permute-start(bf16[128,1024]{1,0:T(8,128)(2,1)S(1)} %pad_maximum_fusion.2), channel_id=1, source_target_pairs={{0,8},{4,12},{8,0},{12,4},{16,24},{20,28},{24,16},{28,20},{1,9},{5... | collective-permute-start | bytes 786440 | tf_op jit(solution)/shard_map/ppermute | solution.py:571
  33.1 15.8 %collective-permute-start.8 = (bf16[128,2048]{1,0:T(8,128)(2,1)S(1)}, bf16[128,2048]{1,0:T(8,128)(2,1)S(1)}, u32[]{:S(2)}, u32[]{:S(2)}) collective-permute-start(bf16[128,2048]{1,0:T(8,128)(2,1)S(1)} %collective-permute-done.7.refs_0_), channel_id=1, source_target_pairs={{0,1},{1,0},{2,3},{3,2},{4,5},{5,4},{6,7},{7,6},{8,9},{9,8},{10,11... | collective-permute-start | bytes 1572872 | tf_op jit(solution)/shard_map/ppermute | solution.py:459
  44.3 7.4 %collective-permute-start.10 = (bf16[128,2048]{1,0:T(8,128)(2,1)S(1)}, bf16[128,2048]{1,0:T(8,128)(2,1)S(1)}, u32[]{:S(2)}, u32[]{:S(2)}) collective-permute-start(bf16[128,2048]{1,0:T(8,128)(2,1)S(1)} %collective-permute-done.9.refs_0_), channel_id=1, source_target_pairs={{0,1},{1,0},{2,3},{3,2},{4,5},{5,4},{6,7},{7,6},{8,9},{9,8},{10,11... | collective-permute-start | bytes 1572872 | tf_op jit(solution)/shard_map/ppermute | solution.py:463
  44.8 13.9 %collective-permute-start.11 = (bf16[128,2048]{1,0:T(8,128)(2,1)S(1)}, bf16[128,2048]{1,0:T(8,128)(2,1)S(1)}, u32[]{:S(2)}, u32[]{:S(2)}) collective-permute-start(bf16[128,2048]{1,0:T(8,128)(2,1)S(1)} %get-tuple-element.39), channel_id=1, source_target_pairs={{0,2},{1,3},{2,0},{3,1},{4,6},{5,7},{6,4},{7,5},{8,10},{9,11},{10,... | collective-permute-start | bytes 1572872 | tf_op jit(solution)/shard_map/ppermute | solution.py:413
  47.3 14.8 %collective-permute-start.16 = (bf16[256,1024]{1,0:T(8,128)(2,1)}, bf16[256,1024]{1,0:T(8,128)(2,1)}, u32[]{:S(2)}, u32[]{:S(2)}) collective-permute-start(bf16[256,1024]{1,0:T(8,128)(2,1)} %pad_maximum_fusion.1), channel_id=1, source_target_pairs={{0,4},{4,0},{8,12},{12,8},{16,20},{20,16},{24,28},{28,24},{1,5},{5... | collective-permute-start | bytes 1572872 | tf_op jit(solution)/shard_map/ppermute | solution.py:571
  58.7 15.6 %collective-permute-start.12 = (bf16[128,2048]{1,0:T(8,128)(2,1)S(1)}, bf16[128,2048]{1,0:T(8,128)(2,1)S(1)}, u32[]{:S(2)}, u32[]{:S(2)}) collective-permute-start(bf16[128,2048]{1,0:T(8,128)(2,1)S(1)} %collective-permute-done.11.refs_0_), channel_id=1, source_target_pairs={{0,1},{1,0},{2,3},{3,2},{4,5},{5,4},{6,7},{7,6},{8,9},{9,8},{10,11... | collective-permute-start | bytes 1572872 | tf_op jit(solution)/shard_map/ppermute | solution.py:467
  60.5 13.8 %copy-start.3 = (bf16[2048,512]{1,0:T(8,128)(2,1)S(1)}, bf16[2048,512]{1,0:T(8,128)(2,1)}, u32[]{:S(2)}) copy-start(bf16[2048,512]{1,0:T(8,128)(2,1)} %wv_ref.1) | copy-start | bytes 6291460
  60.5 13.8 %copy-start.5 = (bf16[2048,512]{1,0:T(8,128)(2,1)S(1)}, bf16[2048,512]{1,0:T(8,128)(2,1)}, u32[]{:S(2)}) copy-start(bf16[2048,512]{1,0:T(8,128)(2,1)} %refs_3_.7) | copy-start | bytes 6291460
  60.6 16.7 %collective-permute-start.13 = (bf16[256,1024]{1,0:T(8,128)(2,1)S(1)}, bf16[256,1024]{1,0:T(8,128)(2,1)S(1)}, u32[]{:S(2)}, u32[]{:S(2)}) collective-permute-start(bf16[256,1024]{1,0:T(8,128)(2,1)S(1)} %constant_dynamic-slice_fusion.2), channel_id=1, source_target_pairs={{4,0},{5,1},{8,4},{9,5},{12,8},{13,9},{16,12},{17,13},{20,16},{21,... | collective-permute-start | bytes 1572872 | tf_op jit(solution)/shard_map/ppermute | solution.py:452
  63.4 24.6 %collective-permute-start.17 = (bf16[128,1024]{1,0:T(8,128)(2,1)S(1)}, bf16[128,1024]{1,0:T(8,128)(2,1)S(1)}, u32[]{:S(2)}, u32[]{:S(2)}) collective-permute-start(bf16[128,1024]{1,0:T(8,128)(2,1)S(1)} %constant_dynamic-slice_fusion.1), channel_id=1, source_target_pairs={{0,4},{1,5},{4,8},{5,9},{8,12},{9,13},{12,16},{13,17},{16,20},{17,... | collective-permute-start | bytes 786440 | tf_op jit(solution)/shard_map/ppermute | solution.py:470
  69.7 18.6 %collective-permute-start.18 = (bf16[128,1024]{1,0:T(8,128)(2,1)}, bf16[128,1024]{1,0:T(8,128)(2,1)S(1)}, u32[]{:S(2)}, u32[]{:S(2)}) collective-permute-start(bf16[128,1024]{1,0:T(8,128)(2,1)} %constant_dynamic-slice_fusion), channel_id=1, source_target_pairs={{0,4},{1,5},{4,8},{5,9},{8,12},{9,13},{12,16},{13,17},{16,20},{17,... | collective-permute-start | bytes 786440 | tf_op jit(solution)/shard_map/ppermute | solution.py:470
  77.3 10.9 %copy-start.28 = (bf16[768,512]{1,0:T(8,128)(2,1)S(1)}, bf16[768,512]{1,0:T(8,128)(2,1)}, u32[]{:S(2)}) copy-start(bf16[768,512]{1,0:T(8,128)(2,1)} %copy-done.27) | copy-start | bytes 2359300
  87.9 40.2 %slice-start = ((s8[8388608]{0:T(1024)(128)(4,1)}), s8[4194304]{0:T(1024)(128)(4,1)S(1)}, s32[]{:S(2)}) async-start(s8[8388608]{0:T(1024)(128)(4,1)} %bitcast.33), calls=%async_computation | async-start | bytes 8388608
  88.0 40.1 %slice-start.1 = ((s8[8388608]{0:T(1024)(128)(4,1)}), s8[4194304]{0:T(1024)(128)(4,1)S(1)}, s32[]{:S(2)}) async-start(s8[8388608]{0:T(1024)(128)(4,1)} %bitcast.33), calls=%async_computation.1 | async-start | bytes 8388608
  98.8 29.4 %copy-start.7 = (bf16[384,2048]{1,0:T(8,128)(2,1)S(1)}, bf16[384,2048]{1,0:T(8,128)(2,1)}, u32[]{:S(2)}) copy-start(bf16[384,2048]{1,0:T(8,128)(2,1)} %refs_5_.9) | copy-start | bytes 4718596
  98.8 11.4 %collective-permute-start.19 = (bf16[384,512]{1,0:T(8,128)(2,1)S(1)}, bf16[384,512]{1,0:T(8,128)(2,1)S(1)}, u32[]{:S(2)}, u32[]{:S(2)}) collective-permute-start(bf16[384,512]{1,0:T(8,128)(2,1)S(1)} %get-tuple-element.44), channel_id=1, source_target_pairs={{0,1},{1,0},{2,3},{3,2},{4,5},{5,4},{6,7},{7,6},{8,9},{9,8},{10,11... | collective-permute-start | bytes 1179656 | tf_op jit(solution)/shard_map/ppermute | solution.py:519
  98.9 21.3 %collective-permute-start.20 = (bf16[384,512]{1,0:T(8,128)(2,1)S(1)}, bf16[384,512]{1,0:T(8,128)(2,1)S(1)}, u32[]{:S(2)}, u32[]{:S(2)}) collective-permute-start(bf16[384,512]{1,0:T(8,128)(2,1)S(1)} %get-tuple-element.43), channel_id=1, source_target_pairs={{0,2},{1,3},{2,0},{3,1},{4,6},{5,7},{6,4},{7,5},{8,10},{9,11},{10,... | collective-permute-start | bytes 1179656 | tf_op jit(solution)/shard_map/ppermute | solution.py:502
  110.2 17.9 %collective-permute-start.21 = (bf16[384,512]{1,0:T(8,128)(2,1)S(1)}, bf16[384,512]{1,0:T(8,128)(2,1)S(1)}, u32[]{:S(2)}, u32[]{:S(2)}) collective-permute-start(bf16[384,512]{1,0:T(8,128)(2,1)S(1)} %get-tuple-element.42), channel_id=1, source_target_pairs={{0,3},{1,2},{2,1},{3,0},{4,7},{5,6},{6,5},{7,4},{8,11},{9,10},{10,... | collective-permute-start | bytes 1179656 | tf_op jit(solution)/shard_map/ppermute | solution.py:503
  (24 other events, 102.9 us)

commit v3 on v1

v3 whole, which is shorter than its diff:
```python
import functools
import math

import jax
import jax.numpy as jnp
from jax import lax
from jax.experimental import pallas as pl
from jax.experimental.pallas import tpu as pltpu
from jax.sharding import PartitionSpec as P


HEAD_DIM = 128
GRID_W = 64
WIN_ROWS = 8
WIN_COLS = 16
REACH = WIN_ROWS // 2
EPS = 1e-06
LOG2E = math.log2(math.e)
BLANK = 2 * WIN_ROWS
TABLES = BLANK + 1
F32 = jnp.float32
BF16 = jnp.bfloat16
MIB = 1 << 20

VM = pl.BlockSpec(memory_space=pltpu.VMEM)
SM = pl.BlockSpec(memory_space=pltpu.SMEM)


def params(mib):
    return pltpu.CompilerParams(vmem_limit_bytes=mib * MIB)


def cost(flops, nbytes, exps=0):
    return pl.CostEstimate(flops=int(flops), bytes_accessed=int(nbytes), transcendentals=int(exps))


def mod_kernel(cond_ref, shift_ref, scale_ref, gate_ref, out_ref):
    cond = cond_ref[...].astype(F32)
    lifted = cond / (1.0 + jnp.exp(-cond))
    lifted = jnp.broadcast_to(lifted.reshape(1, -1), (16, cond.shape[0])).astype(BF16)
    width = shift_ref.shape[1]
    for i, ref in enumerate((shift_ref, scale_ref, gate_ref)):
        part = jnp.dot(lifted, ref[...], preferred_element_type=F32)
        out_ref[:, i * width : (i + 1) * width] = part[:1]


def mod_part(cond, mod_shift, mod_scale, mod_gate):
    rows, width = mod_shift.shape
    return pl.pallas_call(
        mod_kernel,
        out_shape=jax.ShapeDtypeStruct((1, 3 * width), F32),
        in_specs=[VM] * 4,
        out_specs=VM,
        name="mod_part",
        compiler_params=params(8),
        cost_estimate=cost(96 * rows * width, 6 * rows * width),
    )(cond, mod_shift, mod_scale, mod_gate)


def place_kernel(masks, where_ref, *refs):
    pieces, out_ref = refs[:-1], refs[-1]
    width = pieces[0].shape[1] // 3
    for mask, piece in zip(masks, pieces):
        for j in range(3):
            spot = (where_ref[1] ^ mask) + j * len(masks)
            spot = pl.multiple_of(spot * width, width)
            out_ref[:, pl.ds(spot, width)] = piece[:, j * width : (j + 1) * width]


def small_call(kernel, outs, where, *args):
    return pl.pallas_call(
        kernel,
        out_shape=outs,
        in_specs=[SM] + [VM] * len(args),
        out_specs=jax.tree.map(lambda _: VM, outs),
        compiler_params=params(8),
        cost_estimate=cost(1 << 20, 1 << 16),
    )(where, *args)


def place_mods(pieces, masks, where):
    outs = jax.ShapeDtypeStruct((1, len(pieces) * pieces[0].shape[1]), F32)
    return small_call(functools.partial(place_kernel, masks), outs, where, *pieces)


def add_kernel(where_ref, a_ref, b_ref, out_ref):
    out_ref[...] = a_ref[...] + b_ref[...]


def add(a, b, where):
    return small_call(add_kernel, jax.ShapeDtypeStruct(a.shape, a.dtype), where, a, b)


def join_kernel(where_ref, a_ref, b_ref, out_ref):
    out_ref[: a_ref.shape[0], :] = a_ref[...]
    out_ref[a_ref.shape[0] :, :] = b_ref[...]


def join(a, b, where):
    outs = jax.ShapeDtypeStruct((a.shape[0] + b.shape[0], a.shape[1]), a.dtype)
    return small_call(join_kernel, outs, where, a, b)


def pick_kernel(where_ref, inner_ref, outer_ref, send_ref, keep_ref):
    mine = (where_ref[1] & 1) + (where_ref[1] >> 1) == 1

    @pl.when(mine)
    def _():
        send_ref[...] = outer_ref[...]
        keep_ref[...] = inner_ref[...]

    @pl.when(~mine)
    def _():
        send_ref[...] = inner_ref[...]
        keep_ref[...] = outer_ref[...]


def pick(inner, outer, where):
    outs = jax.ShapeDtypeStruct(inner.shape, inner.dtype)
    return small_call(pick_kernel, (outs, outs), where, inner, outer)


def cut_kernel(where_ref, x_ref, *outs):
    count = x_ref.shape[0]
    size = outs[0].shape[0]
    for j, out_ref in enumerate(outs):
        at = jnp.where((where_ref[1] & 1) == 0, j * size, count - (j + 1) * size)
        out_ref[...] = x_ref[pl.ds(pl.multiple_of(at, GRID_W), size), :]


def cut_chunks(x, count, where):
    outs = jax.ShapeDtypeStruct((x.shape[0] // count, x.shape[1]), x.dtype)
    return small_call(cut_kernel, (outs,) * count, where, x)


def table_kernel(bias_ref, out_ref):
    heads = out_ref.shape[0]
    column = lax.broadcasted_iota(jnp.int32, (GRID_W, 2 * GRID_W), 0)
    lane = lax.broadcasted_iota(jnp.int32, (GRID_W, 2 * GRID_W), 1)
    left = lane < GRID_W
    begin = jnp.clip(column - WIN_COLS // 2, 0, GRID_W - WIN_COLS)
    key = jnp.where(left, lane, lane - GRID_W)
    valid = (key >= begin) & (key < begin + WIN_COLS)
    empty = jnp.full((GRID_W, 2 * GRID_W), -1e30, F32)
    for h in range(heads):
        rolled = []
        for d in range(2 * WIN_ROWS - 1):
            row = jnp.broadcast_to(bias_ref[h, d : d + 1, :] * LOG2E, (GRID_W, 2 * GRID_W))
            lo = pltpu.roll(row, 2 * GRID_W - WIN_COLS + 1, 1, stride=1, stride_axis=0)
            hi = pltpu.roll(row, GRID_W - WIN_COLS + 1, 1, stride=1, stride_axis=0)
            rolled.append((jnp.where(valid & left, lo, empty), jnp.where(valid & ~left, hi, empty)))
        for d in range(2 * WIN_ROWS - 2):
            out_ref[h, d] = jnp.where(left, rolled[d][0], rolled[d + 1][1])
        out_ref[h, 2 * WIN_ROWS - 2] = rolled[WIN_ROWS + 2][0]
        out_ref[h, 2 * WIN_ROWS - 1] = rolled[WIN_ROWS - REACH - 1][1]
        out_ref[h, BLANK] = empty


def bias_tables(offset_bias):
    heads, rows, cols = offset_bias.shape
    padded = jnp.pad(offset_bias, ((0, 0), (0, 16 - rows), (0, 2 * GRID_W - cols)))
    return pl.pallas_call(
        table_kernel,
        out_shape=jax.ShapeDtypeStruct((heads, TABLES, GRID_W, 2 * GRID_W), F32),
        in_specs=[VM],
        out_specs=VM,
        name="bias_tables",
        compiler_params=params(8),
        cost_estimate=cost(1 << 22, heads * TABLES * GRID_W * 2 * GRID_W * 4),
    )(padded)


def normed_heads(values, gain, heads):
    parts = []
    for h in range(heads):
        part = values[:, h * HEAD_DIM : (h + 1) * HEAD_DIM]
        square = jnp.mean(part * part, axis=-1, keepdims=True)
        parts.append((part * lax.rsqrt(square + EPS) * gain).astype(BF16))
    return jnp.concatenate(parts, axis=1)


def qkv_kernel(count, heads, tile, take, carried, *refs):
    where_ref, pieces = refs[0], refs[1 : 1 + count]
    refs = refs[1 + count :]
    had, refs = refs[:carried], refs[carried:]
    ma_ref, mb_ref, ng_ref, wq_ref, wk_ref, wv_ref, qg_ref, kg_ref, q_ref, kv_ref = refs[:10]
    edge_ref = refs[10] if take else None
    raw, normed, affine = refs[-3:]
    width = heads * HEAD_DIM
    depth = ng_ref.shape[1]
    strip = 16
    affine[0:1, :] = ma_ref[:, :depth] + mb_ref[:, :depth]
    affine[1:2, :] = ng_ref[...] * (1.0 + (ma_ref[:, depth : 2 * depth] + mb_ref[:, depth : 2 * depth]))
    base = 0
    for piece in pieces:
        raw[base : base + piece.shape[0], :] = piece[...]
        base += piece.shape[0]
    tiles = base // tile
    step = min(width, 2 * HEAD_DIM)
    steps = [(w, at) for w in range(3) for at in range(0, width, step)]
    strips = tile // strip

    def norm_strip(source, slot, j):
        floats = raw[pl.ds(pl.multiple_of(source + j * strip, strip), strip), :].astype(F32)
        inverse = lax.rsqrt(jnp.mean(floats * floats, axis=-1, keepdims=True) + EPS)
        normed[slot, j * strip : (j + 1) * strip, :] = (
            floats * inverse * affine[1:2, :] + affine[0:1, :]
        ).astype(BF16)

    for j in range(strips):
        norm_strip(0, 0, j)

    def store(rows, w, at, values):
        cols = slice(at, at + step)
        if w == 0:
            q_ref[rows, cols] = normed_heads(values, qg_ref[...], step // HEAD_DIM)
        elif w == 1:
            kv_ref[rows, cols] = normed_heads(values, kg_ref[...], step // HEAD_DIM)
        else:
            kv_ref[rows, width + at : width + at + step] = values.astype(BF16)

    def project(i, _, last=False):
        slot = lax.rem(i, 2)
        rows = pl.ds(pl.multiple_of(i * tile, tile), tile)
        held = None
        done = 0
        for n, (w, at) in enumerate(steps):
            ref = (wq_ref, wk_ref, wv_ref)[w]
            values = jnp.dot(
                normed[slot], ref[:, at : at + step], preferred_element_type=F32
            )
            if held is not None:
                store(rows, *held)
            upto = strips * (n + 1) // len(steps)
            while done < upto and not last:
                norm_strip((i + 1) * tile, 1 - slot, done)
                done += 1
            held = (w, at, values)
        store(rows, *held)
        return 0

    lax.fori_loop(0, tiles - 1, project, 0)
    project(tiles - 1, 0, True)
    if take:
        at = 0
        for ref in had:
            edge_ref[: ref.shape[0], :] = ref[...]
            at = ref.shape[0]
        size = edge_ref.shape[0] - at
        start = pl.multiple_of(take(where_ref[0], where_ref[1]), GRID_W)
        edge_ref[at:, :] = kv_ref[pl.ds(start, size), :]


def qkv(
    where,
    pieces,
    mods,
    norm_gain,
    w_query,
    w_key,
    w_value,
    query_gain,
    key_gain,
    heads,
    take=None,
    taken=0,
    had=(),
):
    total = sum(p.shape[0] for p in pieces)
    depth, width = w_query.shape
    tile = 256 if total % 256 == 0 else 128
    outs = [
        jax.ShapeDtypeStruct((total, width), BF16),
        jax.ShapeDtypeStruct((total, 2 * width), BF16),
    ]
    if take:
        outs.append(jax.ShapeDtypeStruct((taken, 2 * width), BF16))
    return pl.pallas_call(
        functools.partial(qkv_kernel, len(pieces), heads, tile, take, len(had)),
        out_shape=tuple(outs),
        in_specs=[SM] + [VM] * (len(pieces) + len(had) + 8),
        out_specs=tuple(VM for _ in outs),
        scratch_shapes=[
            pltpu.VMEM((total, depth), BF16),
            pltpu.VMEM((2, tile, depth), BF16),
            pltpu.VMEM((2, depth), F32),
        ],
        name="qkv",
        compiler_params=params(24),
        cost_estimate=cost(6 * total * depth * width, total * depth * 2 + 6 * depth * width),
    )(
        where,
        *pieces,
        *had,
        *mods,
        norm_gain.reshape(1, -1),
        w_query,
        w_key,
        w_value,
        query_gain.reshape(1, -1),
        key_gain.reshape(1, -1),
    )


def context_kernel(heads, x_ref, gain_ref, wk_ref, wv_ref, kg_ref, kv_ref):
    width = heads * HEAD_DIM
    floats = x_ref[...].astype(F32)
    inverse = lax.rsqrt(jnp.mean(floats * floats, axis=-1, keepdims=True) + EPS)
    x = (floats * inverse * gain_ref[...]).astype(BF16)
    kv_ref[:, :width] = normed_heads(
        jnp.dot(x, wk_ref[...], preferred_element_type=F32), kg_ref[...], heads
    )
    kv_ref[:, width:] = jnp.dot(x, wv_ref[...], preferred_element_type=F32).astype(BF16)


def context_kv(context, norm_gain, w_key, w_value, key_gain, heads):
    count, depth = context.shape
    width = w_key.shape[1]
    return pl.pallas_call(
        functools.partial(context_kernel, heads),
        out_shape=jax.ShapeDtypeStruct((count, 2 * width), BF16),
        in_specs=[VM] * 5,
        out_specs=VM,
        name="context_kv",
        compiler_params=params(16),
        cost_estimate=cost(4 * count * depth * width, 4 * depth * width),
    )(context, norm_gain.reshape(1, -1), w_key, w_value, key_gain.reshape(1, -1))


def attend_kernel(
    heads, span, groups, q_spec, kv_spec, n_ctx, rows_of, total, where_ref, cbias_ref, *refs
):
    n_q, n_kv = q_spec[-1][0] + 1, kv_spec[-1][0] + 1
    q_refs, refs = refs[:n_q], refs[n_q:]
    kv_refs, refs = refs[:n_kv], refs[n_kv:]
    ctx_refs, refs = refs[:n_ctx], refs[n_ctx:]
    tab_ref, out_ref, keys, queries, context, scores, weights = refs
    width = heads * HEAD_DIM
    block = span * GRID_W
    key_rows = span + WIN_ROWS
    window = key_rows * GRID_W
    ctx_count = context.shape[0]
    factor = LOG2E * HEAD_DIM**-0.5
    lines = 2 * GRID_W
    first, rows_at = rows_of(where_ref[0], where_ref[1])
    base = 0
    for i, (j, at, size) in enumerate(q_spec):
        to = pl.multiple_of(rows_at[base + i] * GRID_W, GRID_W)
        queries[pl.ds(to, size), :] = q_refs[j][at : at + size, :]
    base += len(q_spec)
    for i, (j, at, size) in enumerate(kv_spec):
        to = pl.multiple_of((rows_at[base + i] + REACH) * GRID_W, GRID_W)
        keys[pl.ds(to, size), :] = kv_refs[j][at : at + size, :]
    base += len(kv_spec)
    at = 0
    for ref in ctx_refs:
        context[at : at + ref.shape[0], :] = ref[...]
        at += ref.shape[0]
    nt = (((1,), (1,)), ((), ()))

    def group(i, _):
        row = rows_at[base] + i * span
        q_at = pl.multiple_of(row * GRID_W, GRID_W)
        top = first + row
        start = jnp.clip(top - REACH, 0, total - key_rows)
        k_at = pl.multiple_of((start - first + REACH) * GRID_W, GRID_W)
        spots = []
        for r in range(span):
            g = top + r
            a = jnp.clip(g - REACH, 0, total - WIN_ROWS)
            for p in range(key_rows // 2):
                u = start + 2 * p
                lv = (u >= a) & (u < a + WIN_ROWS)
                rv = (u + 1 >= a) & (u + 1 < a + WIN_ROWS)
                both = jnp.where(rv, u - g + WIN_ROWS - 1, BLANK - 2)
                spots.append(jnp.where(lv, both, jnp.where(rv, BLANK - 1, BLANK)))

        def score(h):
            hk = slice(h * HEAD_DIM, (h + 1) * HEAD_DIM)
            q = queries[pl.ds(q_at, block), hk]
            scores[h % 2, :, :window] = lax.dot_general(
                q, keys[pl.ds(k_at, window), hk], nt, preferred_element_type=F32
            )
            scores[h % 2, :, window:] = lax.dot_general(
                q, context[:, hk], nt, preferred_element_type=F32
            )

        def soften(h):
            cbias = cbias_ref[h] * LOG2E
            sums = []
            for r in range(span):
                rows = slice(r * GRID_W, (r + 1) * GRID_W)
                tops = None
                for p in range(key_rows // 2):
                    cols = slice(p * lines, (p + 1) * lines)
                    tile = scores[h % 2, rows, cols] * factor
                    tile = tile + tab_ref[h, spots[r * (key_rows // 2) + p]]
                    scores[h % 2, rows, cols] = tile
                    tops = tile if tops is None else jnp.maximum(tops, tile)
                ctx = scores[h % 2, rows, window : window + lines]
                for p in range(1, ctx_count // lines):
                    cols = slice(window + p * lines, window + (p + 1) * lines)
                    ctx = jnp.maximum(ctx, scores[h % 2, rows, cols])
                tops = jnp.maximum(tops, ctx * factor + cbias)
                high = jnp.max(tops, axis=1, keepdims=True)
                acc = None
                for p in range(key_rows // 2 + ctx_count // lines):
                    cols = slice(p * lines, (p + 1) * lines)
                    tile = scores[h % 2, rows, cols]
                    if p < key_rows // 2:
                        tile = jnp.exp2(tile - high)
                    else:
                        tile = jnp.exp2(tile * factor - (high - cbias))
                    acc = tile if acc is None else acc + tile
                    weights[h % 2, rows, cols] = tile.astype(BF16)
                sums.append(jnp.sum(acc, axis=1, keepdims=True))
            return sums

        def combine(h, sums):
            hk = slice(h * HEAD_DIM, (h + 1) * HEAD_DIM)
            hv = slice(width + h * HEAD_DIM, width + (h + 1) * HEAD_DIM)
            out = jnp.dot(
                weights[h % 2, :, :window], keys[pl.ds(k_at, window), hv], preferred_element_type=F32
            )
            out = out + jnp.dot(
                weights[h % 2, :, window:], context[:, hv], preferred_element_type=F32
            )
            out = (out / jnp.concatenate(sums, axis=0)).astype(BF16)
            out_ref[pl.ds(i * block if groups == 1 else pl.multiple_of(i * block, block), block), hk] = out

        score(0)
        held = None
        for h in range(heads):
            if h + 1 < heads:
                score(h + 1)
            sums = soften(h)
            if held is not None:
                combine(*held)
            held = (h, sums)
        combine(*held)
        return 0

    if groups == 1:
        group(0, 0)
    else:
        lax.fori_loop(0, groups, group, 0)


def attend(
    where, queries, q_spec, kvs, kv_spec, ctx, tables, context_bias, rows_of, total, span, groups, rows
):
    heads = tables.shape[0]
    width = heads * HEAD_DIM
    block = span * GRID_W
    ctx_count = sum(c.shape[0] for c in ctx)
    keys = (span + WIN_ROWS) * GRID_W + ctx_count
    elements = groups * block * heads * keys
    return pl.pallas_call(
        functools.partial(
            attend_kernel, heads, span, groups, q_spec, kv_spec, len(ctx), rows_of, total
        ),
        out_shape=jax.ShapeDtypeStruct((groups * block, width), BF16),
        in_specs=[SM, SM] + [VM] * (len(queries) + len(kvs) + len(ctx) + 1),
        out_specs=VM,
        scratch_shapes=[
            pltpu.VMEM(((rows + 2 * REACH) * GRID_W, 2 * width), BF16),
            pltpu.VMEM((rows * GRID_W, width), BF16),
            pltpu.VMEM((ctx_count, 2 * width), BF16),
            pltpu.VMEM((2, block, keys), F32),
            pltpu.VMEM((2, block, keys), BF16),
        ],
        name="attend",
        compiler_params=params(28),
        cost_estimate=cost(8 * elements * HEAD_DIM, 8 << 20, elements),
    )(where, context_bias, *queries, *kvs, *ctx, tables)


def out_kernel(masks, tile, final, where_ref, *refs):
    count = len(masks)
    pieces, refs = refs[:count], refs[count:]
    w_ref = refs[0]
    before = refs[1:-1]
    out_ref = refs[-1]
    depth = pieces[0].shape[1]
    width = w_ref.shape[1]

    def one(i, _):
        cols = pl.ds(pl.multiple_of(i * tile, tile), tile)
        total = None
        for j, piece in enumerate(pieces):
            rows = pl.ds(pl.multiple_of(masks[j](where_ref[1]) * depth, depth), depth)
            part = jnp.dot(piece[...], w_ref[rows, cols], preferred_element_type=F32)
            total = part if total is None else total + part
        if final:
            resid_ref, ma_ref, mb_ref = before[:3]
            for ref in before[3:]:
                total = total + ref[:, cols]
            spot = pl.ds(pl.multiple_of(2 * width + i * tile, tile), tile)
            gate = ma_ref[:, spot] + mb_ref[:, spot]
            out_ref[:, cols] = (resid_ref[:, cols].astype(F32) + gate * total).astype(BF16)
        else:
            out_ref[:, cols] = total
        return 0

    lax.fori_loop(0, width // tile, one, 0, unroll=2)


def out_project(where, pieces, masks, w_out, before=(), final=True):
    count, width = pieces[0].shape[0], w_out.shape[1]
    depth = sum(p.shape[1] for p in pieces)
    return pl.pallas_call(
        functools.partial(out_kernel, masks, 256, final),
        out_shape=jax.ShapeDtypeStruct((count, width), BF16 if final else F32),
        in_specs=[SM] + [VM] * (len(pieces) + 1 + len(before)),
        out_specs=VM,
        name="out_project",
        compiler_params=params(16),
        cost_estimate=cost(2 * count * width * depth, 2 * depth * width + 8 * count * width),
    )(where, *pieces, w_out, *before)


def swap(count, bit):
    return [(i, i ^ bit) for i in range(count)]


def tie(value, other):
    return lax.optimization_barrier((value, other))[0]


def plain(where, resid, mods, norm_gain, ctx, tables, weights, gains, context_bias, w_out, heads):
    sp, tp = lax.axis_size("sp"), lax.axis_size("tp")
    own = resid.shape[0]
    tokens = own * tp
    rows = tokens // GRID_W
    piece = lax.all_gather(resid, "tp", axis=0, tiled=True)
    q, kv = qkv(where, [piece], mods, norm_gain, *weights, *gains, heads)
    edge = REACH * GRID_W
    above = lax.ppermute(kv[tokens - edge :], "sp", [(i, i + 1) for i in range(sp - 1)])
    below = lax.ppermute(kv[:edge], "sp", [(i + 1, i) for i in range(sp - 1)])
    span = 4 if rows % 4 == 0 else 2
    attended = attend(
        where,
        [q],
        [(0, 0, tokens)],
        [kv, above, below],
        [(0, 0, tokens), (1, 0, edge), (2, 0, edge)],
        ctx,
        tables,
        context_bias,
        lambda s, t: (s * rows, [0, 0, -REACH, rows, 0]),
        sp * rows,
        span,
        rows // span,
        rows,
    )
    full = lax.all_to_all(attended.reshape(tp, own, -1), "tp", split_axis=0, concat_axis=0)
    masks = [lambda t, i=i: jnp.int32(i) for i in range(tp)]
    return out_project(where, [full[i] for i in range(tp)], masks, w_out, (resid, *mods))


CHUNKS = 3


def chunk_row(source, j, block_rows, chunk_rows):
    return source * block_rows + jnp.where(
        (source & 1) == 0, j * chunk_rows, block_rows - (j + 1) * chunk_rows
    )


def staged_tokens(where, resid):
    across = []
    for chunk in cut_chunks(resid, CHUNKS, where):
        across.append(lax.ppermute(chunk, "tp", swap(4, 2)))
    partner = lax.ppermute(resid, "tp", swap(4, 1))
    return partner, across


def staged(
    where, resid, mods, norm_gain, staged_in, ctx, tables, weights, gains, context_bias, w_out, heads
):
    sp, tp = lax.axis_size("sp"), lax.axis_size("tp")
    own = resid.shape[0]
    block_rows = own // GRID_W
    chunk_rows = block_rows // CHUNKS
    chunk = chunk_rows * GRID_W
    rows = block_rows * tp
    edge = REACH * GRID_W
    partner, across = staged_in
    project = functools.partial(
        qkv,
        where,
        mods=mods,
        norm_gain=norm_gain,
        w_query=weights[0],
        w_key=weights[1],
        w_value=weights[2],
        query_gain=gains[0],
        key_gain=gains[1],
        heads=heads,
    )

    def near_rows(t):
        return [t * block_rows, (t ^ 1) * block_rows]

    def chunk_rows_of(t, j):
        return [chunk_row(t ^ mask, j, block_rows, chunk_rows) for mask in (2, 3)]

    def early_at(s, t):
        chip, parity = t >> 1, t & 1
        return jnp.where(chip == parity, 0, own) + jnp.where(chip == 0, 0, own - edge)

    def late_at(s, t):
        return jnp.where((t >> 1) + (t & 1) == 1, 0, chunk)

    down = [(s * tp + t, (s - 1) * tp + t) for s in range(1, sp) for t in range(tp)]
    up = [(s * tp + t, (s + 1) * tp + t) for s in range(sp - 1) for t in range(tp)]
    early = [p for p in down if p[0] % tp < 2] + [p for p in up if p[0] % tp >= 2]
    late = [p for p in up if p[0] % tp < 2] + [p for p in down if p[0] % tp >= 2]

    q0, kv0, edge_kv = project([resid, partner], take=early_at, taken=edge)
    early_kv = lax.ppermute(edge_kv, ("sp", "tp"), early)
    beside0 = lax.ppermute(across[0], "tp", swap(4, 1))
    beside1 = lax.ppermute(tie(across[1], kv0), "tp", swap(4, 1))
    q1, kv1, edge_kv = project(list(tie((across[0], beside0), kv0)), take=late_at, taken=chunk)
    q2, kv2, edge_kv = project(
        list(tie((across[1], beside1), kv1)), take=late_at, taken=2 * chunk, had=(edge_kv,)
    )
    late_kv = lax.ppermute(edge_kv, ("sp", "tp"), late)

    near = [(0, 0, own), (0, own, own)]
    pair = [(0, chunk), (chunk, chunk)]
    kv_spec = near + [(j, at, size) for j in (1, 2, 3) for at, size in pair]

    def block(queries, q_spec, kvs, kv_spec, rows_of):
        return attend(
            where,
            queries,
            q_spec,
            kvs,
            kv_spec,
            ctx,
            tables,
            context_bias,
            rows_of,
            sp * rows,
            block_rows,
            1,
            rows,
        )

    def home_rows(last, late):
        def rows_of(s, t):
            chip = t >> 1
            at = near_rows(t) + near_rows(t) + chunk_rows_of(t, 0) + chunk_rows_of(t, 1)
            if late:
                for j in range(2):
                    at.append(jnp.where(chip == 0, -(j + 1) * chunk_rows, rows + j * chunk_rows))
            return s * rows, at + [last(chip) * block_rows]

        return rows_of

    inner = block([q0], near, [kv0, kv1, kv2], kv_spec[:6], home_rows(lambda chip: 1 + chip, False))

    beside2 = lax.ppermute(tie(across[2], inner), "tp", swap(4, 1))
    q3, kv3 = project(list(tie((across[2], beside2), inner)))

    def far(mask, after):
        def rows_of(s, t):
            chunks = [row for j in range(CHUNKS) for row in chunk_rows_of(t, j)]
            outside = jnp.where(t < 2, rows, -REACH)
            return s * rows, chunks + near_rows(t) + chunks + [outside, (t ^ mask) * block_rows]

        return block(
            [tie(q1, after), q2, q3],
            [(j - 1, at, size) for j, at, size in kv_spec[2:]],
            [kv0, kv1, kv2, kv3, early_kv],
            kv_spec + [(4, 0, edge)],
            rows_of,
        )

    away2 = far(2, kv3)
    from_2 = lax.ppermute(away2, "tp", swap(4, 2))
    away3 = far(3, away2)
    from_3 = lax.ppermute(away3, "tp", swap(4, 3))

    outer = block(
        [tie(q0, away3)],
        near,
        [kv0, kv1, kv2, late_kv],
        kv_spec[:6] + [(3, at, size) for at, size in pair],
        home_rows(lambda chip: 3 * chip, True),
    )
    send, keep = pick(inner, outer, where)
    from_1 = lax.ppermute(send, "tp", swap(4, 1))
    masks = [lambda t, i=i: t ^ i for i in range(4)]
    partial = out_project(where, [keep, from_1, from_2], masks[:3], w_out, final=False)
    return out_project(where, [from_3], masks[3:], w_out, (resid, *mods, partial))


def shards(
    resid,
    cond,
    mod_shift,
    mod_scale,
    mod_gate,
    norm_gain,
    context,
    w_query,
    w_key,
    w_value,
    query_gain,
    key_gain,
    offset_bias,
    context_bias,
    w_out,
):
    heads = offset_bias.shape[0]
    sp, tp = lax.axis_size("sp"), lax.axis_size("tp")
    block_rows = resid.shape[0] // GRID_W
    split = tp == 4 and sp > 1 and block_rows == CHUNKS * REACH // 2
    where = jnp.stack([lax.axis_index("sp"), lax.axis_index("tp")]).astype(jnp.int32)

    tables = bias_tables(offset_bias)
    parts = [mod_part(cond, mod_shift, mod_scale, mod_gate)]
    masks = [0]
    bit = tp // 2
    while bit:
        parts += [lax.ppermute(p, "tp", swap(tp, bit)) for p in parts]
        masks += [v ^ bit for v in masks]
        bit //= 2
    run = plain
    if split:
        run = functools.partial(staged, staged_in=staged_tokens(where, resid))
    mods = place_mods(tie(parts, tables), masks, where)
    bit = 1
    while bit < sp:
        other = lax.ppermute(mods, "sp", swap(sp, bit))
        bit *= 2
        if bit < sp:
            mods = add(mods, other, where)

    ctx = context_kv(context, norm_gain, w_key, w_value, key_gain, heads)
    bit = sp // 2
    while bit:
        got = lax.ppermute(ctx, "sp", swap(sp, bit))
        bit //= 2
        if bit:
            ctx = join(ctx, got, where)
    return run(
        where,
        resid,
        (mods, other),
        norm_gain,
        ctx=[ctx, got],
        tables=tables,
        weights=(w_query, w_key, w_value),
        gains=(query_gain, key_gain),
        context_bias=context_bias,
        w_out=w_out,
        heads=heads,
    )


def solution(mesh):
    in_specs = (
        P(("sp", "tp"), None),
        P("sp"),
        P("sp", "tp"),
        P("sp", "tp"),
        P("sp", "tp"),
        P(),
        P("sp", None),
        P(None, "tp"),
        P(None, "tp"),
        P(None, "tp"),
        P(),
        P(),
        P("tp", None, None),
        P("tp"),
        P(),
    )
    out_specs = P(("sp", "tp"), None)
    return jax.shard_map(shards, mesh=mesh, in_specs=in_specs, out_specs=out_specs, check_vma=False)
```

time: 179 us -> 129 us (0.72)
  blocking collectives: 22.8 us -> 0 us
  waiting for transfers between devices: 55.6 us -> 33.8 us
  starting transfers between devices: 16 us -> 36.2 us
  local copies, waits for them, and re-layouts: 20.8 us -> 6.98 us
  between operations: 13.7 us -> 0.33 us
    all_gather x2 -> x0, waiting for transfers between devices: 45.6 us -> none  [the longest x1 24 us: shards(): piece = lax.all_gather(resid, 'tp', axis=0, tiled=True)]
    ppermute x5 -> x18, waiting for transfers between devices: 6.51 us -> 30.6 us  [the longest x1 9.92 us: staged(): from_2 = lax.ppermute(away2, 'tp', swap(4, 2))]
    all_to_all x1 -> x0, blocking collectives: 22.8 us -> none  [shards(): lax.all_to_all(attended.reshape(tp, own, -1), 'tp', split_axis=0, concat_...]
    ppermute x5 -> x18, starting transfers between devices: 13 us -> 35.6 us  [the longest x1 11.1 us: staged(): from_2 = lax.ppermute(away2, 'tp', swap(4, 2))]
    unnamed x49 -> x43, local copies, waits for them, and re-layouts: 19.5 us -> 6.97 us
    ppermute x3, starting transfers between devices: 3.04 us -> 0.58 us  [shards(): parts += [lax.ppermute(p, 'tp', swap(tp, bit)) for p in parts]]
    pallas_call x4 -> x17, Pallas kernels: 46.4 us -> 48.6 us  [the longest x4 21 us: attend(): pl.pallas_call(functools.partial(attend_kernel, heads, span, groups, q_sp...]
  transfers between devices with their start and end apart: 10 -> 21, of which waited for: 8 -> 10; matrix products, arithmetic and copies ran while one was open for 1% -> 0% of each run, Pallas kernels for 13% -> 32%
where the time goes in v3:
time: 129 us; the launch traced here: 128 us
  Pallas kernels  50.7 us (39%)
  starting transfers between devices  36.2 us (28%)
  waiting for transfers between devices  33.8 us (26%)
  local copies, waits for them, and re-layouts  6.98 us (5%)
    pallas_call x4, Pallas kernels, attend(): pl.pallas_call(functools.partial(attend_kernel, heads, span, groups, q_sp...  21 us
    pallas_call x4, Pallas kernels, qkv(): pl.pallas_call(functools.partial(qkv_kernel, len(pieces), heads, tile, ta...  16.4 us
    ppermute x1, starting transfers between devices, staged(): from_2 = lax.ppermute(away2, 'tp', swap(4, 2))  11.1 us
    ppermute x1, waiting for transfers between devices, staged(): from_2 = lax.ppermute(away2, 'tp', swap(4, 2))  9.92 us
    ppermute x1, waiting for transfers between devices, staged(): early_kv = lax.ppermute(edge_kv, ('sp', 'tp'), early)  7.36 us
    pallas_call x2, Pallas kernels, out_project(): pl.pallas_call(functools.partial(out_kernel, masks, 256, final), out_shap...  7.2 us
    unnamed x43, local copies, waits for them, and re-layouts  6.97 us
    ppermute x3, starting transfers between devices, shards(): got = lax.ppermute(ctx, 'sp', swap(sp, bit))  5.9 us
  transfers between devices with their start and end apart: 21, of which 10 were waited for; matrix products, arithmetic and copies ran while one was open for 0% of the time, Pallas kernels for 32%

profile of v3, /device:TPU:0, one launch (start us, length us, event | category | flops | bytes accessed | tf_op | source)
XLA Modules:
  0.0 128.1 jit_solution(9695415036788892508)
XLA Ops:
  0.6 1.4 %copy-done.5 = bf16[384,2048]{1,0:T(8,128)(2,1)S(1)} copy-done((bf16[384,2048]{1,0:T(8,128)(2,1)S(1)}, bf16[384,2048]{1,0:T(8,128)(2,1)}, u32[]{:S(2)}) %copy-start.5) | copy-done | bytes 1572888
  2.6 2.5 %collective-permute-start = (bf16[128,2048]{1,0:T(8,128)(2,1)S(1)}, bf16[128,2048]{1,0:T(8,128)(2,1)S(1)}, u32[]{:S(2)}, u32[]{:S(2)}) collective-permute-start(bf16[128,2048]{1,0:T(8,128)(2,1)S(1)} %get-tuple-element.36), channel_id=1, source_target_pairs={{0,2},{1,3},{2,0},{3,1},{4,6},{5,7},{6,4},{7,5},{8,10},{9,11},{10,... | collective-permute-start | bytes 1572872 | tf_op jit(solution)/shard_map/ppermute | solution.py:573
  5.2 1.6 %copy-done = bf16[2048,512]{1,0:T(8,128)(2,1)S(1)} copy-done((bf16[2048,512]{1,0:T(8,128)(2,1)S(1)}, bf16[2048,512]{1,0:T(8,128)(2,1)}, u32[]{:S(2)}) %copy-start) | copy-done | bytes 2097176
  6.8 1.6 %copy-done.2 = bf16[2048,512]{1,0:T(8,128)(2,1)S(1)} copy-done((bf16[2048,512]{1,0:T(8,128)(2,1)S(1)}, bf16[2048,512]{1,0:T(8,128)(2,1)}, u32[]{:S(2)}) %copy-start.2) | copy-done | bytes 2097176
  11.7 2.7 %collective-permute-start.12 = (bf16[64,1024]{1,0:T(8,128)(2,1)S(1)}, bf16[64,1024]{1,0:T(8,128)(2,1)S(1)}, u32[]{:S(2)}, u32[]{:S(2)}) collective-permute-start(bf16[64,1024]{1,0:T(8,128)(2,1)S(1)} %context_kv.1.a_ref), channel_id=1, source_target_pairs={{0,16},{4,20},{8,24},{12,28},{16,0},{20,4},{24,8},{28,12},{1,17},{... | collective-permute-start | bytes 393224 | tf_op jit(solution)/shard_map/ppermute | solution.py:745
  15.1 3.1 %collective-permute-done.3.refs_1_ = f32[1,1536]{1,0:T(1,128)S(1)} collective-permute-done((f32[1,1536]{1,0:T(1,128)S(1)}, f32[1,1536]{1,0:T(1,128)S(1)}, u32[]{:S(2)}, u32[]{:S(2)}) %collective-permute-start.3) | collective-permute-done | bytes 6176 | tf_op jit(solution)/shard_map/ppermute | solution.py:728
  18.2 1.0 bias_tables.1.refs_6_.refs_10_.refs_7_
  19.9 1.6 %collective-permute-start.6 = (f32[1,6144]{1,0:T(1,128)S(1)}, f32[1,6144]{1,0:T(1,128)S(1)}, u32[]{:S(2)}, u32[]{:S(2)}) collective-permute-start(f32[1,6144]{1,0:T(1,128)S(1)} %shard_map.146.a_ref), channel_id=1, source_target_pairs={{0,4},{4,0},{8,12},{12,8},{16,20},{20,16},{24,28},{28,24},{1,5},{5... | collective-permute-start | bytes 73736 | tf_op jit(solution)/shard_map/ppermute | solution.py:737
  21.5 1.4 %collective-permute-start.10 = (bf16[128,2048]{1,0:T(8,128)(2,1)S(1)}, bf16[128,2048]{1,0:T(8,128)(2,1)S(1)}, u32[]{:S(2)}, u32[]{:S(2)}) collective-permute-start(bf16[128,2048]{1,0:T(8,128)(2,1)S(1)} %get-tuple-element.48), channel_id=1, source_target_pairs={{0,2},{1,3},{2,0},{3,1},{4,6},{5,7},{6,4},{7,5},{8,10},{9,11},{10,... | collective-permute-start | bytes 1572872 | tf_op jit(solution)/shard_map/ppermute | solution.py:573
  24.4 1.6 %collective-permute-start.7 = (f32[1,6144]{1,0:T(1,128)S(1)}, f32[1,6144]{1,0:T(1,128)S(1)}, u32[]{:S(2)}, u32[]{:S(2)}) collective-permute-start(f32[1,6144]{1,0:T(1,128)S(1)} %shard_map.147.a_ref), channel_id=1, source_target_pairs={{0,8},{4,12},{8,0},{12,4},{16,24},{20,28},{24,16},{28,20},{1,9},{5... | collective-permute-start | bytes 73736 | tf_op jit(solution)/shard_map/ppermute | solution.py:737
  26.0 2.2 %collective-permute-done.7.b_ref = f32[1,6144]{1,0:T(1,128)S(1)} collective-permute-done((f32[1,6144]{1,0:T(1,128)S(1)}, f32[1,6144]{1,0:T(1,128)S(1)}, u32[]{:S(2)}, u32[]{:S(2)}) %collective-permute-start.7) | collective-permute-done | bytes 24608 | tf_op jit(solution)/shard_map/ppermute | solution.py:737
  28.8 2.6 %collective-permute-start.8 = (f32[1,6144]{1,0:T(1,128)S(1)}, f32[1,6144]{1,0:T(1,128)S(1)}, u32[]{:S(2)}, u32[]{:S(2)}) collective-permute-start(f32[1,6144]{1,0:T(1,128)S(1)} %shard_map.148.refs_3_.refs_4_), channel_id=1, source_target_pairs={{0,16},{4,20},{8,24},{12,28},{16,0},{20,4},{24,8},{28,12},{1,17},{... | collective-permute-start | bytes 73736 | tf_op jit(solution)/shard_map/ppermute | solution.py:737
  32.0 1.6 %collective-permute-start.13 = (bf16[128,1024]{1,0:T(8,128)(2,1)S(1)}, bf16[128,1024]{1,0:T(8,128)(2,1)S(1)}, u32[]{:S(2)}, u32[]{:S(2)}) collective-permute-start(bf16[128,1024]{1,0:T(8,128)(2,1)S(1)} %shard_map.149.a_ref), channel_id=1, source_target_pairs={{0,8},{4,12},{8,0},{12,4},{16,24},{20,28},{24,16},{28,20},{1,9},{5... | collective-permute-start | bytes 786440 | tf_op jit(solution)/shard_map/ppermute | solution.py:745
  33.8 8.1 %qkv.4 = (bf16[768,512]{1,0:T(8,128)(2,1)S(1)}, bf16[768,1024]{1,0:T(8,128)(2,1)S(1)}, bf16[256,1024]{1,0:T(8,128)(2,1)S(1)}) custom-call(s32[2]{0:T(128)S(1)} %pad_add_fusion.where_ref.refs_0_, bf16[384,2048]{1,0:T(8,128)(2,1)S(1)} %copy-done.6, bf16[384,2048]{1,0:T(8,128)(2,1)S(1)} %collective-permute-done.2.refs_2_, ...), custom_call_target="tpu_custom_call" | custom-call | flops 4831838208 | bytes 9437184 | tf_op jit(solution)/shard_map/qkv/pallas_call | solution.py:278
  43.0 1.6 %collective-permute-start.14 = (bf16[256,1024]{1,0:T(8,128)(2,1)S(1)}, bf16[256,1024]{1,0:T(8,128)(2,1)S(1)}, u32[]{:S(2)}, u32[]{:S(2)}) collective-permute-start(bf16[256,1024]{1,0:T(8,128)(2,1)S(1)} %shard_map.150.refs_4_.refs_8_.refs_5_), channel_id=1, source_target_pairs={{0,4},{4,0},{8,12},{12,8},{16,20},{20,16},{24,28},{28,24},{1,5},{5... | collective-permute-start | bytes 1572872 | tf_op jit(solution)/shard_map/ppermute | solution.py:745
  44.6 1.5 %collective-permute-start.9 = (bf16[128,2048]{1,0:T(8,128)(2,1)S(1)}, bf16[128,2048]{1,0:T(8,128)(2,1)S(1)}, u32[]{:S(2)}, u32[]{:S(2)}) collective-permute-start(bf16[128,2048]{1,0:T(8,128)(2,1)S(1)} %get-tuple-element.45), channel_id=1, source_target_pairs={{0,2},{1,3},{2,0},{3,1},{4,6},{5,7},{6,4},{7,5},{8,10},{9,11},{10,... | collective-permute-start | bytes 1572872 | tf_op jit(solution)/shard_map/ppermute | solution.py:573
  46.1 2.8 %qkv.5 = (bf16[256,512]{1,0:T(8,128)(2,1)S(1)}, bf16[256,1024]{1,0:T(8,128)(2,1)S(1)}, bf16[128,1024]{1,0:T(8,128)(2,1)S(1)}) custom-call(s32[2]{0:T(128)S(1)} %pad_add_fusion.where_ref.refs_0_, bf16[128,2048]{1,0:T(8,128)(2,1)S(1)} %collective-permute-done.refs_1_, bf16[128,2048]{1,0:T(8,128)(2,1)S(1)} %collective-permute-done.1.refs_2_, ...), custom_call_target="tpu_custom_call" | custom-call | flops 1610612736 | bytes 7340032 | tf_op jit(solution)/shard_map/qkv/pallas_call | solution.py:278
  48.9 2.8 %qkv.6 = (bf16[256,512]{1,0:T(8,128)(2,1)S(1)}, bf16[256,1024]{1,0:T(8,128)(2,1)S(1)}, bf16[256,1024]{1,0:T(8,128)(2,1)S(1)}) custom-call(s32[2]{0:T(128)S(1)} %pad_add_fusion.where_ref.refs_0_, bf16[128,2048]{1,0:T(8,128)(2,1)S(1)} %collective-permute-done.10.refs_1_, bf16[128,2048]{1,0:T(8,128)(2,1)S(1)} %collective-permute-done.11.refs_2_, ...), custom_call_target="tpu_custom_call" | custom-call | flops 1610612736 | bytes 7340032 | tf_op jit(solution)/shard_map/qkv/pallas_call | solution.py:278
  51.6 5.3 %collective-permute-done.14.refs_5_.refs_9_.refs_6_ = bf16[256,1024]{1,0:T(8,128)(2,1)S(1)} collective-permute-done((bf16[256,1024]{1,0:T(8,128)(2,1)S(1)}, bf16[256,1024]{1,0:T(8,128)(2,1)S(1)}, u32[]{:S(2)}, u32[]{:S(2)}) %collective-permute-start.14) | collective-permute-done | bytes 524320 | tf_op jit(solution)/shard_map/ppermute | solution.py:745
  57.0 5.1 %attend.4.inner_ref = bf16[384,512]{1,0:T(8,128)(2,1)S(1)} custom-call(s32[2]{0:T(128)S(1)} %pad_add_fusion.where_ref.refs_0_, f32[4]{0:T(128)S(1)} %copy-done.17, bf16[768,512]{1,0:T(8,128)(2,1)S(1)} %get-tuple-element.63.refs_0_, bf16[768,1024]{1,0:T(8,128)(2,1)S(1)} %get-tuple-element.41.refs_1_.refs_3_, ...), custom_call_target="tpu_custom_call" | custom-call | flops 2214592512 | bytes 8388608 | tf_op jit(solution)/shard_map/attend/pallas_call | solution.py:458
  62.2 1.3 %collective-permute-start.16 = (bf16[256,1024]{1,0:T(8,128)(2,1)S(1)}, bf16[256,1024]{1,0:T(8,128)(2,1)S(1)}, u32[]{:S(2)}, u32[]{:S(2)}) collective-permute-start(bf16[256,1024]{1,0:T(8,128)(2,1)S(1)} %get-tuple-element.61), channel_id=1, source_target_pairs={{4,0},{5,1},{8,4},{9,5},{12,8},{13,9},{16,12},{17,13},{20,16},{21,... | collective-permute-start | bytes 1572872 | tf_op jit(solution)/shard_map/ppermute | solution.py:621
  63.5 4.8 %collective-permute-start.18 = (bf16[256,1024]{1,0:T(8,128)(2,1)S(1)}, bf16[256,1024]{1,0:T(8,128)(2,1)S(1)}, u32[]{:S(2)}, u32[]{:S(2)}) collective-permute-start(bf16[256,1024]{1,0:T(8,128)(2,1)S(1)} %get-tuple-element.64), channel_id=1, source_target_pairs={{0,4},{1,5},{4,8},{5,9},{8,12},{9,13},{12,16},{13,17},{16,20},{17,... | collective-permute-start | bytes 1572872 | tf_op jit(solution)/shard_map/ppermute | solution.py:628
  68.3 2.7 %qkv.7 = (bf16[256,512]{1,0:T(8,128)(2,1)S(1)}, bf16[256,1024]{1,0:T(8,128)(2,1)S(1)}) custom-call(s32[2]{0:T(128)S(1)} %pad_add_fusion.where_ref.refs_0_, bf16[128,2048]{1,0:T(8,128)(2,1)S(1)} %collective-permute-done.9.refs_1_, bf16[128,2048]{1,0:T(8,128)(2,1)S(1)} %collective-permute-done.15.refs_2_, f32[1,6144]{1,0:T(1,128)S(1)} %shard_map.148.refs_3_.refs_4_, ...), custom_call_target="tpu_custom_call" | custom-call | flops 1610612736 | bytes 7340032 | tf_op jit(solution)/shard_map/qkv/pallas_call | solution.py:278
  71.0 7.4 %collective-permute-done.16.refs_7_ = bf16[256,1024]{1,0:T(8,128)(2,1)S(1)} collective-permute-done((bf16[256,1024]{1,0:T(8,128)(2,1)S(1)}, bf16[256,1024]{1,0:T(8,128)(2,1)S(1)}, u32[]{:S(2)}, u32[]{:S(2)}) %collective-permute-start.16) | collective-permute-done | bytes 524320 | tf_op jit(solution)/shard_map/ppermute | solution.py:621
  78.4 5.2 %attend.5 = bf16[384,512]{1,0:T(8,128)(2,1)S(1)} custom-call(s32[2]{0:T(128)S(1)} %pad_add_fusion.where_ref.refs_0_, f32[4]{0:T(128)S(1)} %copy-done.17, bf16[256,512]{1,0:T(8,128)(2,1)S(1)} %get-tuple-element.62.refs_0_, bf16[256,512]{1,0:T(8,128)(2,1)S(1)} %get-tuple-element.59.refs_1_, bf16[256,512]{1,0:T(8,128)(2,1)S(1)} %get-tuple-element.60.refs_2_, ...), custom_call_target="tpu_custom_call" | custom-call | flops 2214592512 | bytes 8388608 | tf_op jit(solution)/shard_map/attend/pallas_call | solution.py:458
  83.6 5.2 %attend.6 = bf16[384,512]{1,0:T(8,128)(2,1)S(1)} custom-call(s32[2]{0:T(128)S(1)} %pad_add_fusion.where_ref.refs_0_, f32[4]{0:T(128)S(1)} %copy-done.17, bf16[256,512]{1,0:T(8,128)(2,1)S(1)} %get-tuple-element.62.refs_0_, bf16[256,512]{1,0:T(8,128)(2,1)S(1)} %get-tuple-element.59.refs_1_, bf16[256,512]{1,0:T(8,128)(2,1)S(1)} %get-tuple-element.60.refs_2_, ...), custom_call_target="tpu_custom_call" | custom-call | flops 2214592512 | bytes 8388608 | tf_op jit(solution)/shard_map/attend/pallas_call | solution.py:458
  89.5 5.4 %attend.7.outer_ref = bf16[384,512]{1,0:T(8,128)(2,1)S(1)} custom-call(s32[2]{0:T(128)S(1)} %pad_add_fusion.where_ref.refs_0_, f32[4]{0:T(128)S(1)} %copy-done.17, bf16[768,512]{1,0:T(8,128)(2,1)S(1)} %get-tuple-element.63.refs_0_, bf16[768,1024]{1,0:T(8,128)(2,1)S(1)} %get-tuple-element.41.refs_1_.refs_3_, ...), custom_call_target="tpu_custom_call" | custom-call | flops 2214592512 | bytes 8388608 | tf_op jit(solution)/shard_map/attend/pallas_call | solution.py:458
  95.7 11.1 %collective-permute-start.20 = (bf16[384,512]{1,0:T(8,128)(2,1)S(1)}, bf16[384,512]{1,0:T(8,128)(2,1)S(1)}, u32[]{:S(2)}, u32[]{:S(2)}) collective-permute-start(bf16[384,512]{1,0:T(8,128)(2,1)S(1)} %attend.5), channel_id=1, source_target_pairs={{0,2},{1,3},{2,0},{3,1},{4,6},{5,7},{6,4},{7,5},{8,10},{9,11},{10,... | collective-permute-start | bytes 1179656 | tf_op jit(solution)/shard_map/ppermute | solution.py:682
  106.9 9.9 %collective-permute-done.20.refs_2_ = bf16[384,512]{1,0:T(8,128)(2,1)S(1)} collective-permute-done((bf16[384,512]{1,0:T(8,128)(2,1)S(1)}, bf16[384,512]{1,0:T(8,128)(2,1)S(1)}, u32[]{:S(2)}, u32[]{:S(2)}) %collective-permute-start.20) | collective-permute-done | bytes 393248 | tf_op jit(solution)/shard_map/ppermute | solution.py:682
  116.8 3.8 %out_project.2.refs_5_ = f32[384,2048]{1,0:T(8,128)S(1)} custom-call(s32[2]{0:T(128)S(1)} %pad_add_fusion.where_ref.refs_0_, bf16[384,512]{1,0:T(8,128)(2,1)S(1)} %get-tuple-element.65.refs_0_, bf16[384,512]{1,0:T(8,128)(2,1)S(1)} %collective-permute-done.19.refs_1_, bf16[384,512]{1,0:T(8,128)(2,1)S(1)} %collective-permute-done.20.refs_2_, ...), custom_call_target="tpu_custom_call" | custom-call | flops 2415919104 | bytes 12582912 | tf_op jit(solution)/shard_map/out_project/pallas_call | solution.py:511
  120.6 4.1 %collective-permute-done.17.refs_0_ = bf16[384,512]{1,0:T(8,128)(2,1)S(1)} collective-permute-done((bf16[384,512]{1,0:T(8,128)(2,1)S(1)}, bf16[384,512]{1,0:T(8,128)(2,1)S(1)}, u32[]{:S(2)}, u32[]{:S(2)}) %collective-permute-start.17) | collective-permute-done | bytes 393248 | tf_op jit(solution)/shard_map/ppermute | solution.py:684
  124.7 3.4 %out_project.3 = bf16[384,2048]{1,0:T(8,128)(2,1)} custom-call(s32[2]{0:T(128)S(1)} %pad_add_fusion.where_ref.refs_0_, bf16[384,512]{1,0:T(8,128)(2,1)S(1)} %collective-permute-done.17.refs_0_, bf16[2048,2048]{1,0:T(8,128)(2,1)S(1)} %bitcast.6, bf16[384,2048]{1,0:T(8,128)(2,1)S(1)} %copy-done.6, f32[1,6144]{1,0:T(1,128)S(1)} %shard_map.148.refs_3_.refs_4_, ...), custom_call_target="tpu_custom_call" | custom-call | flops 805306368 | bytes 8388608 | tf_op jit(solution)/shard_map/out_project/pallas_call | solution.py:511
  (76 shorter events, 11.2 us)
Async XLA Ops:
  0.0 33.7 %collective-permute-start.2 = (bf16[384,2048]{1,0:T(8,128)(2,1)}, bf16[384,2048]{1,0:T(8,128)(2,1)S(1)}, u32[]{:S(2)}, u32[]{:S(2)}) collective-permute-start(bf16[384,2048]{1,0:T(8,128)(2,1)} %refs_2_.1), channel_id=1, source_target_pairs={{0,1},{1,0},{2,3},{3,2},{4,5},{5,4},{6,7},{7,6},{8,9},{9,8},{10,11... | collective-permute-start | bytes 4718600 | tf_op jit(solution)/shard_map/ppermute | solution.py:574
  2.0 12.4 %copy-start.9 = (bf16[256,512]{1,0:T(8,128)(2,1)S(1)}, bf16[256,512]{1,0:T(8,128)(2,1)}, u32[]{:S(2)}) copy-start(bf16[256,512]{1,0:T(8,128)(2,1)} %scale_ref.1) | copy-start | bytes 786436
  2.0 12.4 %copy-start.10 = (bf16[256,512]{1,0:T(8,128)(2,1)S(1)}, bf16[256,512]{1,0:T(8,128)(2,1)}, u32[]{:S(2)}) copy-start(bf16[256,512]{1,0:T(8,128)(2,1)} %gate_ref.1) | copy-start | bytes 786436
  2.6 31.0 %collective-permute-start = (bf16[128,2048]{1,0:T(8,128)(2,1)S(1)}, bf16[128,2048]{1,0:T(8,128)(2,1)S(1)}, u32[]{:S(2)}, u32[]{:S(2)}) collective-permute-start(bf16[128,2048]{1,0:T(8,128)(2,1)S(1)} %get-tuple-element.36), channel_id=1, source_target_pairs={{0,2},{1,3},{2,0},{3,1},{4,6},{5,7},{6,4},{7,5},{8,10},{9,11},{10,... | collective-permute-start | bytes 1572872 | tf_op jit(solution)/shard_map/ppermute | solution.py:573
  10.7 23.1 %copy-start.3 = (bf16[2048,512]{1,0:T(8,128)(2,1)S(1)}, bf16[2048,512]{1,0:T(8,128)(2,1)}, u32[]{:S(2)}) copy-start(bf16[2048,512]{1,0:T(8,128)(2,1)} %refs_8_.7) | copy-start | bytes 6291460
  10.7 23.1 %copy-start.4 = (bf16[2048,512]{1,0:T(8,128)(2,1)S(1)}, bf16[2048,512]{1,0:T(8,128)(2,1)}, u32[]{:S(2)}) copy-start(bf16[2048,512]{1,0:T(8,128)(2,1)} %refs_6_.5) | copy-start | bytes 6291460
  11.6 22.1 %copy-start.1 = (bf16[2048,512]{1,0:T(8,128)(2,1)S(1)}, bf16[2048,512]{1,0:T(8,128)(2,1)}, u32[]{:S(2)}) copy-start(bf16[2048,512]{1,0:T(8,128)(2,1)} %refs_7_.7) | copy-start | bytes 6291460
  11.6 22.1 %copy-start.6 = (bf16[384,2048]{1,0:T(8,128)(2,1)S(1)}, bf16[384,2048]{1,0:T(8,128)(2,1)}, u32[]{:S(2)}) copy-start(bf16[384,2048]{1,0:T(8,128)(2,1)} %refs_2_.1) | copy-start | bytes 4718596
  11.6 22.1 %copy-start.12 = (f32[2048]{0:T(1024)S(1)}, f32[2048]{0:T(1024)}, u32[]{:S(2)}) copy-start(f32[2048]{0:T(1024)} %param.20) | copy-start | bytes 24580
  11.7 22.1 %copy-start.14 = (f32[128]{0:T(128)S(1)}, f32[128]{0:T(128)}, u32[]{:S(2)}) copy-start(f32[128]{0:T(128)} %param.26) | copy-start | bytes 1540
  11.7 22.1 %copy-start.15 = (f32[128]{0:T(128)S(1)}, f32[128]{0:T(128)}, u32[]{:S(2)}) copy-start(f32[128]{0:T(128)} %param.25) | copy-start | bytes 1540
  11.7 19.8 %collective-permute-start.12 = (bf16[64,1024]{1,0:T(8,128)(2,1)S(1)}, bf16[64,1024]{1,0:T(8,128)(2,1)S(1)}, u32[]{:S(2)}, u32[]{:S(2)}) collective-permute-start(bf16[64,1024]{1,0:T(8,128)(2,1)S(1)} %context_kv.1.a_ref), channel_id=1, source_target_pairs={{0,16},{4,20},{8,24},{12,28},{16,0},{20,4},{24,8},{28,12},{1,17},{... | collective-permute-start | bytes 393224 | tf_op jit(solution)/shard_map/ppermute | solution.py:745
  14.6 3.7 %collective-permute-start.3 = (f32[1,1536]{1,0:T(1,128)S(1)}, f32[1,1536]{1,0:T(1,128)S(1)}, u32[]{:S(2)}, u32[]{:S(2)}) collective-permute-start(f32[1,1536]{1,0:T(1,128)S(1)} %mod_part.1.refs_0_), channel_id=1, source_target_pairs={{0,2},{1,3},{2,0},{3,1},{4,6},{5,7},{6,4},{7,5},{8,10},{9,11},{10,... | collective-permute-start | bytes 18440 | tf_op jit(solution)/shard_map/ppermute | solution.py:728
  15.1 4.1 %collective-permute-start.4 = (f32[1,1536]{1,0:T(1,128)S(1)}, f32[1,1536]{1,0:T(1,128)S(1)}, u32[]{:S(2)}, u32[]{:S(2)}) collective-permute-start(f32[1,1536]{1,0:T(1,128)S(1)} %mod_part.1.refs_0_), channel_id=1, source_target_pairs={{0,1},{1,0},{2,3},{3,2},{4,5},{5,4},{6,7},{7,6},{8,9},{9,8},{10,11... | collective-permute-start | bytes 18440 | tf_op jit(solution)/shard_map/ppermute | solution.py:728
  18.2 1.2 collective-permute-start.5
  19.9 3.9 %collective-permute-start.6 = (f32[1,6144]{1,0:T(1,128)S(1)}, f32[1,6144]{1,0:T(1,128)S(1)}, u32[]{:S(2)}, u32[]{:S(2)}) collective-permute-start(f32[1,6144]{1,0:T(1,128)S(1)} %shard_map.146.a_ref), channel_id=1, source_target_pairs={{0,4},{4,0},{8,12},{12,8},{16,20},{20,16},{24,28},{28,24},{1,5},{5... | collective-permute-start | bytes 73736 | tf_op jit(solution)/shard_map/ppermute | solution.py:737
  21.5 20.4 %collective-permute-start.10 = (bf16[128,2048]{1,0:T(8,128)(2,1)S(1)}, bf16[128,2048]{1,0:T(8,128)(2,1)S(1)}, u32[]{:S(2)}, u32[]{:S(2)}) collective-permute-start(bf16[128,2048]{1,0:T(8,128)(2,1)S(1)} %get-tuple-element.48), channel_id=1, source_target_pairs={{0,2},{1,3},{2,0},{3,1},{4,6},{5,7},{6,4},{7,5},{8,10},{9,11},{10,... | collective-permute-start | bytes 1572872 | tf_op jit(solution)/shard_map/ppermute | solution.py:573
  24.4 3.9 %collective-permute-start.7 = (f32[1,6144]{1,0:T(1,128)S(1)}, f32[1,6144]{1,0:T(1,128)S(1)}, u32[]{:S(2)}, u32[]{:S(2)}) collective-permute-start(f32[1,6144]{1,0:T(1,128)S(1)} %shard_map.147.a_ref), channel_id=1, source_target_pairs={{0,8},{4,12},{8,0},{12,4},{16,24},{20,28},{24,16},{28,20},{1,9},{5... | collective-permute-start | bytes 73736 | tf_op jit(solution)/shard_map/ppermute | solution.py:737
  28.8 4.9 %collective-permute-start.8 = (f32[1,6144]{1,0:T(1,128)S(1)}, f32[1,6144]{1,0:T(1,128)S(1)}, u32[]{:S(2)}, u32[]{:S(2)}) collective-permute-start(f32[1,6144]{1,0:T(1,128)S(1)} %shard_map.148.refs_3_.refs_4_), channel_id=1, source_target_pairs={{0,16},{4,20},{8,24},{12,28},{16,0},{20,4},{24,8},{28,12},{1,17},{... | collective-permute-start | bytes 73736 | tf_op jit(solution)/shard_map/ppermute | solution.py:737
  32.0 10.4 %collective-permute-start.13 = (bf16[128,1024]{1,0:T(8,128)(2,1)S(1)}, bf16[128,1024]{1,0:T(8,128)(2,1)S(1)}, u32[]{:S(2)}, u32[]{:S(2)}) collective-permute-start(bf16[128,1024]{1,0:T(8,128)(2,1)S(1)} %shard_map.149.a_ref), channel_id=1, source_target_pairs={{0,8},{4,12},{8,0},{12,4},{16,24},{20,28},{24,16},{28,20},{1,9},{5... | collective-permute-start | bytes 786440 | tf_op jit(solution)/shard_map/ppermute | solution.py:745
  33.6 12.4 %collective-permute-start.1 = (bf16[128,2048]{1,0:T(8,128)(2,1)S(1)}, bf16[128,2048]{1,0:T(8,128)(2,1)S(1)}, u32[]{:S(2)}, u32[]{:S(2)}) collective-permute-start(bf16[128,2048]{1,0:T(8,128)(2,1)S(1)} %collective-permute-done.refs_1_), channel_id=1, source_target_pairs={{0,1},{1,0},{2,3},{3,2},{4,5},{5,4},{6,7},{7,6},{8,9},{9,8},{10,11... | collective-permute-start | bytes 1572872 | tf_op jit(solution)/shard_map/ppermute | solution.py:622
  41.9 6.9 %collective-permute-start.11 = (bf16[128,2048]{1,0:T(8,128)(2,1)S(1)}, bf16[128,2048]{1,0:T(8,128)(2,1)S(1)}, u32[]{:S(2)}, u32[]{:S(2)}) collective-permute-start(bf16[128,2048]{1,0:T(8,128)(2,1)S(1)} %collective-permute-done.10.refs_1_), channel_id=1, source_target_pairs={{0,1},{1,0},{2,3},{3,2},{4,5},{5,4},{6,7},{7,6},{8,9},{9,8},{10,11... | collective-permute-start | bytes 1572872 | tf_op jit(solution)/shard_map/ppermute | solution.py:623
  43.0 14.0 %collective-permute-start.14 = (bf16[256,1024]{1,0:T(8,128)(2,1)S(1)}, bf16[256,1024]{1,0:T(8,128)(2,1)S(1)}, u32[]{:S(2)}, u32[]{:S(2)}) collective-permute-start(bf16[256,1024]{1,0:T(8,128)(2,1)S(1)} %shard_map.150.refs_4_.refs_8_.refs_5_), channel_id=1, source_target_pairs={{0,4},{4,0},{8,12},{12,8},{16,20},{20,16},{24,28},{28,24},{1,5},{5... | collective-permute-start | bytes 1572872 | tf_op jit(solution)/shard_map/ppermute | solution.py:745
  44.6 17.5 %collective-permute-start.9 = (bf16[128,2048]{1,0:T(8,128)(2,1)S(1)}, bf16[128,2048]{1,0:T(8,128)(2,1)S(1)}, u32[]{:S(2)}, u32[]{:S(2)}) collective-permute-start(bf16[128,2048]{1,0:T(8,128)(2,1)S(1)} %get-tuple-element.45), channel_id=1, source_target_pairs={{0,2},{1,3},{2,0},{3,1},{4,6},{5,7},{6,4},{7,5},{8,10},{9,11},{10,... | collective-permute-start | bytes 1572872 | tf_op jit(solution)/shard_map/ppermute | solution.py:573
  62.1 6.2 %collective-permute-start.15 = (bf16[128,2048]{1,0:T(8,128)(2,1)S(1)}, bf16[128,2048]{1,0:T(8,128)(2,1)S(1)}, u32[]{:S(2)}, u32[]{:S(2)}) collective-permute-start(bf16[128,2048]{1,0:T(8,128)(2,1)S(1)} %collective-permute-done.9.refs_1_), channel_id=1, source_target_pairs={{0,1},{1,0},{2,3},{3,2},{4,5},{5,4},{6,7},{7,6},{8,9},{9,8},{10,11... | collective-permute-start | bytes 1572872 | tf_op jit(solution)/shard_map/ppermute | solution.py:664
  62.2 16.2 %collective-permute-start.16 = (bf16[256,1024]{1,0:T(8,128)(2,1)S(1)}, bf16[256,1024]{1,0:T(8,128)(2,1)S(1)}, u32[]{:S(2)}, u32[]{:S(2)}) collective-permute-start(bf16[256,1024]{1,0:T(8,128)(2,1)S(1)} %get-tuple-element.61), channel_id=1, source_target_pairs={{4,0},{5,1},{8,4},{9,5},{12,8},{13,9},{16,12},{17,13},{20,16},{21,... | collective-permute-start | bytes 1572872 | tf_op jit(solution)/shard_map/ppermute | solution.py:621
  63.5 26.1 %collective-permute-start.18 = (bf16[256,1024]{1,0:T(8,128)(2,1)S(1)}, bf16[256,1024]{1,0:T(8,128)(2,1)S(1)}, u32[]{:S(2)}, u32[]{:S(2)}) collective-permute-start(bf16[256,1024]{1,0:T(8,128)(2,1)S(1)} %get-tuple-element.64), channel_id=1, source_target_pairs={{0,4},{1,5},{4,8},{5,9},{8,12},{9,13},{12,16},{13,17},{16,20},{17,... | collective-permute-start | bytes 1572872 | tf_op jit(solution)/shard_map/ppermute | solution.py:628
  83.6 33.2 %slice-start = ((s8[8388608]{0:T(1024)(128)(4,1)}), s8[4194304]{0:T(1024)(128)(4,1)S(1)}, s32[]{:S(2)}) async-start(s8[8388608]{0:T(1024)(128)(4,1)} %bitcast.5), calls=%async_computation | async-start | bytes 8388608
  88.9 27.9 %slice-start.1 = ((s8[8388608]{0:T(1024)(128)(4,1)}), s8[4194304]{0:T(1024)(128)(4,1)S(1)}, s32[]{:S(2)}) async-start(s8[8388608]{0:T(1024)(128)(4,1)} %bitcast.5), calls=%async_computation.1 | async-start | bytes 8388608
  95.6 11.3 %collective-permute-start.19 = (bf16[384,512]{1,0:T(8,128)(2,1)S(1)}, bf16[384,512]{1,0:T(8,128)(2,1)S(1)}, u32[]{:S(2)}, u32[]{:S(2)}) collective-permute-start(bf16[384,512]{1,0:T(8,128)(2,1)S(1)} %get-tuple-element.66), channel_id=1, source_target_pairs={{0,1},{1,0},{2,3},{3,2},{4,5},{5,4},{6,7},{7,6},{8,9},{9,8},{10,11... | collective-permute-start | bytes 1179656 | tf_op jit(solution)/shard_map/ppermute | solution.py:694
  95.7 21.1 %collective-permute-start.20 = (bf16[384,512]{1,0:T(8,128)(2,1)S(1)}, bf16[384,512]{1,0:T(8,128)(2,1)S(1)}, u32[]{:S(2)}, u32[]{:S(2)}) collective-permute-start(bf16[384,512]{1,0:T(8,128)(2,1)S(1)} %attend.5), channel_id=1, source_target_pairs={{0,2},{1,3},{2,0},{3,1},{4,6},{5,7},{6,4},{7,5},{8,10},{9,11},{10,... | collective-permute-start | bytes 1179656 | tf_op jit(solution)/shard_map/ppermute | solution.py:682
  106.8 17.9 %collective-permute-start.17 = (bf16[384,512]{1,0:T(8,128)(2,1)S(1)}, bf16[384,512]{1,0:T(8,128)(2,1)S(1)}, u32[]{:S(2)}, u32[]{:S(2)}) collective-permute-start(bf16[384,512]{1,0:T(8,128)(2,1)S(1)} %attend.6), channel_id=1, source_target_pairs={{0,3},{1,2},{2,1},{3,0},{4,7},{5,6},{6,5},{7,4},{8,11},{9,10},{10,... | collective-permute-start | bytes 1179656 | tf_op jit(solution)/shard_map/ppermute | solution.py:684
  (10 other events, 29.9 us)

commit v4 on v3

--- a/solution.py
+++ b/solution.py
@@ -14,6 +14,7 @@
 WIN_ROWS = 8
 WIN_COLS = 16
 REACH = WIN_ROWS // 2
+LUMP = 16
 EPS = 1e-06
 LOG2E = math.log2(math.e)
 BLANK = 2 * WIN_ROWS
@@ -34,14 +35,25 @@
     return pl.CostEstimate(flops=int(flops), bytes_accessed=int(nbytes), transcendentals=int(exps))
 
 
-def mod_kernel(cond_ref, shift_ref, scale_ref, gate_ref, out_ref):
+HBM = pl.BlockSpec(memory_space=pltpu.HBM)
+
+
+def mod_kernel(cond_hbm, *refs):
+    maps, part_ref, cond_ref, held, sems = refs[:3], *refs[3:]
+    copies = [pltpu.make_async_copy(cond_hbm, cond_ref, sems.at[0])]
+    for i, ref in enumerate(maps):
+        copies.append(pltpu.make_async_copy(ref, held.at[i], sems.at[1 + i]))
+    for copy in copies:
+        copy.start()
+    copies[0].wait()
     cond = cond_ref[...].astype(F32)
     lifted = cond / (1.0 + jnp.exp(-cond))
     lifted = jnp.broadcast_to(lifted.reshape(1, -1), (16, cond.shape[0])).astype(BF16)
-    width = shift_ref.shape[1]
-    for i, ref in enumerate((shift_ref, scale_ref, gate_ref)):
-        part = jnp.dot(lifted, ref[...], preferred_element_type=F32)
-        out_ref[:, i * width : (i + 1) * width] = part[:1]
+    width = held.shape[2]
+    for i in range(3):
+        copies[1 + i].wait()
+        part = jnp.dot(lifted, held[i], preferred_element_type=F32)
+        part_ref[:, i * width : (i + 1) * width] = part[:1]
 
 
 def mod_part(cond, mod_shift, mod_scale, mod_gate):
@@ -49,12 +61,45 @@
     return pl.pallas_call(
         mod_kernel,
         out_shape=jax.ShapeDtypeStruct((1, 3 * width), F32),
-        in_specs=[VM] * 4,
+        in_specs=[HBM] * 4,
         out_specs=VM,
+        scratch_shapes=[
+            pltpu.VMEM((rows,), BF16),
+            pltpu.VMEM((3, rows, width), BF16),
+            pltpu.SemaphoreType.DMA((4,)),
+        ],
         name="mod_part",
-        compiler_params=params(8),
+        compiler_params=params(60),
         cost_estimate=cost(96 * rows * width, 6 * rows * width),
     )(cond, mod_shift, mod_scale, mod_gate)
+
+
+def cut_kernel(where_ref, x_ref, *refs):
+    outs, sems = refs[:-1], refs[-1]
+    copies = []
+    for j, out_ref in enumerate(outs):
+        size = out_ref.shape[0]
+        at = jnp.where((where_ref[1] & 1) == 0, j * size, x_ref.shape[0] - (j + 1) * size)
+        at = pl.multiple_of(at, GRID_W)
+        copies.append(pltpu.make_async_copy(x_ref.at[pl.ds(at, size), :], out_ref, sems.at[j]))
+    for copy in copies:
+        copy.start()
+    for copy in copies:
+        copy.wait()
+
+
+def cut_chunks(where, x, count):
+    outs = (jax.ShapeDtypeStruct((x.shape[0] // count, x.shape[1]), x.dtype),) * count
+    return pl.pallas_call(
+        cut_kernel,
+        out_shape=outs,
+        in_specs=[SM, HBM],
+        out_specs=(VM,) * count,
+        scratch_shapes=[pltpu.SemaphoreType.DMA((count,))],
+        name="cut",
+        compiler_params=params(8),
+        cost_estimate=cost(1 << 20, 4 * x.size),
+    )(where, x)
 
 
 def place_kernel(masks, where_ref, *refs):
@@ -118,19 +163,6 @@
 def pick(inner, outer, where):
     outs = jax.ShapeDtypeStruct(inner.shape, inner.dtype)
     return small_call(pick_kernel, (outs, outs), where, inner, outer)
-
-
-def cut_kernel(where_ref, x_ref, *outs):
-    count = x_ref.shape[0]
-    size = outs[0].shape[0]
-    for j, out_ref in enumerate(outs):
-        at = jnp.where((where_ref[1] & 1) == 0, j * size, count - (j + 1) * size)
-        out_ref[...] = x_ref[pl.ds(pl.multiple_of(at, GRID_W), size), :]
-
-
-def cut_chunks(x, count, where):
-    outs = jax.ShapeDtypeStruct((x.shape[0] // count, x.shape[1]), x.dtype)
-    return small_call(cut_kernel, (outs,) * count, where, x)
 
 
 def table_kernel(bias_ref, out_ref):
@@ -179,10 +211,9 @@
     return jnp.concatenate(parts, axis=1)
 
 
-def qkv_kernel(count, heads, tile, take, carried, *refs):
+def qkv_kernel(count, heads, tile, take, *refs):
     where_ref, pieces = refs[0], refs[1 : 1 + count]
     refs = refs[1 + count :]
-    had, refs = refs[:carried], refs[carried:]
     ma_ref, mb_ref, ng_ref, wq_ref, wk_ref, wv_ref, qg_ref, kg_ref, q_ref, kv_ref = refs[:10]
     edge_ref = refs[10] if take else None
     raw, normed, affine = refs[-3:]
@@ -242,13 +273,11 @@
     lax.fori_loop(0, tiles - 1, project, 0)
     project(tiles - 1, 0, True)
     if take:
-        at = 0
-        for ref in had:
-            edge_ref[: ref.shape[0], :] = ref[...]
-            at = ref.shape[0]
-        size = edge_ref.shape[0] - at
-        start = pl.multiple_of(take(where_ref[0], where_ref[1]), GRID_W)
-        edge_ref[at:, :] = kv_ref[pl.ds(start, size), :]
+        starts = take(where_ref[0], where_ref[1])
+        size = edge_ref.shape[0] // len(starts)
+        for i, start in enumerate(starts):
+            rows = pl.ds(pl.multiple_of(start, GRID_W), size)
+            edge_ref[i * size : (i + 1) * size, :] = kv_ref[rows, :]
 
 
 def qkv(
@@ -264,11 +293,10 @@
     heads,
     take=None,
     taken=0,
-    had=(),
 ):
     total = sum(p.shape[0] for p in pieces)
     depth, width = w_query.shape
-    tile = 256 if total % 256 == 0 else 128
+    tile = 384 if total % 384 == 0 else 256 if total % 256 == 0 else 128
     outs = [
         jax.ShapeDtypeStruct((total, width), BF16),
         jax.ShapeDtypeStruct((total, 2 * width), BF16),
@@ -276,9 +304,9 @@
     if take:
         outs.append(jax.ShapeDtypeStruct((taken, 2 * width), BF16))
     return pl.pallas_call(
-        functools.partial(qkv_kernel, len(pieces), heads, tile, take, len(had)),
+        functools.partial(qkv_kernel, len(pieces), heads, tile, take),
         out_shape=tuple(outs),
-        in_specs=[SM] + [VM] * (len(pieces) + len(had) + 8),
+        in_specs=[SM] + [VM] * (len(pieces) + 8),
         out_specs=tuple(VM for _ in outs),
         scratch_shapes=[
             pltpu.VMEM((total, depth), BF16),
@@ -291,7 +319,6 @@
     )(
         where,
         *pieces,
-        *had,
         *mods,
         norm_gain.reshape(1, -1),
         w_query,
@@ -389,31 +416,30 @@
             cbias = cbias_ref[h] * LOG2E
             sums = []
             for r in range(span):
-                rows = slice(r * GRID_W, (r + 1) * GRID_W)
-                tops = None
-                for p in range(key_rows // 2):
-                    cols = slice(p * lines, (p + 1) * lines)
-                    tile = scores[h % 2, rows, cols] * factor
-                    tile = tile + tab_ref[h, spots[r * (key_rows // 2) + p]]
-                    scores[h % 2, rows, cols] = tile
-                    tops = tile if tops is None else jnp.maximum(tops, tile)
-                ctx = scores[h % 2, rows, window : window + lines]
-                for p in range(1, ctx_count // lines):
-                    cols = slice(window + p * lines, window + (p + 1) * lines)
-                    ctx = jnp.maximum(ctx, scores[h % 2, rows, cols])
-                tops = jnp.maximum(tops, ctx * factor + cbias)
-                high = jnp.max(tops, axis=1, keepdims=True)
-                acc = None
-                for p in range(key_rows // 2 + ctx_count // lines):
-                    cols = slice(p * lines, (p + 1) * lines)
-                    tile = scores[h % 2, rows, cols]
-                    if p < key_rows // 2:
+                for sub in range(GRID_W // LUMP):
+                    rows = slice(r * GRID_W + sub * LUMP, r * GRID_W + (sub + 1) * LUMP)
+                    lump = slice(sub * LUMP, (sub + 1) * LUMP)
+                    tiles = []
+                    for p in range(key_rows // 2):
+                        cols = slice(p * lines, (p + 1) * lines)
+                        bias = tab_ref[h, spots[r * (key_rows // 2) + p], lump, :]
+                        tiles.append(scores[h % 2, rows, cols] * factor + bias)
+                    for p in range(ctx_count // lines):
+                        cols = slice(window + p * lines, window + (p + 1) * lines)
+                        tiles.append(scores[h % 2, rows, cols] * factor + cbias)
+                    tops = tiles
+                    while len(tops) > 1:
+                        tops = [
+                            jnp.maximum(*tops[n : n + 2]) if n + 1 < len(tops) else tops[n]
+                            for n in range(0, len(tops), 2)
+                        ]
+                    high = jnp.max(tops[0], axis=1, keepdims=True)
+                    acc = None
+                    for p, tile in enumerate(tiles):
                         tile = jnp.exp2(tile - high)
-                    else:
-                        tile = jnp.exp2(tile * factor - (high - cbias))
-                    acc = tile if acc is None else acc + tile
-                    weights[h % 2, rows, cols] = tile.astype(BF16)
-                sums.append(jnp.sum(acc, axis=1, keepdims=True))
+                        acc = tile if acc is None else acc + tile
+                        weights[h % 2, rows, p * lines : (p + 1) * lines] = tile.astype(BF16)
+                    sums.append(jnp.sum(acc, axis=1, keepdims=True))
             return sums
 
         def combine(h, sums):
@@ -475,48 +501,39 @@
     )(where, context_bias, *queries, *kvs, *ctx, tables)
 
 
-def out_kernel(masks, tile, final, where_ref, *refs):
+def out_kernel(masks, tile, where_ref, *refs):
     count = len(masks)
-    pieces, refs = refs[:count], refs[count:]
-    w_ref = refs[0]
-    before = refs[1:-1]
-    out_ref = refs[-1]
+    pieces = refs[:count]
+    w_ref, resid_ref, ma_ref, mb_ref, out_ref, held = refs[count:]
     depth = pieces[0].shape[1]
     width = w_ref.shape[1]
-
-    def one(i, _):
-        cols = pl.ds(pl.multiple_of(i * tile, tile), tile)
-        total = None
-        for j, piece in enumerate(pieces):
-            rows = pl.ds(pl.multiple_of(masks[j](where_ref[1]) * depth, depth), depth)
-            part = jnp.dot(piece[...], w_ref[rows, cols], preferred_element_type=F32)
-            total = part if total is None else total + part
-        if final:
-            resid_ref, ma_ref, mb_ref = before[:3]
-            for ref in before[3:]:
-                total = total + ref[:, cols]
-            spot = pl.ds(pl.multiple_of(2 * width + i * tile, tile), tile)
-            gate = ma_ref[:, spot] + mb_ref[:, spot]
-            out_ref[:, cols] = (resid_ref[:, cols].astype(F32) + gate * total).astype(BF16)
-        else:
-            out_ref[:, cols] = total
-        return 0
-
-    lax.fori_loop(0, width // tile, one, 0, unroll=2)
-
-
-def out_project(where, pieces, masks, w_out, before=(), final=True):
-    count, width = pieces[0].shape[0], w_out.shape[1]
-    depth = sum(p.shape[1] for p in pieces)
+    for mask, piece in zip(masks, pieces):
+        spot = pl.ds(pl.multiple_of(mask(where_ref[1]) * depth, depth), depth)
+        held[:, spot] = piece[...]
+    for n in range(width // tile):
+        cols = slice(n * tile, (n + 1) * tile)
+        total = jnp.dot(held[...], w_ref[:, cols], preferred_element_type=F32)
+        spot = slice(2 * width + n * tile, 2 * width + (n + 1) * tile)
+        gate = ma_ref[:, spot] + mb_ref[:, spot]
+        out_ref[:, cols] = (resid_ref[:, cols].astype(F32) + gate * total).astype(BF16)
+
+
+def out_project(where, pieces, masks, w_out, resid, mods):
+    count, width = resid.shape
+    depth = w_out.shape[0]
+    tile = 512
     return pl.pallas_call(
-        functools.partial(out_kernel, masks, 256, final),
-        out_shape=jax.ShapeDtypeStruct((count, width), BF16 if final else F32),
-        in_specs=[SM] + [VM] * (len(pieces) + 1 + len(before)),
+        functools.partial(out_kernel, masks, tile),
+        out_shape=jax.ShapeDtypeStruct((count, width), BF16),
+        in_specs=[SM] + [VM] * len(pieces) + [VM, VM, VM, VM],
         out_specs=VM,
+        scratch_shapes=[
+            pltpu.VMEM((count, depth), BF16),
+        ],
         name="out_project",
         compiler_params=params(16),
         cost_estimate=cost(2 * count * width * depth, 2 * depth * width + 8 * count * width),
-    )(where, *pieces, w_out, *before)
+    )(where, *pieces, w_out, resid, *mods)
 
 
 def swap(count, bit):
@@ -525,6 +542,20 @@
 
 def tie(value, other):
     return lax.optimization_barrier((value, other))[0]
+
+
+def gather_context(where, ctx, bits, after):
+    order = bits[-1:] + bits[:-1]
+    for i, bit in enumerate(order):
+        got = lax.ppermute(ctx, "sp", swap(lax.axis_size("sp"), bit))
+        if i + 2 == len(order):
+            return lambda value: gather_last(where, ctx, got, order[-1], value)
+        ctx = join(ctx, tie(got, after), where)
+
+
+def gather_last(where, ctx, got, bit, value):
+    ctx = join(ctx, tie(got, value), where)
+    return [ctx, lax.ppermute(ctx, "sp", swap(lax.axis_size("sp"), bit))]
 
 
 def plain(where, resid, mods, norm_gain, ctx, tables, weights, gains, context_bias, w_out, heads):
@@ -534,6 +565,7 @@
     rows = tokens // GRID_W
     piece = lax.all_gather(resid, "tp", axis=0, tiled=True)
     q, kv = qkv(where, [piece], mods, norm_gain, *weights, *gains, heads)
+    ctx = ctx(kv)
     edge = REACH * GRID_W
     above = lax.ppermute(kv[tokens - edge :], "sp", [(i, i + 1) for i in range(sp - 1)])
     below = lax.ppermute(kv[:edge], "sp", [(i + 1, i) for i in range(sp - 1)])
@@ -555,7 +587,7 @@
     )
     full = lax.all_to_all(attended.reshape(tp, own, -1), "tp", split_axis=0, concat_axis=0)
     masks = [lambda t, i=i: jnp.int32(i) for i in range(tp)]
-    return out_project(where, [full[i] for i in range(tp)], masks, w_out, (resid, *mods))
+    return out_project(where, [full[i] for i in range(tp)], masks, w_out, resid, mods)
 
 
 CHUNKS = 3
@@ -569,7 +601,7 @@
 
 def staged_tokens(where, resid):
     across = []
-    for chunk in cut_chunks(resid, CHUNKS, where):
+    for chunk in cut_chunks(where, resid, CHUNKS):
         across.append(lax.ppermute(chunk, "tp", swap(4, 2)))
     partner = lax.ppermute(resid, "tp", swap(4, 1))
     return partner, across
@@ -607,10 +639,11 @@
 
     def early_at(s, t):
         chip, parity = t >> 1, t & 1
-        return jnp.where(chip == parity, 0, own) + jnp.where(chip == 0, 0, own - edge)
+        return [jnp.where(chip == parity, 0, own) + jnp.where(chip == 0, 0, own - edge)]
 
     def late_at(s, t):
-        return jnp.where((t >> 1) + (t & 1) == 1, 0, chunk)
+        at = jnp.where((t >> 1) + (t & 1) == 1, 0, chunk)
+        return [at, at + 2 * chunk]
 
     down = [(s * tp + t, (s - 1) * tp + t) for s in range(1, sp) for t in range(tp)]
     up = [(s * tp + t, (s + 1) * tp + t) for s in range(sp - 1) for t in range(tp)]
@@ -618,18 +651,16 @@
     late = [p for p in up if p[0] % tp < 2] + [p for p in down if p[0] % tp >= 2]
 
     q0, kv0, edge_kv = project([resid, partner], take=early_at, taken=edge)
+    ctx = ctx(kv0)
     early_kv = lax.ppermute(edge_kv, ("sp", "tp"), early)
     beside0 = lax.ppermute(across[0], "tp", swap(4, 1))
     beside1 = lax.ppermute(tie(across[1], kv0), "tp", swap(4, 1))
-    q1, kv1, edge_kv = project(list(tie((across[0], beside0), kv0)), take=late_at, taken=chunk)
-    q2, kv2, edge_kv = project(
-        list(tie((across[1], beside1), kv1)), take=late_at, taken=2 * chunk, had=(edge_kv,)
-    )
-    late_kv = lax.ppermute(edge_kv, ("sp", "tp"), late)
-
+    q1, kv1, edge_kv = project(
+        list(tie((across[0], beside0, across[1], beside1), kv0)), take=late_at, taken=2 * chunk
+    )
     near = [(0, 0, own), (0, own, own)]
     pair = [(0, chunk), (chunk, chunk)]
-    kv_spec = near + [(j, at, size) for j in (1, 2, 3) for at, size in pair]
+    kv_spec = near + [(1, j * chunk, chunk) for j in range(4)] + [(2, at, size) for at, size in pair]
 
     def block(queries, q_spec, kvs, kv_spec, rows_of):
         return attend(
@@ -659,42 +690,47 @@
 
         return rows_of
 
-    inner = block([q0], near, [kv0, kv1, kv2], kv_spec[:6], home_rows(lambda chip: 1 + chip, False))
-
-    beside2 = lax.ppermute(tie(across[2], inner), "tp", swap(4, 1))
-    q3, kv3 = project(list(tie((across[2], beside2), inner)))
-
-    def far(mask, after):
+    beside2 = lax.ppermute(tie(across[2], kv0), "tp", swap(4, 1))
+    q2, kv2 = project(list(tie((across[2], beside2), kv1)))
+
+    def far(last, waits):
+        outside = [] if waits is None else [jnp.where]
+
         def rows_of(s, t):
             chunks = [row for j in range(CHUNKS) for row in chunk_rows_of(t, j)]
-            outside = jnp.where(t < 2, rows, -REACH)
-            return s * rows, chunks + near_rows(t) + chunks + [outside, (t ^ mask) * block_rows]
+            at = chunks + near_rows(t) + chunks
+            at += [f(t < 2, rows, -REACH) for f in outside]
+            return s * rows, at + [last(t >> 1) * block_rows]
 
         return block(
-            [tie(q1, after), q2, q3],
+            [tie(q1, waits if outside else kv2), q2],
             [(j - 1, at, size) for j, at, size in kv_spec[2:]],
-            [kv0, kv1, kv2, kv3, early_kv],
-            kv_spec + [(4, 0, edge)],
+            [kv0, kv1, kv2] + [early_kv] * len(outside),
+            kv_spec + [(3, 0, edge)] * len(outside),
             rows_of,
         )
 
-    away2 = far(2, kv3)
-    from_2 = lax.ppermute(away2, "tp", swap(4, 2))
-    away3 = far(3, away2)
-    from_3 = lax.ppermute(away3, "tp", swap(4, 3))
-
+    away2 = far(lambda chip: 2 - chip, None)
+    first = lax.ppermute(away2, "tp", swap(4, 2))
+    inner = block(
+        [tie(q0, away2)], near, [kv0, kv1], kv_spec[:6], home_rows(lambda chip: 1 + chip, False)
+    )
+    late_kv = lax.ppermute(tie(edge_kv, away2), ("sp", "tp"), late)
+    away3 = far(lambda chip: 3 - 3 * chip, inner)
+    second = lax.ppermute(away3, "tp", swap(4, 2))
     outer = block(
         [tie(q0, away3)],
         near,
-        [kv0, kv1, kv2, late_kv],
-        kv_spec[:6] + [(3, at, size) for at, size in pair],
+        [kv0, kv1, late_kv],
+        kv_spec[:6] + [(2, at, size) for at, size in pair],
         home_rows(lambda chip: 3 * chip, True),
     )
     send, keep = pick(inner, outer, where)
     from_1 = lax.ppermute(send, "tp", swap(4, 1))
+    send, kept = pick(first, tie(second, send), where)
+    from_3 = lax.ppermute(send, "tp", swap(4, 1))
     masks = [lambda t, i=i: t ^ i for i in range(4)]
-    partial = out_project(where, [keep, from_1, from_2], masks[:3], w_out, final=False)
-    return out_project(where, [from_3], masks[3:], w_out, (resid, *mods, partial))
+    return out_project(where, [keep, from_1, kept, from_3], masks, w_out, resid, mods)
 
 
 def shards(
@@ -717,7 +753,7 @@
     heads = offset_bias.shape[0]
     sp, tp = lax.axis_size("sp"), lax.axis_size("tp")
     block_rows = resid.shape[0] // GRID_W
-    split = tp == 4 and sp > 1 and block_rows == CHUNKS * REACH // 2
+    split = tp == 4 and sp == 8 and block_rows == CHUNKS * REACH // 2
     where = jnp.stack([lax.axis_index("sp"), lax.axis_index("tp")]).astype(jnp.int32)
 
     tables = bias_tables(offset_bias)
@@ -731,7 +767,7 @@
     run = plain
     if split:
         run = functools.partial(staged, staged_in=staged_tokens(where, resid))
-    mods = place_mods(tie(parts, tables), masks, where)
+    mods = place_mods(parts, masks, where)
     bit = 1
     while bit < sp:
         other = lax.ppermute(mods, "sp", swap(sp, bit))
@@ -740,18 +776,14 @@
             mods = add(mods, other, where)
 
     ctx = context_kv(context, norm_gain, w_key, w_value, key_gain, heads)
-    bit = sp // 2
-    while bit:
-        got = lax.ppermute(ctx, "sp", swap(sp, bit))
-        bit //= 2
-        if bit:
-            ctx = join(ctx, got, where)
+    bits = [1 << i for i in range(sp.bit_length() - 1)]
+    ctx = gather_context(where, ctx, bits, other)
     return run(
         where,
         resid,
         (mods, other),
         norm_gain,
-        ctx=[ctx, got],
+        ctx=ctx,
         tables=tables,
         weights=(w_query, w_key, w_value),
         gains=(query_gain, key_gain),

time: 129 us -> 126 us (0.977)
  starting transfers between devices: 36.2 us -> 24.4 us
  waiting for transfers between devices: 33.8 us -> 42.6 us
    ppermute x7 -> x8, starting transfers between devices: 22 us -> 9.29 us  [the longest x2 4.44 us: gather_context(): got = lax.ppermute(ctx, 'sp', swap(lax.axis_size('sp'), bit))]
    ppermute x3, waiting for transfers between devices: 3.2 us -> 11.7 us  [shards(): parts += [lax.ppermute(p, 'tp', swap(tp, bit)) for p in parts]]
    ppermute x7 -> x8, waiting for transfers between devices: 20 us -> 27.4 us  [the longest x2 13.3 us: gather_context(): got = lax.ppermute(ctx, 'sp', swap(lax.axis_size('sp'), bit))]
    ppermute x1, waiting for transfers between devices: 7.36 us -> 0.01 us  [staged(): early_kv = lax.ppermute(edge_kv, ('sp', 'tp'), early)]
    pallas_call x1, Pallas kernels: 0.2 us -> 2.05 us  [mod_part(): pl.pallas_call(mod_kernel, out_shape=jax.ShapeDtypeStruct((1, 3 * width),...]
    pallas_call x4 -> x3, Pallas kernels: 16.4 us -> 14.9 us  [qkv(): pl.pallas_call(functools.partial(qkv_kernel, len(pieces), heads, tile, ta...]
    unnamed x43 -> x35, local copies, waits for them, and re-layouts: 6.97 us -> 6.81 us
  transfers between devices with their start and end apart: 21 -> 22, of which waited for: 10 -> 12; matrix products, arithmetic and copies ran while one was open for 0% -> 0% of each run, Pallas kernels for 32% -> 36%
where the time goes in v4:
time: 126 us; the launch traced here: 125 us
  Pallas kernels  50.7 us (40%)
  waiting for transfers between devices  42.6 us (34%)
  starting transfers between devices  24.4 us (19%)
  local copies, waits for them, and re-layouts  6.81 us (5%)
    pallas_call x4, Pallas kernels, attend(): pl.pallas_call(functools.partial(attend_kernel, heads, span, groups, q_sp...  21.1 us
    pallas_call x3, Pallas kernels, qkv(): pl.pallas_call(functools.partial(qkv_kernel, len(pieces), heads, tile, ta...  14.9 us
    ppermute x2, waiting for transfers between devices, gather_context(): got = lax.ppermute(ctx, 'sp', swap(lax.axis_size('sp'), bit))  13.3 us
    ppermute x3, waiting for transfers between devices, shards(): parts += [lax.ppermute(p, 'tp', swap(tp, bit)) for p in parts]  11.7 us
    unnamed x35, local copies, waits for them, and re-layouts  6.81 us
    ppermute x3, starting transfers between devices, shards(): other = lax.ppermute(mods, 'sp', swap(sp, bit))  6.63 us
    ppermute x3, starting transfers between devices, staged_tokens(): across.append(lax.ppermute(chunk, 'tp', swap(4, 2)))  5.6 us
    ppermute x1, waiting for transfers between devices, staged(): first = lax.ppermute(away2, 'tp', swap(4, 2))  5.35 us
  transfers between devices with their start and end apart: 22, of which 12 were waited for; matrix products, arithmetic and copies ran while one was open for 0% of the time, Pallas kernels for 36%

profile of v4, /device:TPU:0, one launch (start us, length us, event | category | flops | bytes accessed | tf_op | source)
XLA Modules:
  0.0 125.0 jit_solution(12266928142973789898)
XLA Ops:
  0.6 1.5 %copy-done.3 = bf16[384,2048]{1,0:T(8,128)(2,1)S(1)} copy-done((bf16[384,2048]{1,0:T(8,128)(2,1)S(1)}, bf16[384,2048]{1,0:T(8,128)(2,1)}, u32[]{:S(2)}) %copy-start.3) | copy-done | bytes 1572888
  2.0 1.5 %cut.1 = (bf16[128,2048]{1,0:T(8,128)(2,1)}, bf16[128,2048]{1,0:T(8,128)(2,1)S(1)}, bf16[128,2048]{1,0:T(8,128)(2,1)S(1)}) custom-call(s32[2]{0:T(128)S(1)} %pad_add_fusion.where_ref.refs_0_, bf16[384,2048]{1,0:T(8,128)(2,1)S(1)} %copy-done.3), custom_call_target="tpu_custom_call" | custom-call | flops 1048576 | bytes 3145728 | tf_op jit(solution)/shard_map/cut/pallas_call | solution.py:93
  3.5 2.6 %collective-permute-start.7 = (bf16[128,2048]{1,0:T(8,128)(2,1)}, bf16[128,2048]{1,0:T(8,128)(2,1)S(1)}, u32[]{:S(2)}, u32[]{:S(2)}) collective-permute-start(bf16[128,2048]{1,0:T(8,128)(2,1)} %get-tuple-element.37), channel_id=1, source_target_pairs={{0,2},{1,3},{2,0},{3,1},{4,6},{5,7},{6,4},{7,5},{8,10},{9,11},{10,... | collective-permute-start | bytes 1572872 | tf_op jit(solution)/shard_map/ppermute | solution.py:605
  6.2 2.1 %mod_part.1.refs_0_ = f32[1,1536]{1,0:T(1,128)} custom-call(bf16[256]{0:T(256)(128)(2,1)} %cond_hbm.1, bf16[256,512]{1,0:T(8,128)(2,1)} %refs_0_.1, bf16[256,512]{1,0:T(8,128)(2,1)} %refs_1_.2, bf16[256,512]{1,0:T(8,128)(2,1)} %refs_2_.1), custom_call_target="tpu_custom_call" | custom-call | flops 12582912 | bytes 786432 | tf_op jit(solution)/shard_map/mod_part/pallas_call | solution.py:61
  8.4 10.5 %collective-permute-done.1.refs_1_ = f32[1,1536]{1,0:T(1,128)S(1)} collective-permute-done((f32[1,1536]{1,0:T(1,128)}, f32[1,1536]{1,0:T(1,128)S(1)}, u32[]{:S(2)}, u32[]{:S(2)}) %collective-permute-start.1) | collective-permute-done | bytes 6176 | tf_op jit(solution)/shard_map/ppermute | solution.py:764
  21.4 1.8 %collective-permute-start.4 = (f32[1,6144]{1,0:T(1,128)S(1)}, f32[1,6144]{1,0:T(1,128)S(1)}, u32[]{:S(2)}, u32[]{:S(2)}) collective-permute-start(f32[1,6144]{1,0:T(1,128)S(1)} %shard_map.145.a_ref), channel_id=1, source_target_pairs={{0,4},{4,0},{8,12},{12,8},{16,20},{20,16},{24,28},{28,24},{1,5},{5... | collective-permute-start | bytes 73736 | tf_op jit(solution)/shard_map/ppermute | solution.py:773
  23.2 1.5 %collective-permute-start.9 = (bf16[128,2048]{1,0:T(8,128)(2,1)S(1)}, bf16[128,2048]{1,0:T(8,128)(2,1)S(1)}, u32[]{:S(2)}, u32[]{:S(2)}) collective-permute-start(bf16[128,2048]{1,0:T(8,128)(2,1)S(1)} %get-tuple-element.38), channel_id=1, source_target_pairs={{0,2},{1,3},{2,0},{3,1},{4,6},{5,7},{6,4},{7,5},{8,10},{9,11},{10,... | collective-permute-start | bytes 1572872 | tf_op jit(solution)/shard_map/ppermute | solution.py:605
  25.8 1.9 %collective-permute-start.5 = (f32[1,6144]{1,0:T(1,128)S(1)}, f32[1,6144]{1,0:T(1,128)S(1)}, u32[]{:S(2)}, u32[]{:S(2)}) collective-permute-start(f32[1,6144]{1,0:T(1,128)S(1)} %shard_map.146.a_ref), channel_id=1, source_target_pairs={{0,8},{4,12},{8,0},{12,4},{16,24},{20,28},{24,16},{28,20},{1,9},{5... | collective-permute-start | bytes 73736 | tf_op jit(solution)/shard_map/ppermute | solution.py:773
  27.7 2.0 %collective-permute-done.5.b_ref = f32[1,6144]{1,0:T(1,128)S(1)} collective-permute-done((f32[1,6144]{1,0:T(1,128)S(1)}, f32[1,6144]{1,0:T(1,128)S(1)}, u32[]{:S(2)}, u32[]{:S(2)}) %collective-permute-start.5) | collective-permute-done | bytes 24608 | tf_op jit(solution)/shard_map/ppermute | solution.py:773
  30.3 2.9 %collective-permute-start.6 = (f32[1,6144]{1,0:T(1,128)S(1)}, f32[1,6144]{1,0:T(1,128)S(1)}, u32[]{:S(2)}, u32[]{:S(2)}) collective-permute-start(f32[1,6144]{1,0:T(1,128)S(1)} %shard_map.147.refs_3_.refs_5_.refs_6_), channel_id=1, source_target_pairs={{0,16},{4,20},{8,24},{12,28},{16,0},{20,4},{24,8},{28,12},{1,17},{... | collective-permute-start | bytes 73736 | tf_op jit(solution)/shard_map/ppermute | solution.py:773
  33.2 1.5 %collective-permute-start.11 = (bf16[128,2048]{1,0:T(8,128)(2,1)S(1)}, bf16[128,2048]{1,0:T(8,128)(2,1)S(1)}, u32[]{:S(2)}, u32[]{:S(2)}) collective-permute-start(bf16[128,2048]{1,0:T(8,128)(2,1)S(1)} %get-tuple-element.46), channel_id=1, source_target_pairs={{0,2},{1,3},{2,0},{3,1},{4,6},{5,7},{6,4},{7,5},{8,10},{9,11},{10,... | collective-permute-start | bytes 1572872 | tf_op jit(solution)/shard_map/ppermute | solution.py:605
  35.1 1.6 %copy-done.1 = bf16[2048,512]{1,0:T(8,128)(2,1)S(1)} copy-done((bf16[2048,512]{1,0:T(8,128)(2,1)S(1)}, bf16[2048,512]{1,0:T(8,128)(2,1)}, u32[]{:S(2)}) %copy-start.1) | copy-done | bytes 2097176
  36.7 1.4 %copy-done.4 = bf16[384,2048]{1,0:T(8,128)(2,1)S(1)} copy-done((bf16[384,2048]{1,0:T(8,128)(2,1)S(1)}, bf16[384,2048]{1,0:T(8,128)(2,1)}, u32[]{:S(2)}) %copy-start.4) | copy-done | bytes 1572888
  38.1 1.6 %copy-done.6 = bf16[2048,512]{1,0:T(8,128)(2,1)S(1)} copy-done((bf16[2048,512]{1,0:T(8,128)(2,1)S(1)}, bf16[2048,512]{1,0:T(8,128)(2,1)}, u32[]{:S(2)}) %copy-start.6) | copy-done | bytes 2097176
  39.7 7.5 %qkv.3 = (bf16[768,512]{1,0:T(8,128)(2,1)S(1)}, bf16[768,1024]{1,0:T(8,128)(2,1)S(1)}, bf16[256,1024]{1,0:T(8,128)(2,1)S(1)}) custom-call(s32[2]{0:T(128)S(1)} %pad_add_fusion.where_ref.refs_0_, bf16[384,2048]{1,0:T(8,128)(2,1)S(1)} %copy-done.4, bf16[384,2048]{1,0:T(8,128)(2,1)} %collective-permute-done.refs_2_, ...), custom_call_target="tpu_custom_call" | custom-call | flops 4831838208 | bytes 9437184 | tf_op jit(solution)/shard_map/qkv/pallas_call | solution.py:306
  48.3 2.8 %collective-permute-start.13 = (bf16[64,1024]{1,0:T(8,128)(2,1)S(1)}, bf16[64,1024]{1,0:T(8,128)(2,1)S(1)}, u32[]{:S(2)}, u32[]{:S(2)}) collective-permute-start(bf16[64,1024]{1,0:T(8,128)(2,1)S(1)} %context_kv.1.a_ref), channel_id=1, source_target_pairs={{0,16},{4,20},{8,24},{12,28},{16,0},{20,4},{24,8},{28,12},{1,17},{... | collective-permute-start | bytes 393224 | tf_op jit(solution)/shard_map/ppermute | solution.py:550
  51.1 6.9 %collective-permute-done.13.b_ref = bf16[64,1024]{1,0:T(8,128)(2,1)S(1)} collective-permute-done((bf16[64,1024]{1,0:T(8,128)(2,1)S(1)}, bf16[64,1024]{1,0:T(8,128)(2,1)S(1)}, u32[]{:S(2)}, u32[]{:S(2)}) %collective-permute-start.13) | collective-permute-done | bytes 131104 | tf_op jit(solution)/shard_map/ppermute | solution.py:550
  58.6 1.6 %collective-permute-start.14 = (bf16[128,1024]{1,0:T(8,128)(2,1)S(1)}, bf16[128,1024]{1,0:T(8,128)(2,1)S(1)}, u32[]{:S(2)}, u32[]{:S(2)}) collective-permute-start(bf16[128,1024]{1,0:T(8,128)(2,1)S(1)} %shard_map.148.a_ref), channel_id=1, source_target_pairs={{0,4},{4,0},{8,12},{12,8},{16,20},{20,16},{24,28},{28,24},{1,5},{5... | collective-permute-start | bytes 786440 | tf_op jit(solution)/shard_map/ppermute | solution.py:550
  60.3 6.3 %collective-permute-done.14.b_ref = bf16[128,1024]{1,0:T(8,128)(2,1)S(1)} collective-permute-done((bf16[128,1024]{1,0:T(8,128)(2,1)S(1)}, bf16[128,1024]{1,0:T(8,128)(2,1)S(1)}, u32[]{:S(2)}, u32[]{:S(2)}) %collective-permute-start.14) | collective-permute-done | bytes 262176 | tf_op jit(solution)/shard_map/ppermute | solution.py:550
  69.4 1.5 %collective-permute-start.16 = (bf16[256,1024]{1,0:T(8,128)(2,1)S(1)}, bf16[256,1024]{1,0:T(8,128)(2,1)S(1)}, u32[]{:S(2)}, u32[]{:S(2)}) collective-permute-start(bf16[256,1024]{1,0:T(8,128)(2,1)S(1)} %get-tuple-element.58), channel_id=1, source_target_pairs={{4,0},{5,1},{8,4},{9,5},{12,8},{13,9},{16,12},{17,13},{20,16},{21,... | collective-permute-start | bytes 1572872 | tf_op jit(solution)/shard_map/ppermute | solution.py:655
  70.9 4.7 %qkv.4 = (bf16[512,512]{1,0:T(8,128)(2,1)S(1)}, bf16[512,1024]{1,0:T(8,128)(2,1)S(1)}, bf16[256,1024]{1,0:T(8,128)(2,1)S(1)}) custom-call(s32[2]{0:T(128)S(1)} %pad_add_fusion.where_ref.refs_0_, bf16[128,2048]{1,0:T(8,128)(2,1)S(1)} %collective-permute-done.7.refs_1_, bf16[128,2048]{1,0:T(8,128)(2,1)S(1)} %collective-permute-done.8.refs_2_, ...), custom_call_target="tpu_custom_call" | custom-call | flops 3221225472 | bytes 8388608 | tf_op jit(solution)/shard_map/qkv/pallas_call | solution.py:306
  75.6 2.7 %qkv.5 = (bf16[256,512]{1,0:T(8,128)(2,1)S(1)}, bf16[256,1024]{1,0:T(8,128)(2,1)S(1)}) custom-call(s32[2]{0:T(128)S(1)} %pad_add_fusion.where_ref.refs_0_, bf16[128,2048]{1,0:T(8,128)(2,1)S(1)} %collective-permute-done.11.refs_1_, bf16[128,2048]{1,0:T(8,128)(2,1)S(1)} %collective-permute-done.12.refs_2_, f32[1,6144]{1,0:T(1,128)S(1)} %shard_map.147.refs_3_.refs_5_.refs_6_, ...), custom_call_target="tpu_custom_call" | custom-call | flops 1610612736 | bytes 7340032 | tf_op jit(solution)/shard_map/qkv/pallas_call | solution.py:306
  78.3 3.7 %collective-permute-done.15.refs_6_.refs_4_.refs_7_.refs_5_ = bf16[256,1024]{1,0:T(8,128)(2,1)S(1)} collective-permute-done((bf16[256,1024]{1,0:T(8,128)(2,1)S(1)}, bf16[256,1024]{1,0:T(8,128)(2,1)S(1)}, u32[]{:S(2)}, u32[]{:S(2)}) %collective-permute-start.15) | collective-permute-done | bytes 524320 | tf_op jit(solution)/shard_map/ppermute | solution.py:558
  82.1 5.2 %attend.4 = bf16[384,512]{1,0:T(8,128)(2,1)S(1)} custom-call(s32[2]{0:T(128)S(1)} %pad_add_fusion.where_ref.refs_0_, f32[4]{0:T(128)S(1)} %copy-done.13, bf16[512,512]{1,0:T(8,128)(2,1)S(1)} %get-tuple-element.57.refs_0_, bf16[256,512]{1,0:T(8,128)(2,1)S(1)} %get-tuple-element.53.refs_1_, bf16[768,1024]{1,0:T(8,128)(2,1)S(1)} %get-tuple-element.39.refs_2_.refs_1_, ...), custom_call_target="tpu_custom_call" | custom-call | flops 2214592512 | bytes 8388608 | tf_op jit(solution)/shard_map/attend/pallas_call | solution.py:484
  87.3 1.5 %collective-permute-start.17 = (bf16[256,1024]{1,0:T(8,128)(2,1)S(1)}, bf16[256,1024]{1,0:T(8,128)(2,1)S(1)}, u32[]{:S(2)}, u32[]{:S(2)}) collective-permute-start(bf16[256,1024]{1,0:T(8,128)(2,1)S(1)} %get-tuple-element.61), channel_id=1, source_target_pairs={{0,4},{1,5},{4,8},{5,9},{8,12},{9,13},{12,16},{13,17},{16,20},{17,... | collective-permute-start | bytes 1572872 | tf_op jit(solution)/shard_map/ppermute | solution.py:718
  88.8 5.2 %attend.5.inner_ref = bf16[384,512]{1,0:T(8,128)(2,1)S(1)} custom-call(s32[2]{0:T(128)S(1)} %pad_add_fusion.where_ref.refs_0_, f32[4]{0:T(128)S(1)} %copy-done.13, bf16[768,512]{1,0:T(8,128)(2,1)S(1)} %get-tuple-element.59.refs_0_, bf16[768,1024]{1,0:T(8,128)(2,1)S(1)} %get-tuple-element.39.refs_2_.refs_1_, ...), custom_call_target="tpu_custom_call" | custom-call | flops 2214592512 | bytes 8388608 | tf_op jit(solution)/shard_map/attend/pallas_call | solution.py:484
  94.0 5.2 %attend.6 = bf16[384,512]{1,0:T(8,128)(2,1)S(1)} custom-call(s32[2]{0:T(128)S(1)} %pad_add_fusion.where_ref.refs_0_, f32[4]{0:T(128)S(1)} %copy-done.13, bf16[512,512]{1,0:T(8,128)(2,1)S(1)} %get-tuple-element.57.refs_0_, bf16[256,512]{1,0:T(8,128)(2,1)S(1)} %get-tuple-element.53.refs_1_, bf16[768,1024]{1,0:T(8,128)(2,1)S(1)} %get-tuple-element.39.refs_2_.refs_1_, ...), custom_call_target="tpu_custom_call" | custom-call | flops 2214592512 | bytes 8388608 | tf_op jit(solution)/shard_map/attend/pallas_call | solution.py:484
  99.4 2.0 %collective-permute-start.19 = (bf16[384,512]{1,0:T(8,128)(2,1)S(1)}, bf16[384,512]{1,0:T(8,128)(2,1)S(1)}, u32[]{:S(2)}, u32[]{:S(2)}) collective-permute-start(bf16[384,512]{1,0:T(8,128)(2,1)S(1)} %attend.4), channel_id=1, source_target_pairs={{0,2},{1,3},{2,0},{3,1},{4,6},{5,7},{6,4},{7,5},{8,10},{9,11},{10,... | collective-permute-start | bytes 1179656 | tf_op jit(solution)/shard_map/ppermute | solution.py:714
  101.4 5.5 %attend.7.outer_ref = bf16[384,512]{1,0:T(8,128)(2,1)S(1)} custom-call(s32[2]{0:T(128)S(1)} %pad_add_fusion.where_ref.refs_0_, f32[4]{0:T(128)S(1)} %copy-done.13, bf16[768,512]{1,0:T(8,128)(2,1)S(1)} %get-tuple-element.59.refs_0_, bf16[768,1024]{1,0:T(8,128)(2,1)S(1)} %get-tuple-element.39.refs_2_.refs_1_, ...), custom_call_target="tpu_custom_call" | custom-call | flops 2214592512 | bytes 8388608 | tf_op jit(solution)/shard_map/attend/pallas_call | solution.py:484
  107.5 3.8 %collective-permute-done.20.outer_ref = bf16[384,512]{1,0:T(8,128)(2,1)S(1)} collective-permute-done((bf16[384,512]{1,0:T(8,128)(2,1)S(1)}, bf16[384,512]{1,0:T(8,128)(2,1)S(1)}, u32[]{:S(2)}, u32[]{:S(2)}) %collective-permute-start.20) | collective-permute-done | bytes 393248 | tf_op jit(solution)/shard_map/ppermute | solution.py:720
  111.3 5.3 %collective-permute-done.19.inner_ref = bf16[384,512]{1,0:T(8,128)(2,1)S(1)} collective-permute-done((bf16[384,512]{1,0:T(8,128)(2,1)S(1)}, bf16[384,512]{1,0:T(8,128)(2,1)S(1)}, u32[]{:S(2)}, u32[]{:S(2)}) %collective-permute-start.19) | collective-permute-done | bytes 393248 | tf_op jit(solution)/shard_map/ppermute | solution.py:714
  119.7 5.3 %out_project.1 = bf16[384,2048]{1,0:T(8,128)(2,1)} custom-call(s32[2]{0:T(128)S(1)} %pad_add_fusion.where_ref.refs_0_, bf16[384,512]{1,0:T(8,128)(2,1)S(1)} %get-tuple-element.62.refs_0_, bf16[384,512]{1,0:T(8,128)(2,1)S(1)} %collective-permute-done.18.refs_1_, bf16[384,512]{1,0:T(8,128)(2,1)S(1)} %get-tuple-element.65.refs_2_, ...), custom_call_target="tpu_custom_call" | custom-call | flops 3221225472 | bytes 14680064 | tf_op jit(solution)/shard_map/out_project/pallas_call | solution.py:525
  (69 shorter events, 13.4 us)
Async XLA Ops:
  0.0 35.1 %copy-start = (bf16[2048,512]{1,0:T(8,128)(2,1)S(1)}, bf16[2048,512]{1,0:T(8,128)(2,1)}, u32[]{:S(2)}) copy-start(bf16[2048,512]{1,0:T(8,128)(2,1)} %wk_ref.1) | copy-start | bytes 6291460
  0.0 35.1 %collective-permute-start = (bf16[384,2048]{1,0:T(8,128)(2,1)}, bf16[384,2048]{1,0:T(8,128)(2,1)}, u32[]{:S(2)}, u32[]{:S(2)}) collective-permute-start(bf16[384,2048]{1,0:T(8,128)(2,1)} %refs_5_.1), channel_id=1, source_target_pairs={{0,1},{1,0},{2,3},{3,2},{4,5},{5,4},{6,7},{7,6},{8,9},{9,8},{10,11... | collective-permute-start | bytes 4718600 | tf_op jit(solution)/shard_map/ppermute | solution.py:606
  2.0 33.0 %copy-start.9 = (f32[2048]{0:T(1024)S(1)}, f32[2048]{0:T(1024)}, u32[]{:S(2)}) copy-start(f32[2048]{0:T(1024)} %param.20) | copy-start | bytes 24580
  2.0 33.0 %copy-start.11 = (f32[128]{0:T(128)S(1)}, f32[128]{0:T(128)}, u32[]{:S(2)}) copy-start(f32[128]{0:T(128)} %param.26) | copy-start | bytes 1540
  2.0 33.0 %copy-start.12 = (f32[128]{0:T(128)S(1)}, f32[128]{0:T(128)}, u32[]{:S(2)}) copy-start(f32[128]{0:T(128)} %param.25) | copy-start | bytes 1540
  3.5 31.1 %collective-permute-start.7 = (bf16[128,2048]{1,0:T(8,128)(2,1)}, bf16[128,2048]{1,0:T(8,128)(2,1)S(1)}, u32[]{:S(2)}, u32[]{:S(2)}) collective-permute-start(bf16[128,2048]{1,0:T(8,128)(2,1)} %get-tuple-element.37), channel_id=1, source_target_pairs={{0,2},{1,3},{2,0},{3,1},{4,6},{5,7},{6,4},{7,5},{8,10},{9,11},{10,... | collective-permute-start | bytes 1572872 | tf_op jit(solution)/shard_map/ppermute | solution.py:605
  8.2 10.7 %collective-permute-start.1 = (f32[1,1536]{1,0:T(1,128)}, f32[1,1536]{1,0:T(1,128)S(1)}, u32[]{:S(2)}, u32[]{:S(2)}) collective-permute-start(f32[1,1536]{1,0:T(1,128)} %mod_part.1.refs_0_), channel_id=1, source_target_pairs={{0,2},{1,3},{2,0},{3,1},{4,6},{5,7},{6,4},{7,5},{8,10},{9,11},{10,... | collective-permute-start | bytes 18440 | tf_op jit(solution)/shard_map/ppermute | solution.py:764
  8.3 10.7 %collective-permute-start.2 = (f32[1,1536]{1,0:T(1,128)}, f32[1,1536]{1,0:T(1,128)S(1)}, u32[]{:S(2)}, u32[]{:S(2)}) collective-permute-start(f32[1,1536]{1,0:T(1,128)} %mod_part.1.refs_0_), channel_id=1, source_target_pairs={{0,1},{1,0},{2,3},{3,2},{4,5},{5,4},{6,7},{7,6},{8,9},{9,8},{10,11... | collective-permute-start | bytes 18440 | tf_op jit(solution)/shard_map/ppermute | solution.py:764
  19.0 1.2 collective-permute-start.3
  21.4 3.9 %collective-permute-start.4 = (f32[1,6144]{1,0:T(1,128)S(1)}, f32[1,6144]{1,0:T(1,128)S(1)}, u32[]{:S(2)}, u32[]{:S(2)}) collective-permute-start(f32[1,6144]{1,0:T(1,128)S(1)} %shard_map.145.a_ref), channel_id=1, source_target_pairs={{0,4},{4,0},{8,12},{12,8},{16,20},{20,16},{24,28},{28,24},{1,5},{5... | collective-permute-start | bytes 73736 | tf_op jit(solution)/shard_map/ppermute | solution.py:773
  23.2 23.9 %collective-permute-start.9 = (bf16[128,2048]{1,0:T(8,128)(2,1)S(1)}, bf16[128,2048]{1,0:T(8,128)(2,1)S(1)}, u32[]{:S(2)}, u32[]{:S(2)}) collective-permute-start(bf16[128,2048]{1,0:T(8,128)(2,1)S(1)} %get-tuple-element.38), channel_id=1, source_target_pairs={{0,2},{1,3},{2,0},{3,1},{4,6},{5,7},{6,4},{7,5},{8,10},{9,11},{10,... | collective-permute-start | bytes 1572872 | tf_op jit(solution)/shard_map/ppermute | solution.py:605
  25.8 3.9 %collective-permute-start.5 = (f32[1,6144]{1,0:T(1,128)S(1)}, f32[1,6144]{1,0:T(1,128)S(1)}, u32[]{:S(2)}, u32[]{:S(2)}) collective-permute-start(f32[1,6144]{1,0:T(1,128)S(1)} %shard_map.146.a_ref), channel_id=1, source_target_pairs={{0,8},{4,12},{8,0},{12,4},{16,24},{20,28},{24,16},{28,20},{1,9},{5... | collective-permute-start | bytes 73736 | tf_op jit(solution)/shard_map/ppermute | solution.py:773
  30.3 4.8 %collective-permute-start.6 = (f32[1,6144]{1,0:T(1,128)S(1)}, f32[1,6144]{1,0:T(1,128)S(1)}, u32[]{:S(2)}, u32[]{:S(2)}) collective-permute-start(f32[1,6144]{1,0:T(1,128)S(1)} %shard_map.147.refs_3_.refs_5_.refs_6_), channel_id=1, source_target_pairs={{0,16},{4,20},{8,24},{12,28},{16,0},{20,4},{24,8},{28,12},{1,17},{... | collective-permute-start | bytes 73736 | tf_op jit(solution)/shard_map/ppermute | solution.py:773
  33.2 27.1 %collective-permute-start.11 = (bf16[128,2048]{1,0:T(8,128)(2,1)S(1)}, bf16[128,2048]{1,0:T(8,128)(2,1)S(1)}, u32[]{:S(2)}, u32[]{:S(2)}) collective-permute-start(bf16[128,2048]{1,0:T(8,128)(2,1)S(1)} %get-tuple-element.46), channel_id=1, source_target_pairs={{0,2},{1,3},{2,0},{3,1},{4,6},{5,7},{6,4},{7,5},{8,10},{9,11},{10,... | collective-permute-start | bytes 1572872 | tf_op jit(solution)/shard_map/ppermute | solution.py:605
  34.7 36.2 %collective-permute-start.8 = (bf16[128,2048]{1,0:T(8,128)(2,1)S(1)}, bf16[128,2048]{1,0:T(8,128)(2,1)S(1)}, u32[]{:S(2)}, u32[]{:S(2)}) collective-permute-start(bf16[128,2048]{1,0:T(8,128)(2,1)S(1)} %collective-permute-done.7.refs_1_), channel_id=1, source_target_pairs={{0,1},{1,0},{2,3},{3,2},{4,5},{5,4},{6,7},{7,6},{8,9},{9,8},{10,11... | collective-permute-start | bytes 1572872 | tf_op jit(solution)/shard_map/ppermute | solution.py:656
  47.2 21.2 %copy-start.14 = (f32[4,15,31]{2,0,1:T(4,128)S(1)}, f32[4,15,31]{2,0,1:T(4,128)}, u32[]{:S(2)}) copy-start(f32[4,15,31]{2,0,1:T(4,128)} %param.27) | copy-start | bytes 22324
  47.2 23.7 %collective-permute-start.10 = (bf16[128,2048]{1,0:T(8,128)(2,1)S(1)}, bf16[128,2048]{1,0:T(8,128)(2,1)S(1)}, u32[]{:S(2)}, u32[]{:S(2)}) collective-permute-start(bf16[128,2048]{1,0:T(8,128)(2,1)S(1)} %collective-permute-done.9.refs_3_), channel_id=1, source_target_pairs={{0,1},{1,0},{2,3},{3,2},{4,5},{5,4},{6,7},{7,6},{8,9},{9,8},{10,11... | collective-permute-start | bytes 1572872 | tf_op jit(solution)/shard_map/ppermute | solution.py:657
  47.4 23.5 %copy-start.7 = (bf16[2048,512]{1,0:T(8,128)(2,1)S(1)}, bf16[2048,512]{1,0:T(8,128)(2,1)}, u32[]{:S(2)}) copy-start(bf16[2048,512]{1,0:T(8,128)(2,1)} %refs_6_.3) | copy-start | bytes 6291460
  48.3 22.6 %copy-start.2 = (bf16[2048,512]{1,0:T(8,128)(2,1)S(1)}, bf16[2048,512]{1,0:T(8,128)(2,1)}, u32[]{:S(2)}) copy-start(bf16[2048,512]{1,0:T(8,128)(2,1)} %wv_ref.1) | copy-start | bytes 6291460
  48.3 9.7 %collective-permute-start.13 = (bf16[64,1024]{1,0:T(8,128)(2,1)S(1)}, bf16[64,1024]{1,0:T(8,128)(2,1)S(1)}, u32[]{:S(2)}, u32[]{:S(2)}) collective-permute-start(bf16[64,1024]{1,0:T(8,128)(2,1)S(1)} %context_kv.1.a_ref), channel_id=1, source_target_pairs={{0,16},{4,20},{8,24},{12,28},{16,0},{20,4},{24,8},{28,12},{1,17},{... | collective-permute-start | bytes 393224 | tf_op jit(solution)/shard_map/ppermute | solution.py:550
  58.6 8.0 %collective-permute-start.14 = (bf16[128,1024]{1,0:T(8,128)(2,1)S(1)}, bf16[128,1024]{1,0:T(8,128)(2,1)S(1)}, u32[]{:S(2)}, u32[]{:S(2)}) collective-permute-start(bf16[128,1024]{1,0:T(8,128)(2,1)S(1)} %shard_map.148.a_ref), channel_id=1, source_target_pairs={{0,4},{4,0},{8,12},{12,8},{16,20},{20,16},{24,28},{28,24},{1,5},{5... | collective-permute-start | bytes 786440 | tf_op jit(solution)/shard_map/ppermute | solution.py:550
  60.3 15.3 %collective-permute-start.12 = (bf16[128,2048]{1,0:T(8,128)(2,1)S(1)}, bf16[128,2048]{1,0:T(8,128)(2,1)S(1)}, u32[]{:S(2)}, u32[]{:S(2)}) collective-permute-start(bf16[128,2048]{1,0:T(8,128)(2,1)S(1)} %collective-permute-done.11.refs_1_), channel_id=1, source_target_pairs={{0,1},{1,0},{2,3},{3,2},{4,5},{5,4},{6,7},{7,6},{8,9},{9,8},{10,11... | collective-permute-start | bytes 1572872 | tf_op jit(solution)/shard_map/ppermute | solution.py:693
  67.2 14.9 %collective-permute-start.15 = (bf16[256,1024]{1,0:T(8,128)(2,1)S(1)}, bf16[256,1024]{1,0:T(8,128)(2,1)S(1)}, u32[]{:S(2)}, u32[]{:S(2)}) collective-permute-start(bf16[256,1024]{1,0:T(8,128)(2,1)S(1)} %shard_map.149.refs_5_.refs_3_.refs_6_.refs_4_), channel_id=1, source_target_pairs={{0,8},{4,12},{8,0},{12,4},{16,24},{20,28},{24,16},{28,20},{1,9},{5... | collective-permute-start | bytes 1572872 | tf_op jit(solution)/shard_map/ppermute | solution.py:558
  69.4 24.6 %collective-permute-start.16 = (bf16[256,1024]{1,0:T(8,128)(2,1)S(1)}, bf16[256,1024]{1,0:T(8,128)(2,1)S(1)}, u32[]{:S(2)}, u32[]{:S(2)}) collective-permute-start(bf16[256,1024]{1,0:T(8,128)(2,1)S(1)} %get-tuple-element.58), channel_id=1, source_target_pairs={{4,0},{5,1},{8,4},{9,5},{12,8},{13,9},{16,12},{17,13},{20,16},{21,... | collective-permute-start | bytes 1572872 | tf_op jit(solution)/shard_map/ppermute | solution.py:655
  87.3 14.1 %collective-permute-start.17 = (bf16[256,1024]{1,0:T(8,128)(2,1)S(1)}, bf16[256,1024]{1,0:T(8,128)(2,1)S(1)}, u32[]{:S(2)}, u32[]{:S(2)}) collective-permute-start(bf16[256,1024]{1,0:T(8,128)(2,1)S(1)} %get-tuple-element.61), channel_id=1, source_target_pairs={{0,4},{1,5},{4,8},{5,9},{8,12},{9,13},{12,16},{13,17},{16,20},{17,... | collective-permute-start | bytes 1572872 | tf_op jit(solution)/shard_map/ppermute | solution.py:718
  94.0 25.6 %slice-start = ((s8[8388608]{0:T(1024)(128)(4,1)}), s8[4194304]{0:T(1024)(128)(4,1)S(1)}, s32[]{:S(2)}) async-start(s8[8388608]{0:T(1024)(128)(4,1)} %bitcast.5), calls=%async_computation | async-start | bytes 8388608
  99.3 20.4 %slice-start.1 = ((s8[8388608]{0:T(1024)(128)(4,1)}), s8[4194304]{0:T(1024)(128)(4,1)S(1)}, s32[]{:S(2)}) async-start(s8[8388608]{0:T(1024)(128)(4,1)} %bitcast.5), calls=%async_computation.1 | async-start | bytes 8388608
  99.3 12.1 %collective-permute-start.20 = (bf16[384,512]{1,0:T(8,128)(2,1)S(1)}, bf16[384,512]{1,0:T(8,128)(2,1)S(1)}, u32[]{:S(2)}, u32[]{:S(2)}) collective-permute-start(bf16[384,512]{1,0:T(8,128)(2,1)S(1)} %attend.6), channel_id=1, source_target_pairs={{0,2},{1,3},{2,0},{3,1},{4,6},{5,7},{6,4},{7,5},{8,10},{9,11},{10,... | collective-permute-start | bytes 1179656 | tf_op jit(solution)/shard_map/ppermute | solution.py:720
  99.4 17.3 %collective-permute-start.19 = (bf16[384,512]{1,0:T(8,128)(2,1)S(1)}, bf16[384,512]{1,0:T(8,128)(2,1)S(1)}, u32[]{:S(2)}, u32[]{:S(2)}) collective-permute-start(bf16[384,512]{1,0:T(8,128)(2,1)S(1)} %attend.4), channel_id=1, source_target_pairs={{0,2},{1,3},{2,0},{3,1},{4,6},{5,7},{6,4},{7,5},{8,10},{9,11},{10,... | collective-permute-start | bytes 1179656 | tf_op jit(solution)/shard_map/ppermute | solution.py:714
  106.9 12.8 %copy-start.5 = (bf16[384,2048]{1,0:T(8,128)(2,1)S(1)}, bf16[384,2048]{1,0:T(8,128)(2,1)}, u32[]{:S(2)}) copy-start(bf16[384,2048]{1,0:T(8,128)(2,1)} %refs_5_.1) | copy-start | bytes 4718596
  117.3 1.8 %collective-permute-start.21 = (bf16[384,512]{1,0:T(8,128)(2,1)S(1)}, bf16[384,512]{1,0:T(8,128)(2,1)S(1)}, u32[]{:S(2)}, u32[]{:S(2)}) collective-permute-start(bf16[384,512]{1,0:T(8,128)(2,1)S(1)} %get-tuple-element.66), channel_id=1, source_target_pairs={{0,1},{1,0},{2,3},{3,2},{4,5},{5,4},{6,7},{7,6},{8,9},{9,8},{10,11... | collective-permute-start | bytes 1179656 | tf_op jit(solution)/shard_map/ppermute | solution.py:731
  117.4 2.3 %collective-permute-start.18 = (bf16[384,512]{1,0:T(8,128)(2,1)S(1)}, bf16[384,512]{1,0:T(8,128)(2,1)S(1)}, u32[]{:S(2)}, u32[]{:S(2)}) collective-permute-start(bf16[384,512]{1,0:T(8,128)(2,1)S(1)} %get-tuple-element.63), channel_id=1, source_target_pairs={{0,1},{1,0},{2,3},{3,2},{4,5},{5,4},{6,7},{7,6},{8,9},{9,8},{10,11... | collective-permute-start | bytes 1179656 | tf_op jit(solution)/shard_map/ppermute | solution.py:729
  (7 other events, 20.9 us)
